TPU v7x, 512 devices: a 4x2x32 block of a 4x8x32 slice. The times are simulated.
512 devices in a mesh: grp: 2 (over y), sp: 32 (over z), tp: 8 (over x, core).
Axes of the slice: x: 4, y: 2, z: 32, core: 2. Of those that a mesh axis runs over, the one named last changes fastest.
The devices are a block of a 4x8x32 slice.
Arguments:
- latent: bfloat16 [16384, 4096], P(('grp', 'sp')), parts along dimension 0, may hold values from -6 to 6
- context: bfloat16 [512, 4096], P(('grp', 'sp')), parts along dimension 0, may hold values from -6 to 6
- cond_latent: float32 [8192], P(('grp', 'sp')), parts along dimension 0, may hold values from -6 to 6
- cond_context: float32 [8192], P(('grp', 'sp')), parts along dimension 0, may hold values from -6 to 6
- mod_weight: bfloat16 [3, 4096, 4096], P(None, 'sp', 'tp'), may hold values from -0.09375 to 0.09375
- norm_gain: float32 [4096], replicated, may hold values from 0.1 to 1.9
- w_query: bfloat16 [4096, 1024], P('sp', 'tp'), may hold values from -0.09375 to 0.09375
- w_key: bfloat16 [4096, 1024], P('sp', 'tp'), may hold values from -0.09375 to 0.09375
- w_value: bfloat16 [4096, 2048], P('sp', 'tp'), may hold values from -0.09375 to 0.09375
- w_rank: bfloat16 [2, 4096, 64], P(None, 'sp'), may hold values from -0.09375 to 0.09375
- w_decay: bfloat16 [2, 64, 1024], P(None, None, 'tp'), may hold values from -0.75 to 0.75
- decay_bias: float32 [2, 1024], P(None, 'tp'), may hold values from -1 to 20
- decay_shift: float32 [16384, 16], P(('grp', 'sp'), 'tp'), parts along dimension 0, may hold values from -1 to 0
- out_gain: float32 [2048], P('tp'), may hold values from 0.1 to 1.9
- w_out: bfloat16 [2048, 4096], P('tp', 'sp'), may hold values from -0.125 to 0.125
Outputs:
- mixed: bfloat16 [16384, 4096], P(('grp', 'sp')), parts along dimension 0
There are 2 independent parts, one for each index of `grp`. A program takes and returns all parts, laid end to end along the dimension named above; an argument that names none is the same for every part. Nothing has to cross between parts.
All inputs are finite; a program needn't handle non-finite values.
Results may differ from a plain program's by a relative error of at most 0.0095.
Values may be sent and summed in bfloat16 or wider, within the bound.
No kernel may reach another device: no remote copies, remote signals or barrier semaphores. Data moves between devices by JAX's collectives and lax.ppermute only.
A program may use at most 128 MiB of HBM per device.

v0:
```python
import jax
import jax.numpy as jnp
from jax import lax
from jax.sharding import PartitionSpec as P

DK = 64
DV = 128
BLOCK = 64


eps = 1e-06
normalizer = 16.0
precise = lax.Precision.HIGHEST


def sent_to_all(array, axis):
    copies = jnp.broadcast_to(array, (lax.axis_size(axis), *array.shape))
    return lax.all_to_all(copies, axis, split_axis=0, concat_axis=0, tiled=True)


def of_everyone(array, axis):
    return sent_to_all(array, axis).sum(axis=0)


def joined_along(pieces, dim):
    pieces = jnp.moveaxis(pieces, 0, dim)
    shape = pieces.shape
    return pieces.reshape(*shape[:dim], shape[dim] * shape[dim + 1], *shape[dim + 2 :])


def gather_directly(array, axis, dim):
    pieces = sent_to_all(array, axis)
    return joined_along(pieces, dim)


def gather_together(arrays, axis, dims):
    vector = jnp.concatenate([a.reshape(-1) for a in arrays])
    lines, at, outs = (lax.all_gather(vector, axis), 0, [])
    for a, dim in zip(arrays, dims):
        pieces = lines[:, at : at + a.size].reshape(-1, *a.shape)
        outs.append(joined_along(pieces, dim))
        at += a.size
    return tuple(outs)


def all_in_one(array, axis):
    leaves = jax.tree.leaves(array)
    turns = sorted(range(len(leaves)), key=lambda k: -leaves[k].size)
    width = (1, *leaves[turns[0]].shape)[-1]
    lines = [
        jnp.pad(leaves[k].reshape(-1), (0, -leaves[k].size % width)).reshape(-1, width)
        for k in turns
    ]
    both, at, found = (lax.all_gather(jnp.concatenate(lines), axis), 0, {})
    for k, line in zip(turns, lines):
        piece = both[:, at : at + len(line)].reshape(len(both), -1)
        found[k] = piece[:, : leaves[k].size].reshape(-1, *leaves[k].shape)
        at += len(line)
    numbers = iter(range(len(leaves)))
    return jax.tree.map(lambda _: found[next(numbers)], array)


def prefix(array, axis, join, neutral, backward):
    count = lax.axis_size(axis)
    place = lax.axis_index(axis)
    ahead = count - 1 - place if backward else place
    gathered = all_in_one(
        jax.tree.map(
            lambda a, kind: a.astype(kind),
            array,
            jax.tree.map(lambda a: jnp.bfloat16 if a.dtype == jnp.float32 else a.dtype, array),
        ),
        axis,
    )
    state = jax.tree.map(lambda a, e: jnp.zeros_like(a) + jnp.asarray(e, a.dtype), array, neutral)

    def one(turn, state):
        source = count - 1 - turn if backward else turn
        return join(
            state,
            jax.tree.map(
                lambda a, own: lax.dynamic_index_in_dim(a, source, 0, False).astype(own.dtype),
                gathered,
                array,
            ),
        )

    return lax.fori_loop(0, ahead, one, state)


def rounded(tensor):
    return lax.optimization_barrier(tensor.astype(jnp.bfloat16))


def modulated(tokens, norm_gain, shift_row, scale_row):
    widened = tokens.astype(jnp.float32)
    normalized = widened * lax.rsqrt(jnp.mean(widened * widened, axis=-1, keepdims=True) + eps)
    return (normalized * norm_gain * (1.0 + scale_row) + shift_row).astype(jnp.bfloat16)


def project(tokens, weight):
    return rounded(jnp.dot(tokens, weight, preferred_element_type=jnp.float32))


def log_decay(rank_rows, weight, bias):
    return (
        jax.nn.log_sigmoid(jnp.dot(rank_rows, weight, preferred_element_type=jnp.float32) + bias)
        / normalizer
    )


def by_heads(tensor, width):
    return tensor.astype(jnp.float32).reshape(tensor.shape[0], -1, width)


def context_state(key_rows, value_rows, decays, forward):
    running = jnp.cumsum(decays, axis=0)
    if forward:
        factor = jnp.exp(running[-1] - running)
    else:
        factor = jnp.exp(running - decays)
    return jnp.einsum("thd,the->hde", key_rows * factor, value_rows, precision=precise)


def chained(earlier, later):
    return (earlier[0] + later[0], jnp.exp(later[0])[:, :, None] * earlier[1] + later[1])


def segment_chain(queries, key_rows, value_rows, decays):
    length, head_count, width = queries.shape
    blocks = length // BLOCK
    lower_mask = jnp.tril(jnp.ones((BLOCK, BLOCK), dtype=bool))

    def in_blocks(tensor):
        return tensor.reshape(blocks, BLOCK, head_count, tensor.shape[-1])

    def advance(carry, inputs):
        carry_state, offset = carry
        query_block, key_block, value_block, decay_block = inputs
        running = jnp.cumsum(decay_block, axis=0)
        carried = jnp.einsum(
            "chd,hde->che", query_block * jnp.exp(running), carry_state, precision=precise
        )
        flat_running = running.reshape(BLOCK, head_count * width)
        relative = jnp.where(
            lower_mask[:, :, None], flat_running[:, None] - flat_running[None, :], -jnp.inf
        )
        products = (
            jnp.exp(relative) * query_block.reshape(BLOCK, 1, -1) * key_block.reshape(1, BLOCK, -1)
        )
        scores = products.reshape(BLOCK, BLOCK, head_count, width).sum(axis=-1)
        within = jnp.einsum("ijh,jhe->ihe", scores, value_block, precision=precise)
        block_total = running[-1]
        carry_state = jnp.exp(block_total)[:, :, None] * carry_state + jnp.einsum(
            "chd,che->hde",
            key_block * jnp.exp(block_total - running),
            value_block,
            precision=precise,
        )
        lifted = query_block * jnp.exp(offset + running)
        return ((carry_state, offset + block_total), (carried + within, lifted))

    initial = (
        jnp.zeros((head_count, width, value_rows.shape[-1]), jnp.float32),
        jnp.zeros((head_count, width), jnp.float32),
    )
    (final_state, totals), (outputs, lifted) = lax.scan(
        advance,
        initial,
        (in_blocks(queries), in_blocks(key_rows), in_blocks(value_rows), in_blocks(decays)),
    )
    return (
        outputs.reshape(length, head_count, -1),
        lifted.reshape(length, head_count, width),
        (totals, final_state),
    )


def local(
    latent,
    context,
    cond_latent,
    cond_context,
    mod_weight,
    norm_gain,
    w_query,
    w_key,
    w_value,
    w_rank,
    w_decay,
    decay_bias,
    decay_shift,
    out_gain,
    w_out,
):
    silu_latent = jax.nn.silu(cond_latent).astype(jnp.bfloat16)
    silu_context = jax.nn.silu(cond_context).astype(jnp.bfloat16)
    term_latent = jnp.einsum(
        "d,rdc->rc", silu_latent, mod_weight, preferred_element_type=jnp.float32
    )
    term_context = jnp.einsum(
        "d,rdc->rc", silu_context, mod_weight[:2], preferred_element_type=jnp.float32
    )
    terms = jnp.concatenate([term_latent, term_context], axis=0)
    summed_terms = of_everyone(terms, "sp")
    modulation = gather_directly(summed_terms, "tp", 1)
    query_all, key_all, value_all, rank_all, output_all, context_rows = gather_together(
        (w_query, w_key, w_value, w_rank, w_out, context), "sp", (0, 0, 0, 1, 1, 0)
    )
    h_latent = modulated(latent, norm_gain, modulation[0], modulation[1])
    h_context = modulated(context_rows, norm_gain, modulation[3], modulation[4])
    queries = by_heads(project(h_latent, query_all), DK)
    key_rows = by_heads(project(h_latent, key_all), DK)
    value_rows = by_heads(project(h_latent, value_all), DV)
    shift_rows = decay_shift[:, :, None]
    log_fwd = (
        by_heads(log_decay(project(h_latent, rank_all[0]), w_decay[0], decay_bias[0]), DK)
        + shift_rows
    )
    log_bwd = (
        by_heads(log_decay(project(h_latent, rank_all[1]), w_decay[1], decay_bias[1]), DK)
        + shift_rows
    )
    context_keys = by_heads(project(h_context, key_all), DK)
    context_values = by_heads(project(h_context, value_all), DV)
    context_fwd = by_heads(
        log_decay(project(h_context, rank_all[0]), w_decay[0], decay_bias[0]), DK
    )
    context_bwd = by_heads(
        log_decay(project(h_context, rank_all[1]), w_decay[1], decay_bias[1]), DK
    )
    own_fwd = (
        jnp.sum(context_fwd, axis=0),
        context_state(context_keys, context_values, context_fwd, True),
    )
    own_bwd = (
        jnp.sum(context_bwd, axis=0),
        context_state(context_keys, context_values, context_bwd, False),
    )
    out_fwd, lift_fwd, pair_fwd = segment_chain(queries, key_rows, value_rows, log_fwd)
    flipped_out, flipped_lift, pair_bwd = segment_chain(
        jnp.flip(queries, 0), jnp.flip(key_rows, 0), jnp.flip(value_rows, 0), jnp.flip(log_bwd, 0)
    )
    out_bwd = jnp.flip(flipped_out, 0)
    lift_bwd = jnp.flip(flipped_lift, 0)
    zero_pair = (jnp.zeros_like(pair_fwd[0]), jnp.zeros_like(pair_fwd[1]))
    before = prefix(pair_fwd, "sp", chained, zero_pair, False)
    after = prefix(pair_bwd, "sp", chained, zero_pair, True)
    start_fwd = own_fwd[1]
    start_bwd = own_bwd[1]
    entry_forward = chained((zero_pair[0], start_fwd), before)[1]
    entry_bwd = chained((zero_pair[0], start_bwd), after)[1]
    combined = (
        out_fwd
        + out_bwd
        + jnp.einsum("thd,hde->the", lift_fwd, entry_forward, precision=precise)
        + jnp.einsum("thd,hde->the", lift_bwd, entry_bwd, precision=precise)
    )
    combined = combined * lax.rsqrt(jnp.mean(combined * combined, axis=-1, keepdims=True) + eps)
    normed = (combined.reshape(combined.shape[0], -1) * out_gain).astype(jnp.bfloat16)
    partial_out = jnp.dot(normed, output_all, preferred_element_type=jnp.float32)
    summed = lax.psum(partial_out.astype(jnp.bfloat16), "tp").astype(jnp.float32)
    return (latent.astype(jnp.float32) + modulation[2] * summed).astype(jnp.bfloat16)


def solution(mesh):
    return jax.shard_map(
        local,
        mesh=mesh,
        in_specs=(
            P(("grp", "sp"), None),
            P(("grp", "sp"), None),
            P(("grp", "sp")),
            P(("grp", "sp")),
            P(None, "sp", "tp"),
            P(),
            P("sp", "tp"),
            P("sp", "tp"),
            P("sp", "tp"),
            P(None, "sp", None),
            P(None, None, "tp"),
            P(None, "tp"),
            P(("grp", "sp"), "tp"),
            P("tp"),
            P("tp", "sp"),
        ),
        out_specs=P(("grp", "sp"), None),
        check_vma=False,
    )
```

profile of v0, /device:TPU:33, one launch (start us, length us, event | category | flops | bytes accessed | tf_op | source)
XLA Modules:
  0.0 703.8 jit_solution(6498869063182972282)
XLA Ops:
  15.8 46.4 %all-to-all-start = ((f32[32,5,512]{2,1,0:T(8,128)}), f32[32,5,512]{2,1,0:T(8,128)S(1)}, u32[]{:S(2)}, u32[]{:S(2)}) async-start(f32[32,5,512]{2,1,0:T(8,128)} %broadcast_in_dim.58), calls=%async_computation | async-start | bytes 1048576 | tf_op jit(solution)/shard_map/all_to_all | solution.py:18
  62.8 69.2 %all-to-all-done = f32[32,5,512]{2,1,0:T(8,128)S(1)} async-done(((f32[32,5,512]{2,1,0:T(8,128)}), f32[32,5,512]{2,1,0:T(8,128)S(1)}, u32[]{:S(2)}, u32[]{:S(2)}) %all-to-all-start) | async-done | bytes 327712 | tf_op jit(solution)/shard_map/all_to_all | solution.py:18
  132.7 6.1 all-to-all-start.1
  140.8 3.2 all-to-all-done.1
  147.9 67.9 %all-gather.9.cloned.1.call-done = bf16[4718592]{0:T(1024)(128)(2,1)} async-done(((bf16[147456]{0:T(1024)(128)(2,1)}), bf16[4718592]{0:T(1024)(128)(2,1)}) %all-gather.9.cloned.1.call-update) | async-done | bytes 9437200 | tf_op jit(solution)/shard_map/all_gather | solution.py:38
  215.8 9.5 %reshape.363 = bf16[32,147456]{1,0:T(8,128)(2,1)} reshape(bf16[4718592]{0:T(1024)(128)(2,1)} %all-gather.9.cloned.1.call-done) | data formatting | bytes 18874368 | tf_op jit(solution)/shard_map/all_gather | solution.py:38
  225.3 3.6 fusion.111
  239.8 4.0 convert_multiply_fusion.3
  243.8 4.5 slice_bitcast_fusion.2
  248.3 4.2 reshape_reshape.33
  264.7 4.0 reshape.328
  275.4 5.0 mul.248
  283.3 4.5 copy.265
  288.1 15.9 %while.63 = (s32[]{:T(128)}, f32[2,64,128]{2,1,0:T(8,128)S(1)}, f32[2,64]{1,0:T(2,128)S(1)}, f32[4,64,2,128]{3,1,0,2:T(8,128)S(1)}, f32[4,64,2,64]{3,2,1,0:T(2,1...) while((s32[]{:T(128)}, f32[2,64,128]{2,1,0:T(8,128)S(1)}, ...), condition=%wide.region_9.10_spmd.clone, body=%wide.region_6.9_spmd.clone.sunk | while | flops 41005312 | bytes 1522833 | solution.py:167
  305.4 23.1 %while.62 = (s32[]{:T(128)}, f32[2,64,128]{2,1,0:T(8,128)S(1)}, f32[2,64]{1,0:T(2,128)}, f32[4,64,2,128]{3,1,0,2:T(8,128)S(1)}, f32[4,64,2,64]{3,2,1,0:T(2,128)S...) while((s32[]{:T(128)}, f32[2,64,128]{2,1,0:T(8,128)S(1)}, ...), condition=%wide.region_5.6_spmd.clone, body=%wide.region_2.5_spmd.clone.sunk | while | flops 41005312 | bytes 1619605 | solution.py:167
  329.4 4.9 fusion.51
  334.3 2.9 convert_element_type.152
  346.8 3.4 copy.269
  350.2 3.3 copy.232
  360.4 65.6 %all-gather.13.cloned.1.call-done = bf16[32,129,128]{2,1,0:T(8,128)(2,1)} async-done(((bf16[1,129,128]{2,1,0:T(8,128)(2,1)}), bf16[32,129,128]{2,1,0:T(8,128)(2,1)}) %all-gather.13.cloned.1.call-update) | async-done | bytes 1056784 | tf_op jit(solution)/shard_map/all_gather | solution.py:54
  427.2 4.3 while.61
  431.6 123.5 %all-gather.11.cloned.1.call-done = bf16[32,129,128]{2,1,0:T(8,128)(2,1)} async-done(((bf16[1,129,128]{2,1,0:T(8,128)(2,1)}), bf16[32,129,128]{2,1,0:T(8,128)(2,1)}) %all-gather.11.cloned.1.call-update) | async-done | bytes 1056784 | tf_op jit(solution)/shard_map/all_gather | solution.py:54
  564.4 129.2 %all-reduce.2.cloned.1.call-done = bf16[256,4096]{1,0:T(8,128)(2,1)} async-done(((bf16[256,4096]{1,0:T(8,128)(2,1)}), bf16[256,4096]{1,0:T(8,128)(2,1)}) %all-reduce.2.cloned.1.call-update) | async-done | bytes 2097168 | tf_op jit(solution)/shard_map/psum | solution.py:262
  693.6 3.7 fusion.57
  (376 shorter events, 119.6 us)
Async XLA Ops:
  6.5 55.7 %copy-start = (bf16[256,4096]{1,0:T(8,128)(2,1)S(1)}, bf16[256,4096]{1,0:T(8,128)(2,1)}, u32[]{:S(2)}) copy-start(bf16[256,4096]{1,0:T(8,128)(2,1)} %param.23) | copy-start | bytes 6291460
  6.5 209.2 %all-gather.9.cloned.1.call-start = ((), (), s32[]{:S(2)}) async-start(), calls=%async_computation.3 | async-start | bytes 9732096 | tf_op jit(solution)/shard_map/all_gather | solution.py:38
  13.7 49.0 %copy-start.28 = (f32[4096]{0:T(1024)S(1)}, f32[4096]{0:T(1024)}, u32[]{:S(2)}) copy-start(f32[4096]{0:T(1024)} %param.28) | copy-start | bytes 49156
  15.8 122.9 %copy-start.32 = (f32[2,128]{1,0:T(2,128)S(1)}, f32[2,128]{1,0:T(2,128)}, u32[]{:S(2)}) copy-start(f32[2,128]{1,0:T(2,128)} %param.34) | copy-start | bytes 3076
  15.8 124.2 %copy-start.30 = (f32[256,2]{0,1:T(2,128)S(1)}, f32[256,2]{0,1:T(2,128)}, u32[]{:S(2)}) copy-start(f32[256,2]{0,1:T(2,128)} %param.35) | copy-start | bytes 6148
  15.8 116.2 %all-to-all-start = ((f32[32,5,512]{2,1,0:T(8,128)}), f32[32,5,512]{2,1,0:T(8,128)S(1)}, u32[]{:S(2)}, u32[]{:S(2)}) async-start(f32[32,5,512]{2,1,0:T(8,128)} %broadcast_in_dim.58), calls=%async_computation | async-start | bytes 1048576 | tf_op jit(solution)/shard_map/all_to_all | solution.py:18
  132.7 11.3 %all-to-all-start.1 = ((f32[8,5,512]{2,1,0:T(8,128)}), f32[8,5,512]{2,1,0:T(8,128)S(1)}, u32[]{:S(2)}, u32[]{:S(2)}) async-start(f32[8,5,512]{2,1,0:T(8,128)} %broadcast_in_dim.59), calls=%async_computation.1 | async-start | bytes 262144 | tf_op jit(solution)/shard_map/all_to_all | solution.py:18
  138.7 287.3 %all-gather.13.cloned.1.call-start = ((), (), s32[]{:S(2)}) async-start(), calls=%async_computation.5 | async-start | bytes 1148928 | tf_op jit(solution)/shard_map/all_gather | solution.py:54
  283.2 4.6 copy-start.13
  283.2 4.8 copy-start.5
  283.2 4.8 copy-start.29
  288.0 16.9 %copy-start.25 = (f32[256,2]{1,0:T(8,128)S(1)}, f32[256,2]{1,0:T(8,128)}, u32[]{:S(2)}) copy-start(f32[256,2]{1,0:T(8,128)} %copy.238) | copy-start | bytes 6148
  304.9 250.2 %all-gather.11.cloned.1.call-start = ((), (), s32[]{:S(2)}) async-start(), calls=%async_computation.4 | async-start | bytes 1148928 | tf_op jit(solution)/shard_map/all_gather | solution.py:54
  305.4 24.0 %copy-start.21 = (f32[1,32,8,128]{3,1,2,0:T(8,128)S(1)}, f32[1,32,8,128]{3,1,2,0:T(8,128)}, u32[]{:S(2)}) copy-start(f32[1,32,8,128]{3,1,2,0:T(8,128)} %copy.266) | copy-start | bytes 393220
  305.4 24.0 %copy-start.22 = (f32[1,32,8,128]{3,1,2,0:T(8,128)S(1)}, f32[1,32,8,128]{3,1,2,0:T(8,128)}, u32[]{:S(2)}) copy-start(f32[1,32,8,128]{3,1,2,0:T(8,128)} %copy.268) | copy-start | bytes 393220
  305.4 24.0 %copy-start.23 = (f32[1,32,8,128]{3,1,2,0:T(8,128)S(1)}, f32[1,32,8,128]{3,1,2,0:T(8,128)}, u32[]{:S(2)}) copy-start(f32[1,32,8,128]{3,1,2,0:T(8,128)} %copy.267) | copy-start | bytes 393220
  346.4 347.1 %all-reduce.2.cloned.1.call-start = ((), (), s32[]{:S(2)}) async-start(), calls=%async_computation.2 | async-start | bytes 4194304 | tf_op jit(solution)/shard_map/psum | solution.py:262
  350.2 5.7 copy-start.15
  350.2 6.7 copy-start.19
  355.6 4.8 copy-start.7
  431.6 127.2 %copy-start.9 = (f32[256,128]{0,1:T(8,128)S(1)}, f32[256,128]{0,1:T(8,128)}, u32[]{:S(2)}) copy-start(f32[256,128]{0,1:T(8,128)} %copy.215) | copy-start | bytes 393220
  431.6 127.2 %copy-start.26 = (bf16[256,256]{1,0:T(8,128)(2,1)S(1)}, bf16[256,256]{1,0:T(8,128)(2,1)}, u32[]{:S(2)}) copy-start(bf16[256,256]{1,0:T(8,128)(2,1)} %convolution_convert_fusion.1) | copy-start | bytes 393220
  431.6 127.5 %copy-start.8 = (f32[64,2,2,128]{3,0,1,2:T(8,128)S(1)}, f32[64,2,2,128]{3,0,1,2:T(8,128)}, u32[]{:S(2)}) copy-start(f32[64,2,2,128]{3,0,1,2:T(8,128)} %copy-done.7) | copy-start | bytes 393220
  564.3 129.2 %copy-start.1 = (bf16[256,4096]{1,0:T(8,128)(2,1)S(1)}, bf16[256,4096]{1,0:T(8,128)(2,1)}, u32[]{:S(2)}) copy-start(bf16[256,4096]{1,0:T(8,128)(2,1)} %param.23) | copy-start | bytes 6291460
  (22 other events, 36.5 us)
Sparse Core Ops, SparseCore 0:
  12.7 203.0 all-gather.8
  305.0 120.9 all-gather.12
  428.1 126.9 all-gather.10
  564.5 128.9 all-reduce.1
where the time goes:
time: 708 us; the launch traced here: 704 us
  waiting for transfers between devices  459 us (65%)
  local copies, waits for them, and re-layouts  92.2 us (13%)
  other arithmetic  57.8 us (8%)
  starting transfers between devices  52.6 us (7%)
  matrix products  26.6 us (4%)
  between operations  14 us (2%)
    all_gather x2, waiting for transfers between devices, all_in_one(): both, at, found = (lax.all_gather(jnp.concatenate(lines), axis), 0, {})  189 us
    psum x1, waiting for transfers between devices, local(): lax.psum(partial_out.astype(jnp.bfloat16), 'tp').astype(jnp.float32)  129 us
    all_to_all x2, waiting for transfers between devices, sent_to_all(): return lax.all_to_all(copies, axis, split_axis=0, concat_axis=0, tiled=True)  72.3 us
    all_gather x1, waiting for transfers between devices, gather_together(): lines, at, outs = (lax.all_gather(vector, axis), 0, [])  67.9 us
    all_to_all x2, starting transfers between devices, sent_to_all(): return lax.all_to_all(copies, axis, split_axis=0, concat_axis=0, tiled=True)  52.5 us
    unnamed x98, local copies, waits for them, and re-layouts  26.4 us
    reduce_sum x8, other arithmetic, advance(): scores = products.reshape(BLOCK, BLOCK, head_count, width).sum(axis=-1)  16.1 us
  transfers between devices with their start and end apart: 6, of which 6 were waited for; matrix products, arithmetic and copies ran while one was open for 10% of the time, Pallas kernels for 0%

commit v1 on v0

v1 whole, which is shorter than its diff:
```python
import jax
import jax.numpy as jnp
from jax import lax
from jax.experimental import pallas as pl
from jax.experimental.pallas import tpu as pltpu
from jax.sharding import PartitionSpec as P

DK = 64
DV = 128
eps = 1e-06
normalizer = 16.0
f32 = jnp.float32
bf16 = jnp.bfloat16
VMEM_LIMIT = 50 * 1024 * 1024


def sent_to_all(array, axis):
    copies = jnp.broadcast_to(array, (lax.axis_size(axis), *array.shape))
    return lax.all_to_all(copies, axis, split_axis=0, concat_axis=0, tiled=True)


def dot(a, b):
    return jnp.dot(a, b, preferred_element_type=f32)


def dot_nt(a, b):
    return lax.dot_general(a, b, (((1,), (1,)), ((), ())), preferred_element_type=f32)


def dot_tn(a, b):
    return lax.dot_general(a, b, (((0,), (0,)), ((), ())), preferred_element_type=f32)


def halves(x):
    high = x.astype(bf16)
    low = (x - high.astype(f32)).astype(bf16)
    return high, low


def iota(shape, dim):
    return lax.broadcasted_iota(jnp.int32, shape, dim)


def log_sigmoid(u):
    return jnp.minimum(u, 0.0) - jnp.log1p(jnp.exp(-jnp.abs(u)))


def head_state(keys, values):
    both = dot_tn(keys, values)
    rows = iota((2 * DK, DV), 0)
    return jnp.where(rows < DK, both[:, :DV], both[:, DV:])


def mixing_kernel(
    h_ref, wqk_ref, wv_ref, wr_ref, wd_ref, bias_ref, shift_ref,
    loc_ref, lift_ref, send_ref, acc,
):
    step = pl.program_id(0)
    T = shift_ref.shape[0]
    C = h_ref.shape[0] - T
    h = h_ref[...]

    @pl.when(step == 0)
    def _():
        acc[...] = jnp.zeros_like(acc)

    acc[:, 0:256] += dot(h, wqk_ref[...])
    acc[:, 256:512] += dot(h, wv_ref[...])
    acc[:, 512:640] += dot(h, wr_ref[...])

    @pl.when(step == pl.num_programs(0) - 1)
    def _():
        q16 = acc[0:T, 0:128].astype(bf16)
        k16 = acc[0:T, 128:256].astype(bf16)
        v = acc[0:T, 256:512].astype(bf16)
        q = q16.astype(f32)
        k = k16.astype(f32)
        ranks = acc[:, 512:640].astype(bf16)
        logs = log_sigmoid(dot(ranks, wd_ref[...]) + bias_ref[...]) / normalizer
        lat = logs[0:T] + shift_ref[...]
        f_high, f_low = halves(lat[:, 0:128])
        b_high, b_low = halves(lat[:, 128:256])
        f_pair = jnp.concatenate([f_high, f_low], axis=1)
        b_pair = jnp.concatenate([b_high, b_low], axis=1)

        def summed(where, pair):
            both = dot(jnp.where(where, 1.0, 0.0).astype(bf16), pair)
            return both[:, 0:128] + both[:, 128:256]

        r = iota((T, T), 0)
        s = iota((T, T), 1)
        lane = iota((T, 128), 1)
        row = iota((T, 128), 0)
        first = lane < DK
        zero = jnp.zeros((T, 128), bf16)

        def scores(qs, ks):
            return (
                dot_nt(qs, jnp.where(first, ks, zero)),
                dot_nt(qs, jnp.where(first, zero, ks)),
            )

        s0, s1 = scores(q16, k16)
        s0 = 2.0 * s0
        s1 = 2.0 * s1
        m = 1
        while m < T:
            base = (r // (2 * m)) * (2 * m)
            ref = base + m
            upper = r >= ref
            lower = r < ref
            d_f = (upper & (s >= ref) & (s <= r)) | (lower & (s > r) & (s < ref))
            d_b = (upper & (s >= ref) & (s < r)) | (lower & (s >= r) & (s < ref))
            fac_f = jnp.exp(summed(d_f, f_pair))
            fac_b = jnp.exp(summed(d_b, b_pair))
            up = (row & m) != 0
            qs = (q * jnp.where(up, fac_f, fac_b)).astype(bf16)
            ks = (k * jnp.where(up, fac_b, fac_f)).astype(bf16)
            m0, m1 = scores(qs, ks)
            pick = ((r ^ s) >= m) & ((r ^ s) < 2 * m)
            s0 = jnp.where(pick, m0, s0)
            s1 = jnp.where(pick, m1, s1)
            m *= 2
        loc_ref[:, 0:128] = dot(s0.astype(bf16), v[:, 0:128])
        loc_ref[:, 128:256] = dot(s1.astype(bf16), v[:, 128:256])

        lift_ref[:, 0:128] = (q * jnp.exp(summed(s <= r, f_pair))).astype(bf16)
        lift_ref[:, 128:256] = (q * jnp.exp(summed(s >= r, b_pair))).astype(bf16)
        k_f = (k * jnp.exp(summed(s > r, f_pair))).astype(bf16)
        k_b = (k * jnp.exp(summed(s < r, b_pair))).astype(bf16)

        def total(high, low):
            ones = jnp.ones((high.shape[0], 128), bf16)
            return jnp.exp(dot_tn(high, ones) + dot_tn(low, ones))

        n = send_ref.shape[0]
        st_f = head_state(k_f, v)
        st_b = head_state(k_b, v)
        half = n // 2
        send_ref[0:half, 0:8, :] = st_f.reshape(half, 8, 128).astype(bf16)
        send_ref[half:n, 0:8, :] = st_b.reshape(half, 8, 128).astype(bf16)

        crow = iota((C, 128), 0)
        live = crow < 8
        kc = jnp.where(live, acc[T : T + C, 128:256].astype(bf16).astype(f32), 0.0)
        vc = acc[T : T + C, 256:512].astype(bf16)
        ctx_f = jnp.where(live, logs[T : T + C, 0:128], 0.0)
        ctx_b = jnp.where(live, logs[T : T + C, 128:256], 0.0)
        cf_high, cf_low = halves(ctx_f)
        cb_high, cb_low = halves(ctx_b)
        rc = iota((C, C), 0)
        sc = iota((C, C), 1)
        kc_f = (kc * jnp.exp(summed(sc > rc, jnp.concatenate([cf_high, cf_low], axis=1)))).astype(bf16)
        kc_b = (kc * jnp.exp(summed(sc < rc, jnp.concatenate([cb_high, cb_low], axis=1)))).astype(bf16)
        send_ref[0:half, 8:16, :] = head_state(kc_f, vc).reshape(half, 8, 128).astype(bf16)
        send_ref[half:n, 8:16, :] = head_state(kc_b, vc).reshape(half, 8, 128).astype(bf16)

        lanes = iota((128, 128), 1)

        def packed(latent_total, context_total):
            lh, ll = halves(latent_total)
            ch, cl = halves(context_total)
            lat2 = jnp.where(lanes < 32, lh.astype(f32), ll.astype(f32))
            ctx2 = jnp.where(lanes < 96, ch.astype(f32), cl.astype(f32))
            return jnp.where(lanes < 64, lat2, ctx2).reshape(half, 8, 128).astype(bf16)

        send_ref[0:half, 16:24, :] = packed(total(f_high, f_low), total(cf_high, cf_low))
        send_ref[half:n, 16:24, :] = packed(total(b_high, b_low), total(cb_high, cb_low))


def mixing(h, gathered, decay_weight, decay_bias, shifts, members):
    T = shifts.shape[0]
    rows, width = h.shape
    steps = 8
    depth = width // steps
    whole = lambda *shape: pl.BlockSpec(shape, lambda i: (0,) * len(shape))
    return pl.pallas_call(
        mixing_kernel,
        grid=(steps,),
        in_specs=[
            pl.BlockSpec((rows, depth), lambda i: (0, i)),
            pl.BlockSpec((depth, 256), lambda i: (i, 1)),
            pl.BlockSpec((depth, 256), lambda i: (i, 2)),
            pl.BlockSpec((depth, 128), lambda i: (i, 6)),
            whole(128, 256),
            whole(1, 256),
            whole(T, 256),
        ],
        out_specs=[whole(T, 256), whole(T, 256), whole(members, 24, 128)],
        out_shape=[
            jax.ShapeDtypeStruct((T, 256), f32),
            jax.ShapeDtypeStruct((T, 256), bf16),
            jax.ShapeDtypeStruct((members, 24, 128), bf16),
        ],
        scratch_shapes=[pltpu.VMEM((rows, 640), f32)],
        compiler_params=pltpu.CompilerParams(vmem_limit_bytes=VMEM_LIMIT),
        name="mixing",
    )(h, gathered, gathered, gathered, decay_weight, decay_bias, shifts)


def chain_kernel(in_ref, out_ref):
    n = in_ref.shape[0]
    backward = lax.axis_index("sp") >= n // 2

    def place(i):
        return jnp.where(backward, n - 1 - i, i)

    def decay(at, lane):
        rows = in_ref[at, 16:24, :].astype(f32)
        return rows[:, lane : lane + 1] + rows[:, lane + 32 : lane + 33]

    state = jnp.zeros((8, 128), f32)
    for i in range(n):
        at = place(i)
        state = decay(at, 64) * state + in_ref[at, 8:16, :].astype(f32)
    for i in range(n):
        at = place(i)
        out_ref[at] = state.astype(bf16)
        if i + 1 < n:
            state = decay(at, 0) * state + in_ref[at, 0:8, :].astype(f32)


def chain(received):
    n = received.shape[0]
    return pl.pallas_call(
        chain_kernel,
        out_shape=jax.ShapeDtypeStruct((n, 8, 128), bf16),
        in_specs=[pl.BlockSpec(memory_space=pltpu.VMEM)],
        out_specs=pl.BlockSpec(memory_space=pltpu.VMEM),
        name="chain",
    )(received)


def output_kernel(loc_ref, lift_ref, entry_ref, gain_ref, w_ref, out_ref, normed):
    @pl.when(pl.program_id(0) == 0)
    def _():
        entry = entry_ref[...].astype(f32)
        head = (iota(entry.shape, 0) // DK) % 2
        spread = jnp.concatenate(
            [jnp.where(head == 0, entry, 0.0), jnp.where(head == 1, entry, 0.0)], axis=1
        ).astype(bf16)
        combined = loc_ref[...] + dot(lift_ref[...], spread)
        for g in range(2):
            part = combined[:, g * DV : (g + 1) * DV]
            scaled = part * lax.rsqrt(jnp.mean(part * part, axis=-1, keepdims=True) + eps)
            normed[:, g * DV : (g + 1) * DV] = (
                scaled * gain_ref[:, g * DV : (g + 1) * DV]
            ).astype(bf16)

    w = w_ref[...]
    for j in range(w.shape[0] // 128):
        rows = slice(j * 128, (j + 1) * 128)
        out_ref[0, :, rows] = (
            dot(normed[:, 0:128], w[rows, 0:128]) + dot(normed[:, 128:256], w[rows, 128:256])
        ).astype(bf16)


def output(loc, lift, entry, gain, gathered, pieces):
    T = loc.shape[0]
    width = gathered.shape[0] // pieces
    whole = lambda *shape: pl.BlockSpec(shape, lambda i: (0,) * len(shape))
    return pl.pallas_call(
        output_kernel,
        grid=(pieces,),
        in_specs=[
            whole(T, 256),
            whole(T, 256),
            whole(256, 128),
            whole(1, 256),
            pl.BlockSpec((width, 256), lambda i: (i, 0)),
        ],
        out_specs=pl.BlockSpec((1, T, width), lambda i: (i, 0, 0)),
        out_shape=jax.ShapeDtypeStruct((pieces, T, width), bf16),
        scratch_shapes=[pltpu.VMEM((T, 256), bf16)],
        compiler_params=pltpu.CompilerParams(vmem_limit_bytes=VMEM_LIMIT),
        name="output",
    )(loc, lift, entry, gain, gathered)


def local(
    latent,
    context,
    cond_latent,
    cond_context,
    mod_weight,
    norm_gain,
    w_query,
    w_key,
    w_value,
    w_rank,
    w_decay,
    decay_bias,
    decay_shift,
    out_gain,
    w_out,
):
    T, width = latent.shape
    members = lax.axis_size("sp")
    pieces = lax.axis_size("tp")
    depth = w_query.shape[0]
    own = jnp.concatenate(
        [w_out[:depth], w_out[depth:], w_query, w_key, w_value, w_rank[0], w_rank[1]], axis=1
    )
    gathered = lax.all_gather(own, "sp").reshape(members * depth, own.shape[1])

    silu = jnp.stack([jax.nn.silu(cond_latent), jax.nn.silu(cond_context)]).astype(bf16)
    terms = jnp.einsum("nd,rdc->nrc", silu, mod_weight, preferred_element_type=f32)
    terms = jnp.concatenate([terms[0], terms[1, :2]], axis=0)
    summed_terms = lax.all_gather(terms, "sp").sum(axis=0)
    rows = sent_to_all(summed_terms, "tp")
    modulation = jnp.moveaxis(rows, 0, 1).reshape(rows.shape[1], width)

    extra = 16 - context.shape[0]
    tokens = jnp.concatenate([latent, context, jnp.zeros((extra, width), bf16)], axis=0)
    widened = tokens.astype(f32)
    normalized = widened * lax.rsqrt(jnp.mean(widened * widened, axis=-1, keepdims=True) + eps)
    is_latent = (jnp.arange(T + 16) < T)[:, None]
    scale = jnp.where(is_latent, modulation[1], modulation[4])
    shift = jnp.where(is_latent, modulation[0], modulation[3])
    h = (normalized * norm_gain * (1.0 + scale) + shift).astype(bf16)

    decay_weight = jnp.zeros((128, 256), bf16)
    decay_weight = decay_weight.at[:64, :128].set(w_decay[0]).at[64:, 128:].set(w_decay[1])
    shifts = jnp.repeat(decay_shift, DK, axis=1)
    shifts = jnp.concatenate([shifts, shifts], axis=1)

    loc, lift, send = mixing(
        h, gathered, decay_weight, decay_bias.reshape(1, 256), shifts, members
    )
    received = lax.all_to_all(send, "sp", split_axis=0, concat_axis=0, tiled=True)
    entries = lax.all_to_all(chain(received), "sp", split_axis=0, concat_axis=0, tiled=True)
    parts = output(
        loc, lift, entries.reshape(members * 8, 128), out_gain.reshape(1, 256), gathered, pieces
    )
    parts = lax.all_to_all(parts, "tp", split_axis=0, concat_axis=0, tiled=True)
    summed = parts.astype(f32).sum(axis=0)
    columns = width // pieces
    own_latent = lax.dynamic_slice_in_dim(latent, lax.axis_index("tp") * columns, columns, 1)
    mixed = (own_latent.astype(f32) + summed_terms[2] * summed).astype(bf16)
    return jnp.moveaxis(sent_to_all(mixed, "tp"), 0, 1).reshape(T, width)


def solution(mesh):
    return jax.shard_map(
        local,
        mesh=mesh,
        in_specs=(
            P(("grp", "sp"), None),
            P(("grp", "sp"), None),
            P(("grp", "sp")),
            P(("grp", "sp")),
            P(None, "sp", "tp"),
            P(),
            P("sp", "tp"),
            P("sp", "tp"),
            P("sp", "tp"),
            P(None, "sp", None),
            P(None, None, "tp"),
            P(None, "tp"),
            P(("grp", "sp"), "tp"),
            P("tp"),
            P("tp", "sp"),
        ),
        out_specs=P(("grp", "sp"), None),
        check_vma=False,
    )
```

time: 708 us -> 352 us (0.50)
  waiting for transfers between devices: 459 us -> 68.2 us
  blocking collectives: 0 us -> 187 us
  local copies, waits for them, and re-layouts: 92.2 us -> 12.6 us
  other arithmetic: 57.8 us -> 7.41 us
  matrix products: 26.6 us -> 0.15 us
  Pallas kernels: 0 us -> 19.9 us
  starting transfers between devices: 52.6 us -> 42.9 us
    all_gather x3 -> x1, waiting for transfers between devices: 257 us -> 40 us  [local(): gathered = lax.all_gather(own, 'sp').reshape(members * depth, own.shape[1])]
    psum x1 -> x0, waiting for transfers between devices: 129 us -> none  [local(): lax.psum(partial_out.astype(jnp.bfloat16), 'tp').astype(jnp.float32)]
    all_to_all x0 -> x3, blocking collectives: none -> 97.6 us  [the longest x1 40.6 us: local(): lax.all_to_all(send, 'sp', split_axis=0, concat_axis=0, tiled=True)]
    all_gather x0 -> x1, blocking collectives: none -> 89 us  [local(): summed_terms = lax.all_gather(terms, 'sp').sum(axis=0)]
    all_to_all x2 -> x1, waiting for transfers between devices: 72.3 us -> 1.96 us  [sent_to_all(): return lax.all_to_all(copies, axis, split_axis=0, concat_axis=0, tiled=True)]
    all_to_all x2 -> x1, starting transfers between devices: 52.5 us -> 16.3 us  [sent_to_all(): return lax.all_to_all(copies, axis, split_axis=0, concat_axis=0, tiled=True)]
    all_to_all x0 -> x1, starting transfers between devices: none -> 26.6 us  [local(): parts = lax.all_to_all(parts, 'tp', split_axis=0, concat_axis=0, tiled=True)]
    dot_general x44 -> x1, matrix products: 26.6 us -> 0.15 us  [local(): jnp.einsum('nd,rdc->nrc', silu, mod_weight, preferred_element_type=f32)]
  transfers between devices with their start and end apart: 6 -> 3, of which waited for: 6 -> 3; matrix products, arithmetic and copies ran while one was open for 10% -> 2% of each run, Pallas kernels for 0% -> 0%
where the time goes in v1:
time: 352 us; the launch traced here: 351 us
  blocking collectives  187 us (53%)
  waiting for transfers between devices  68.2 us (19%)
  starting transfers between devices  42.9 us (12%)
  Pallas kernels  19.9 us (6%)
  between operations  13.6 us (4%)
  local copies, waits for them, and re-layouts  12.6 us (4%)
  other arithmetic  7.41 us (2%)
    all_gather x1, blocking collectives, local(): summed_terms = lax.all_gather(terms, 'sp').sum(axis=0)  89 us
    all_to_all x1, blocking collectives, local(): lax.all_to_all(send, 'sp', split_axis=0, concat_axis=0, tiled=True)  40.6 us
    all_gather x1, waiting for transfers between devices, local(): gathered = lax.all_gather(own, 'sp').reshape(members * depth, own.shape[1])  40 us
    all_to_all x1, blocking collectives, sent_to_all(): return lax.all_to_all(copies, axis, split_axis=0, concat_axis=0, tiled=True)  29.7 us
    all_to_all x1, blocking collectives, local(): lax.all_to_all(chain(received), 'sp', split_axis=0, concat_axis=0, tiled=...  27.3 us
    all_to_all x1, starting transfers between devices, local(): parts = lax.all_to_all(parts, 'tp', split_axis=0, concat_axis=0, tiled=True)  26.6 us
    all_to_all x1, waiting for transfers between devices, local(): parts = lax.all_to_all(parts, 'tp', split_axis=0, concat_axis=0, tiled=True)  26.2 us
    all_to_all x1, starting transfers between devices, sent_to_all(): return lax.all_to_all(copies, axis, split_axis=0, concat_axis=0, tiled=True)  16.3 us
  transfers between devices with their start and end apart: 3, of which 3 were waited for; matrix products, arithmetic and copies ran while one was open for 2% of the time, Pallas kernels for 0%

profile of v1, /device:TPU:33, one launch (start us, length us, event | category | flops | bytes accessed | tf_op | source)
XLA Modules:
  0.0 351.3 jit_solution(8035955795996234734)
XLA Ops:
  6.6 0.9 fusion.11
  7.8 0.8 fusion.10
  8.6 1.7 concatenate.18
  10.3 0.7 convert_bitcast_fusion
  11.2 89.0 %all-gather.2 = f32[32,5,512]{2,1,0:T(8,128)S(1)} all-gather(f32[1,5,512]{2,1,0:T(8,128)S(1)} %maximum_bitcast_fusion), channel_id=2, replica_groups=mesh['grp'=2,'sp'=32,'tp'=8] {'sp'}, dimensions={0}, use_global_device_ids=true | all-gather | bytes 337920 | tf_op jit(solution)/shard_map/all_gather | solution.py:309
  100.3 0.7 broadcast_in_dim.45
  100.9 16.3 %all-to-all-start = ((f32[8,5,512]{2,1,0:T(8,128)}), f32[8,5,512]{2,1,0:T(8,128)S(1)}, u32[]{:S(2)}, u32[]{:S(2)}) async-start(f32[8,5,512]{2,1,0:T(8,128)} %broadcast_in_dim.45), calls=%async_computation | async-start | bytes 262144 | tf_op jit(solution)/shard_map/all_to_all | solution.py:19
  117.2 0.7 broadcast_in_dim.50
  118.0 0.7 slice_bitcast_fusion
  118.9 1.6 fusion
  120.5 2.0 all-to-all-done
  122.5 3.7 %fusion.4.h_ref = bf16[272,4096]{1,0:T(8,128)(2,1)S(1)} fusion(f32[4096]{0:T(1024)S(1)} %bitcast.44, f32[4096]{0:T(1024)S(1)} %bitcast.45, f32[4096]{0:T(1024)S(1)} %bitcast.46, f32[4096]{0:T(1024)S(1)} %bitcast.43, f32[4096]{0:T(1024)S(1)} %copy-done.6, f32[272]{0:T(512)S(1)} %add_rsqrt_fusion, pred[272]{0:T(512)(128)(4,1)S(1)} %iota_compare_fusion, ...), kind=kLoop, calls=%fused_computation.6 | loop fusion | flops 15597568 | bytes 4474736 | tf_op jit(solution)/shard_map/convert_element_type | solution.py:320
  126.2 40.0 %all-gather.5.cloned.1.call-done.wqk_ref.wv_ref.wr_ref.w_ref = bf16[4096,896]{1,0:T(8,128)(2,1)} async-done(((bf16[128,896]{1,0:T(8,128)(2,1)}), bf16[4096,896]{1,0:T(8,128)(2,1)}) %all-gather.5.cloned.1.call-update) | async-done | bytes 7340048 | tf_op jit(solution)/shard_map/all_gather | solution.py:304
  166.2 11.0 %mixing.1 = (f32[256,256]{1,0:T(8,128)S(1)}, bf16[256,256]{1,0:T(8,128)(2,1)S(1)}, bf16[32,24,128]{2,1,0:T(8,128)(2,1)S(1)}) custom-call(bf16[272,4096]{1,0:T(8,128)(2,1)S(1)} %fusion.4.h_ref, bf16[4096,896]{1,0:T(8,128)(2,1)} %all-gather.5.cloned.1.call-done.wqk_ref.wv_ref.wr_ref.w_ref, ...), custom_call_target="tpu_custom_call" | custom-call | tf_op jit(solution)/shard_map/mixing/pallas_call | solution.py:177
  177.3 40.6 %all_to_all.25.in_ref = bf16[32,24,128]{2,1,0:T(8,128)(2,1)} all-to-all(bf16[32,24,128]{2,1,0:T(8,128)(2,1)S(1)} %get-tuple-element.34), channel_id=1, replica_groups=mesh['grp'=2,'sp'=32,'tp'=8] {'sp'}, dimensions={0} | all-to-all | bytes 393216 | tf_op jit(solution)/shard_map/all_to_all | solution.py:330
  217.9 1.9 chain.1
  219.8 27.3 %all_to_all.26 = bf16[32,8,128]{2,1,0:T(8,128)(2,1)S(1)} all-to-all(bf16[32,8,128]{2,1,0:T(8,128)(2,1)} %chain.1), channel_id=1, replica_groups=mesh['grp'=2,'sp'=32,'tp'=8] {'sp'}, dimensions={0} | all-to-all | bytes 131072 | tf_op jit(solution)/shard_map/all_to_all | solution.py:331
  247.1 6.9 %output.1 = bf16[8,256,512]{2,1,0:T(8,128)(2,1)} custom-call(f32[256,256]{1,0:T(8,128)S(1)} %get-tuple-element.32.loc_ref, bf16[256,256]{1,0:T(8,128)(2,1)S(1)} %get-tuple-element.33.lift_ref, bf16[256,128]{1,0:T(8,128)(2,1)S(1)} %bitcast.35, f32[1,256]{1,0:T(1,128)S(1)} %bitcast.37, bf16[4096,896]{1,0:T(8,128)(2,1)} %all-gather.5.cloned.1.call-done.wqk_ref.wv_ref.wr_ref.w_ref), custom_call_target="tpu_custom_call" | custom-call | tf_op jit(solution)/shard_map/output/pallas_call | solution.py:262
  254.1 26.6 %all-to-all-start.3 = ((bf16[8,256,512]{2,1,0:T(8,128)(2,1)}), bf16[8,256,512]{2,1,0:T(8,128)(2,1)S(1)}, u32[]{:S(2)}, u32[]{:S(2)}) async-start(bf16[8,256,512]{2,1,0:T(8,128)(2,1)} %output.1), calls=%async_computation.3 | async-start | bytes 4194304 | tf_op jit(solution)/shard_map/all_to_all | solution.py:335
  280.6 26.2 %all-to-all-done.3 = bf16[8,256,512]{2,1,0:T(8,128)(2,1)S(1)} async-done(((bf16[8,256,512]{2,1,0:T(8,128)(2,1)}), bf16[8,256,512]{2,1,0:T(8,128)(2,1)S(1)}, u32[]{:S(2)}, u32[]{:S(2)}) %all-to-all-start.3) | async-done | bytes 2097184 | tf_op jit(solution)/shard_map/all_to_all | solution.py:335
  307.1 1.0 add_convert_fusion
  308.4 29.7 %all_to_all.27 = bf16[8,256,512]{2,1,0:T(8,128)(2,1)S(1)} all-to-all(bf16[8,256,512]{2,1,0:T(8,128)(2,1)S(1)} %broadcast_in_dim.51), channel_id=1, replica_groups=mesh['grp'=2,'sp'=32,'tp'=8] {'tp'}, dimensions={0} | all-to-all | bytes 4194304 | tf_op jit(solution)/shard_map/all_to_all | solution.py:19
  338.0 2.4 copy.31
  340.4 4.1 %copy.32 = bf16[256,4096]{1,0:T(8,128)(2,1)} copy(bf16[256,4096]{0,1:T(8,128)(2,1)} %bitcast.38) | data formatting | bytes 4194304 | tf_op jit(solution)/shard_map/reshape | solution.py:340
  (37 shorter events, 1.4 us)
Async XLA Ops:
  6.5 4.4 %copy-start = (bf16[3,128,512]{2,1,0:T(8,128)(2,1)S(1)}, bf16[3,128,512]{2,1,0:T(8,128)(2,1)}, u32[]{:S(2)}) copy-start(bf16[3,128,512]{2,1,0:T(8,128)(2,1)} %param.23) | copy-start | bytes 1179652
  6.6 113.9 %copy-start.5 = (bf16[2,64,128]{2,1,0:T(8,128)(2,1)S(1)}, bf16[2,64,128]{2,1,0:T(8,128)(2,1)}, u32[]{:S(2)}) copy-start(bf16[2,64,128]{2,1,0:T(8,128)(2,1)} %param.29) | copy-start | bytes 98308
  6.6 112.3 %copy-start.3 = (bf16[256,4096]{1,0:T(8,128)(2,1)S(1)}, bf16[256,4096]{1,0:T(8,128)(2,1)}, u32[]{:S(2)}) copy-start(bf16[256,4096]{1,0:T(8,128)(2,1)} %param.19) | copy-start | bytes 6291460
  6.6 116.0 %copy-start.4 = (bf16[8,4096]{1,0:T(8,128)(2,1)S(1)}, bf16[8,4096]{1,0:T(8,128)(2,1)}, u32[]{:S(2)}) copy-start(bf16[8,4096]{1,0:T(8,128)(2,1)} %param.20) | copy-start | bytes 196612
  6.6 116.0 %copy-start.6 = (f32[4096]{0:T(1024)S(1)}, f32[4096]{0:T(1024)}, u32[]{:S(2)}) copy-start(f32[4096]{0:T(1024)} %param.24) | copy-start | bytes 49156
  6.6 159.7 %all-gather.5.cloned.1.call-start = ((), (), s32[]{:S(2)}) async-start(), calls=%async_computation.5 | async-start | bytes 7569408 | tf_op jit(solution)/shard_map/all_gather | solution.py:304
  100.2 66.0 %copy-start.1 = (f32[2,128]{1,0:T(2,128)S(1)}, f32[2,128]{1,0:T(2,128)}, u32[]{:S(2)}) copy-start(f32[2,128]{1,0:T(2,128)} %param.30) | copy-start | bytes 3076
  100.9 21.5 %all-to-all-start = ((f32[8,5,512]{2,1,0:T(8,128)}), f32[8,5,512]{2,1,0:T(8,128)S(1)}, u32[]{:S(2)}, u32[]{:S(2)}) async-start(f32[8,5,512]{2,1,0:T(8,128)} %broadcast_in_dim.45), calls=%async_computation | async-start | bytes 262144 | tf_op jit(solution)/shard_map/all_to_all | solution.py:19
  166.2 80.9 %copy-start.2 = (f32[256]{0:T(256)S(1)}, f32[256]{0:T(256)}, u32[]{:S(2)}) copy-start(f32[256]{0:T(256)} %param.32) | copy-start | bytes 3076
  254.1 52.8 %all-to-all-start.3 = ((bf16[8,256,512]{2,1,0:T(8,128)(2,1)}), bf16[8,256,512]{2,1,0:T(8,128)(2,1)S(1)}, u32[]{:S(2)}, u32[]{:S(2)}) async-start(bf16[8,256,512]{2,1,0:T(8,128)(2,1)} %output.1), calls=%async_computation.3 | async-start | bytes 4194304 | tf_op jit(solution)/shard_map/all_to_all | solution.py:335
Sparse Core Ops, SparseCore 0:
  10.4 155.7 all-gather.4

commit v2 on v1

--- a/solution.py
+++ b/solution.py
@@ -231,50 +231,137 @@
     )(received)
 
 
-def output_kernel(loc_ref, lift_ref, entry_ref, gain_ref, w_ref, out_ref, normed):
+def normalized_output(loc_ref, lift_ref, entry_ref, gain_ref, normed):
+    entry = entry_ref[...].astype(f32)
+    head = (iota(entry.shape, 0) // DK) % 2
+    spread = jnp.concatenate(
+        [jnp.where(head == 0, entry, 0.0), jnp.where(head == 1, entry, 0.0)], axis=1
+    ).astype(bf16)
+    combined = loc_ref[...] + dot(lift_ref[...], spread)
+    for g in range(2):
+        part = combined[:, g * DV : (g + 1) * DV]
+        scaled = part * lax.rsqrt(jnp.mean(part * part, axis=-1, keepdims=True) + eps)
+        normed[:, g * DV : (g + 1) * DV] = (
+            scaled * gain_ref[:, g * DV : (g + 1) * DV]
+        ).astype(bf16)
+
+
+def column(normed, w, j):
+    rows = slice(j * 128, (j + 1) * 128)
+    return dot(normed[:, 0:128], w[rows, 0:128]) + dot(normed[:, 128:256], w[rows, 128:256])
+
+
+def sent_kernel(order_ref, loc_ref, lift_ref, entry_ref, gain_ref, w_ref, normed, out_ref):
     @pl.when(pl.program_id(0) == 0)
     def _():
-        entry = entry_ref[...].astype(f32)
-        head = (iota(entry.shape, 0) // DK) % 2
-        spread = jnp.concatenate(
-            [jnp.where(head == 0, entry, 0.0), jnp.where(head == 1, entry, 0.0)], axis=1
-        ).astype(bf16)
-        combined = loc_ref[...] + dot(lift_ref[...], spread)
-        for g in range(2):
-            part = combined[:, g * DV : (g + 1) * DV]
-            scaled = part * lax.rsqrt(jnp.mean(part * part, axis=-1, keepdims=True) + eps)
-            normed[:, g * DV : (g + 1) * DV] = (
-                scaled * gain_ref[:, g * DV : (g + 1) * DV]
-            ).astype(bf16)
+        normalized_output(loc_ref, lift_ref, entry_ref, gain_ref, normed)
 
     w = w_ref[...]
     for j in range(w.shape[0] // 128):
-        rows = slice(j * 128, (j + 1) * 128)
-        out_ref[0, :, rows] = (
-            dot(normed[:, 0:128], w[rows, 0:128]) + dot(normed[:, 128:256], w[rows, 128:256])
-        ).astype(bf16)
-
-
-def output(loc, lift, entry, gain, gathered, pieces):
+        out_ref[0, :, j * 128 : (j + 1) * 128] = column(normed, w, j).astype(bf16)
+
+
+def kept_kernel(order_ref, normed, received_ref, w_ref, *out_refs):
+    w = w_ref[...]
+    for k, out_ref in enumerate(out_refs):
+
+        @pl.when(pl.program_id(0) == k)
+        def _():
+            for j in range(w.shape[0] // 128):
+                cols = slice(j * 128, (j + 1) * 128)
+                out_ref[:, cols] = (
+                    column(normed, w, j) + received_ref[0, :, cols].astype(f32)
+                ).astype(bf16)
+
+
+def constant_block(*shape):
+    return pl.BlockSpec(shape, lambda i, order: (0,) * len(shape))
+
+
+def sent_parts(order, loc, lift, entry, gain, gathered, width):
     T = loc.shape[0]
-    width = gathered.shape[0] // pieces
-    whole = lambda *shape: pl.BlockSpec(shape, lambda i: (0,) * len(shape))
+    chips = order.shape[0]
     return pl.pallas_call(
-        output_kernel,
-        grid=(pieces,),
-        in_specs=[
-            whole(T, 256),
-            whole(T, 256),
-            whole(256, 128),
-            whole(1, 256),
-            pl.BlockSpec((width, 256), lambda i: (i, 0)),
+        sent_kernel,
+        grid_spec=pltpu.PrefetchScalarGridSpec(
+            num_scalar_prefetch=1,
+            grid=(chips,),
+            in_specs=[
+                constant_block(T, 256),
+                constant_block(T, 256),
+                constant_block(256, 128),
+                constant_block(1, 256),
+                pl.BlockSpec((width, 256), lambda i, order: (order[i], 0)),
+            ],
+            out_specs=[
+                constant_block(T, 256),
+                pl.BlockSpec((1, T, width), lambda i, order: (i, 0, 0)),
+            ],
+        ),
+        out_shape=[
+            jax.ShapeDtypeStruct((T, 256), bf16),
+            jax.ShapeDtypeStruct((chips, T, width), bf16),
         ],
-        out_specs=pl.BlockSpec((1, T, width), lambda i: (i, 0, 0)),
-        out_shape=jax.ShapeDtypeStruct((pieces, T, width), bf16),
-        scratch_shapes=[pltpu.VMEM((T, 256), bf16)],
         compiler_params=pltpu.CompilerParams(vmem_limit_bytes=VMEM_LIMIT),
-        name="output",
-    )(loc, lift, entry, gain, gathered)
+        name="sent",
+    )(order, loc, lift, entry, gain, gathered)
+
+
+def kept_parts(order, normed, received, gathered, width):
+    T = normed.shape[0]
+    chips = order.shape[0]
+    return pl.pallas_call(
+        kept_kernel,
+        grid_spec=pltpu.PrefetchScalarGridSpec(
+            num_scalar_prefetch=1,
+            grid=(chips,),
+            in_specs=[
+                constant_block(T, 256),
+                pl.BlockSpec((1, T, width), lambda i, order: (i, 0, 0)),
+                pl.BlockSpec((width, 256), lambda i, order: (order[i], 0)),
+            ],
+            out_specs=[constant_block(T, width)] * chips,
+        ),
+        out_shape=[jax.ShapeDtypeStruct((T, width), bf16)] * chips,
+        compiler_params=pltpu.CompilerParams(vmem_limit_bytes=VMEM_LIMIT),
+        name="kept",
+    )(order, normed, received, gathered)
+
+
+def joined_kernel(*refs):
+    out_ref = refs[-1]
+    pieces = refs[:-1]
+    chips = len(pieces) // 2
+    place = lax.axis_index("tp")
+    width = pieces[0].shape[1]
+    for i in range(chips):
+        base = 2 * lax.rem(place // 2 + i, chips)
+        for piece, core in ((pieces[i], place % 2), (pieces[chips + i], 1 - place % 2)):
+            start = pl.multiple_of((base + core) * width, width)
+            out_ref[:, pl.ds(start, width)] = piece[...]
+
+
+def joined(pieces):
+    T, width = pieces[0].shape
+    vmem = pl.BlockSpec(memory_space=pltpu.VMEM)
+    return pl.pallas_call(
+        joined_kernel,
+        out_shape=jax.ShapeDtypeStruct((T, width * len(pieces)), bf16),
+        in_specs=[vmem] * len(pieces),
+        out_specs=vmem,
+        compiler_params=pltpu.CompilerParams(vmem_limit_bytes=VMEM_LIMIT),
+        name="joined",
+    )(*pieces)
+
+
+def to_partner(array):
+    n = lax.axis_size("tp")
+    return lax.ppermute(array, "tp", [(i, i ^ 1) for i in range(n)])
+
+
+def to_chip(array, ahead):
+    n = lax.axis_size("tp")
+    return lax.ppermute(array, "tp", [(i, (i + 2 * ahead) % n) for i in range(n)])
 
 
 def local(
@@ -329,15 +416,23 @@
     )
     received = lax.all_to_all(send, "sp", split_axis=0, concat_axis=0, tiled=True)
     entries = lax.all_to_all(chain(received), "sp", split_axis=0, concat_axis=0, tiled=True)
-    parts = output(
-        loc, lift, entries.reshape(members * 8, 128), out_gain.reshape(1, 256), gathered, pieces
+    columns = width // pieces
+    chips = pieces // 2
+    place = lax.axis_index("tp")
+    order = 2 * ((place // 2 + jnp.arange(chips)) % chips) + place % 2
+    normed, sent = sent_parts(
+        order ^ 1, loc, lift, entries.reshape(members * 8, 128), out_gain.reshape(1, 256),
+        gathered, columns,
     )
-    parts = lax.all_to_all(parts, "tp", split_axis=0, concat_axis=0, tiled=True)
-    summed = parts.astype(f32).sum(axis=0)
-    columns = width // pieces
-    own_latent = lax.dynamic_slice_in_dim(latent, lax.axis_index("tp") * columns, columns, 1)
+    sums = kept_parts(order, normed, to_partner(sent), gathered, columns)
+    own_latent = lax.dynamic_slice_in_dim(latent, place * columns, columns, 1)
+    summed = sums[0].astype(f32)
+    for i in range(1, chips):
+        summed = summed + to_chip(sums[i], i).astype(f32)
     mixed = (own_latent.astype(f32) + summed_terms[2] * summed).astype(bf16)
-    return jnp.moveaxis(sent_to_all(mixed, "tp"), 0, 1).reshape(T, width)
+    mine = [mixed] + [to_chip(mixed, chips - i) for i in range(1, chips)]
+    theirs = [to_partner(piece) for piece in mine]
+    return joined(mine + theirs)
 
 
 def solution(mesh):

time: 352 us -> 335 us (0.952)
  blocking collectives: 187 us -> 134 us
  starting transfers between devices: 42.9 us -> 78.3 us
  local copies, waits for them, and re-layouts: 12.6 us -> 5.94 us
  waiting for transfers between devices: 68.2 us -> 72.4 us
    all_to_all x2 -> x0, blocking collectives: 57 us -> none  [the longest x1 29.7 us: sent_to_all(): return lax.all_to_all(copies, axis, split_axis=0, concat_axis=0, tiled=True)]
    ppermute x0 -> x11, starting transfers between devices: none -> 56.5 us  [the longest x5 35.2 us: to_partner(): return lax.ppermute(array, 'tp', [(i, i ^ 1) for i in range(n)])]
    all_to_all x1, starting transfers between devices: 26.6 us -> 4.77 us  [local(): lax.all_to_all(chain(received), 'sp', split_axis=0, concat_axis=0, tiled=...]
    ppermute x0 -> x11, waiting for transfers between devices: none -> 13.2 us  [the longest x6 9.47 us: to_chip(): lax.ppermute(array, 'tp', [(i, (i + 2 * ahead) % n) for i in range(n)])]
    all_gather x1, waiting for transfers between devices: 40 us -> 34.6 us  [local(): gathered = lax.all_gather(own, 'sp').reshape(members * depth, own.shape[1])]
    all_gather x1, blocking collectives: 89 us -> 93.2 us  [local(): summed_terms = lax.all_gather(terms, 'sp').sum(axis=0)]
    reshape x1 -> x0, local copies, waits for them, and re-layouts: 4.06 us -> none  [local(): return jnp.moveaxis(sent_to_all(mixed, 'tp'), 0, 1).reshape(T, width)]
    all_to_all x1, waiting for transfers between devices: 26.2 us -> 22.5 us  [local(): lax.all_to_all(chain(received), 'sp', split_axis=0, concat_axis=0, tiled=...]
  transfers between devices with their start and end apart: 3 -> 14, of which waited for: 3 -> 9; matrix products, arithmetic and copies ran while one was open for 2% -> 3% of each run, Pallas kernels for 0% -> 0%
where the time goes in v2:
time: 335 us; the launch traced here: 334 us
  blocking collectives  134 us (40%)
  starting transfers between devices  78.3 us (23%)
  waiting for transfers between devices  72.4 us (22%)
  Pallas kernels  21.6 us (6%)
  between operations  13.8 us (4%)
  other arithmetic  8.29 us (2%)
  local copies, waits for them, and re-layouts  5.94 us (2%)
    all_gather x1, blocking collectives, local(): summed_terms = lax.all_gather(terms, 'sp').sum(axis=0)  93.2 us
    all_to_all x1, blocking collectives, local(): lax.all_to_all(send, 'sp', split_axis=0, concat_axis=0, tiled=True)  40.6 us
    ppermute x5, starting transfers between devices, to_partner(): return lax.ppermute(array, 'tp', [(i, i ^ 1) for i in range(n)])  35.2 us
    all_gather x1, waiting for transfers between devices, local(): gathered = lax.all_gather(own, 'sp').reshape(members * depth, own.shape[1])  34.6 us
    all_to_all x1, waiting for transfers between devices, local(): lax.all_to_all(chain(received), 'sp', split_axis=0, concat_axis=0, tiled=...  22.5 us
    ppermute x6, starting transfers between devices, to_chip(): lax.ppermute(array, 'tp', [(i, (i + 2 * ahead) % n) for i in range(n)])  21.3 us
    all_to_all x1, starting transfers between devices, sent_to_all(): return lax.all_to_all(copies, axis, split_axis=0, concat_axis=0, tiled=True)  17 us
    pallas_call x1, Pallas kernels, mixing(): pl.pallas_call(mixing_kernel, grid=(steps,), in_specs=[pl.BlockSpec((rows...  11 us
  transfers between devices with their start and end apart: 14, of which 9 were waited for; matrix products, arithmetic and copies ran while one was open for 3% of the time, Pallas kernels for 0%

profile of v2, /device:TPU:33, one launch (start us, length us, event | category | flops | bytes accessed | tf_op | source)
XLA Modules:
  0.0 334.1 jit_solution(7137131388373003119)
XLA Ops:
  11.2 93.2 %all-gather.2 = f32[32,5,512]{2,1,0:T(8,128)} all-gather(f32[1,5,512]{2,1,0:T(8,128)S(1)} %maximum_bitcast_fusion), channel_id=2, replica_groups=mesh['grp'=2,'sp'=32,'tp'=8] {'sp'}, dimensions={0}, use_global_device_ids=true | all-gather | bytes 337920 | tf_op jit(solution)/shard_map/all_gather | solution.py:396
  106.1 17.0 %all-to-all-start = ((f32[8,5,512]{2,1,0:T(8,128)}), f32[8,5,512]{2,1,0:T(8,128)S(1)}, u32[]{:S(2)}, u32[]{:S(2)}) async-start(f32[8,5,512]{2,1,0:T(8,128)} %broadcast_in_dim.42), calls=%async_computation | async-start | bytes 262144 | tf_op jit(solution)/shard_map/all_to_all | solution.py:19
  126.4 2.0 all-to-all-done
  128.5 3.7 %fusion.4.h_ref = bf16[272,4096]{1,0:T(8,128)(2,1)S(1)} fusion(f32[4096]{0:T(1024)S(1)} %bitcast.40, f32[4096]{0:T(1024)S(1)} %bitcast.41, f32[4096]{0:T(1024)S(1)} %bitcast.42, f32[4096]{0:T(1024)S(1)} %bitcast.39, f32[4096]{0:T(1024)S(1)} %copy-done.6, f32[272]{0:T(512)S(1)} %add_rsqrt_fusion, pred[272]{0:T(512)(128)(4,1)S(1)} %iota_compare_fusion, ...), kind=kLoop, calls=%fused_computation.6 | loop fusion | flops 15597568 | bytes 4474736 | tf_op jit(solution)/shard_map/convert_element_type | solution.py:407
  132.2 34.6 %all-gather.5.cloned.1.call-done.wqk_ref.wv_ref.wr_ref.w_ref = bf16[4096,896]{1,0:T(8,128)(2,1)} async-done(((bf16[128,896]{1,0:T(8,128)(2,1)}), bf16[4096,896]{1,0:T(8,128)(2,1)}) %all-gather.5.cloned.1.call-update) | async-done | bytes 7340048 | tf_op jit(solution)/shard_map/all_gather | solution.py:391
  166.7 11.0 %mixing.1 = (f32[256,256]{1,0:T(8,128)S(1)}, bf16[256,256]{1,0:T(8,128)(2,1)S(1)}, bf16[32,24,128]{2,1,0:T(8,128)(2,1)S(1)}) custom-call(bf16[272,4096]{1,0:T(8,128)(2,1)S(1)} %fusion.4.h_ref, bf16[4096,896]{1,0:T(8,128)(2,1)} %all-gather.5.cloned.1.call-done.wqk_ref.wv_ref.wr_ref.w_ref, ...), custom_call_target="tpu_custom_call" | custom-call | tf_op jit(solution)/shard_map/mixing/pallas_call | solution.py:177
  177.8 40.6 %all_to_all.15.in_ref = bf16[32,24,128]{2,1,0:T(8,128)(2,1)} all-to-all(bf16[32,24,128]{2,1,0:T(8,128)(2,1)S(1)} %get-tuple-element.40), channel_id=1, replica_groups=mesh['grp'=2,'sp'=32,'tp'=8] {'sp'}, dimensions={0} | all-to-all | bytes 393216 | tf_op jit(solution)/shard_map/all_to_all | solution.py:417
  220.2 4.8 %all-to-all-start.2 = ((bf16[32,8,128]{2,1,0:T(8,128)(2,1)}), bf16[32,8,128]{2,1,0:T(8,128)(2,1)S(1)}, u32[]{:S(2)}, u32[]{:S(2)}) async-start(bf16[32,8,128]{2,1,0:T(8,128)(2,1)} %chain.1), calls=%async_computation.2 | async-start | bytes 131072 | tf_op jit(solution)/shard_map/all_to_all | solution.py:418
  225.1 22.5 %all-to-all-done.2 = bf16[32,8,128]{2,1,0:T(8,128)(2,1)S(1)} async-done(((bf16[32,8,128]{2,1,0:T(8,128)(2,1)}), bf16[32,8,128]{2,1,0:T(8,128)(2,1)S(1)}, u32[]{:S(2)}, u32[]{:S(2)}) %all-to-all-start.2) | async-done | bytes 65568 | tf_op jit(solution)/shard_map/all_to_all | solution.py:418
  247.6 3.7 %sent.1 = (bf16[256,256]{1,0:T(8,128)(2,1)S(1)}, bf16[4,256,512]{2,1,0:T(8,128)(2,1)S(1)}) custom-call(s32[4]{0:T(128)S(1)} %get-tuple-element.47.order_ref, f32[256,256]{1,0:T(8,128)S(1)} %get-tuple-element.38.loc_ref, bf16[256,256]{1,0:T(8,128)(2,1)S(1)} %get-tuple-element.39.lift_ref, bf16[256,128]{1,0:T(8,128)(2,1)S(1)} %bitcast.32, ...), custom_call_target="tpu_custom_call" | custom-call | tf_op jit(solution)/shard_map/sent/pallas_call | solution.py:284
  251.3 24.4 %collective-permute-start = (bf16[4,256,512]{2,1,0:T(8,128)(2,1)S(1)}, bf16[4,256,512]{2,1,0:T(8,128)(2,1)S(1)}, u32[]{:S(2)}, u32[]{:S(2)}) collective-permute-start(bf16[4,256,512]{2,1,0:T(8,128)(2,1)S(1)} %get-tuple-element.42), channel_id=1, source_target_pairs={{0,1},{1,0},{2,3},{3,2},{4,5},{5,4},{6,7},{7,6},{8,9},{9,8},{10,11... | collective-permute-start | bytes 3145736 | tf_op jit(solution)/shard_map/ppermute | solution.py:359
  275.7 2.3 collective-permute-done.received_ref
  278.0 3.5 %kept.1 = (bf16[256,512]{1,0:T(8,128)(2,1)S(1)}, bf16[256,512]{1,0:T(8,128)(2,1)S(1)}, bf16[256,512]{1,0:T(8,128)(2,1)S(1)}, bf16[256,512]{1,0:T(8,128)(2,1)S(1)}) custom-call(s32[4]{0:T(128)S(1)} %get-tuple-element.48.order_ref, bf16[256,256]{1,0:T(8,128)(2,1)S(1)} %get-tuple-element.41.normed, bf16[4,256,512]{2,1,0:T(8,128)(2,1)S(1)} %collective-permute-done.received_ref, ...), custom_call_target="tpu_custom_call" | custom-call | tf_op jit(solution)/shard_map/kept/pallas_call | solution.py:313
  281.4 2.7 collective-permute-start.1
  284.1 3.6 %collective-permute-start.2 = (bf16[256,512]{1,0:T(8,128)(2,1)S(1)}, bf16[256,512]{1,0:T(8,128)(2,1)S(1)}, u32[]{:S(2)}, u32[]{:S(2)}) collective-permute-start(bf16[256,512]{1,0:T(8,128)(2,1)S(1)} %get-tuple-element.45), channel_id=1, source_target_pairs={{0,4},{1,5},{2,6},{3,7},{4,0},{5,1},{6,2},{7,3},{8,12},{9,13},{10,... | collective-permute-start | bytes 786440 | tf_op jit(solution)/shard_map/ppermute | solution.py:364
  287.7 4.0 %collective-permute-start.3 = (bf16[256,512]{1,0:T(8,128)(2,1)S(1)}, bf16[256,512]{1,0:T(8,128)(2,1)S(1)}, u32[]{:S(2)}, u32[]{:S(2)}) collective-permute-start(bf16[256,512]{1,0:T(8,128)(2,1)S(1)} %get-tuple-element.46), channel_id=1, source_target_pairs={{0,6},{1,7},{2,0},{3,1},{4,2},{5,3},{6,4},{7,5},{8,14},{9,15},{10,... | collective-permute-start | bytes 786440 | tf_op jit(solution)/shard_map/ppermute | solution.py:364
  292.1 5.5 %collective-permute-done.2 = bf16[256,512]{1,0:T(8,128)(2,1)S(1)} collective-permute-done((bf16[256,512]{1,0:T(8,128)(2,1)S(1)}, bf16[256,512]{1,0:T(8,128)(2,1)S(1)}, u32[]{:S(2)}, u32[]{:S(2)}) %collective-permute-start.2) | collective-permute-done | bytes 262176 | tf_op jit(solution)/shard_map/ppermute | solution.py:364
  297.6 2.3 collective-permute-done.3
  301.1 4.7 %collective-permute-start.6 = (bf16[256,512]{1,0:T(8,128)(2,1)S(1)}, bf16[256,512]{1,0:T(8,128)(2,1)S(1)}, u32[]{:S(2)}, u32[]{:S(2)}) collective-permute-start(bf16[256,512]{1,0:T(8,128)(2,1)S(1)} %add_convert_fusion.refs_0_), channel_id=1, source_target_pairs={{0,2},{1,3},{2,4},{3,5},{4,6},{5,7},{6,0},{7,1},{8,10},{9,11},{10,... | collective-permute-start | bytes 786440 | tf_op jit(solution)/shard_map/ppermute | solution.py:364
  305.8 3.7 %collective-permute-start.5 = (bf16[256,512]{1,0:T(8,128)(2,1)S(1)}, bf16[256,512]{1,0:T(8,128)(2,1)S(1)}, u32[]{:S(2)}, u32[]{:S(2)}) collective-permute-start(bf16[256,512]{1,0:T(8,128)(2,1)S(1)} %add_convert_fusion.refs_0_), channel_id=1, source_target_pairs={{0,4},{1,5},{2,6},{3,7},{4,0},{5,1},{6,2},{7,3},{8,12},{9,13},{10,... | collective-permute-start | bytes 786440 | tf_op jit(solution)/shard_map/ppermute | solution.py:364
  309.5 2.6 collective-permute-start.4
  312.1 3.6 %collective-permute-start.7 = (bf16[256,512]{1,0:T(8,128)(2,1)S(1)}, bf16[256,512]{1,0:T(8,128)(2,1)S(1)}, u32[]{:S(2)}, u32[]{:S(2)}) collective-permute-start(bf16[256,512]{1,0:T(8,128)(2,1)S(1)} %add_convert_fusion.refs_0_), channel_id=1, source_target_pairs={{0,1},{1,0},{2,3},{3,2},{4,5},{5,4},{6,7},{7,6},{8,9},{9,8},{10,11... | collective-permute-start | bytes 786440 | tf_op jit(solution)/shard_map/ppermute | solution.py:359
  319.0 3.3 %collective-permute-start.9 = (bf16[256,512]{1,0:T(8,128)(2,1)S(1)}, bf16[256,512]{1,0:T(8,128)(2,1)S(1)}, u32[]{:S(2)}, u32[]{:S(2)}) collective-permute-start(bf16[256,512]{1,0:T(8,128)(2,1)S(1)} %collective-permute-done.5.refs_2_), channel_id=1, source_target_pairs={{0,1},{1,0},{2,3},{3,2},{4,5},{5,4},{6,7},{7,6},{8,9},{9,8},{10,11... | collective-permute-start | bytes 786440 | tf_op jit(solution)/shard_map/ppermute | solution.py:359
  322.3 2.0 collective-permute-start.8
  (56 shorter events, 19.3 us)
Async XLA Ops:
  6.5 4.4 %copy-start = (bf16[3,128,512]{2,1,0:T(8,128)(2,1)S(1)}, bf16[3,128,512]{2,1,0:T(8,128)(2,1)}, u32[]{:S(2)}) copy-start(bf16[3,128,512]{2,1,0:T(8,128)(2,1)} %param.23) | copy-start | bytes 1179652
  6.6 119.8 %copy-start.5 = (bf16[2,64,128]{2,1,0:T(8,128)(2,1)S(1)}, bf16[2,64,128]{2,1,0:T(8,128)(2,1)}, u32[]{:S(2)}) copy-start(bf16[2,64,128]{2,1,0:T(8,128)(2,1)} %param.29) | copy-start | bytes 98308
  6.6 118.2 %copy-start.3 = (bf16[256,4096]{1,0:T(8,128)(2,1)S(1)}, bf16[256,4096]{1,0:T(8,128)(2,1)}, u32[]{:S(2)}) copy-start(bf16[256,4096]{1,0:T(8,128)(2,1)} %param.19) | copy-start | bytes 6291460
  6.6 121.9 %copy-start.4 = (bf16[8,4096]{1,0:T(8,128)(2,1)S(1)}, bf16[8,4096]{1,0:T(8,128)(2,1)}, u32[]{:S(2)}) copy-start(bf16[8,4096]{1,0:T(8,128)(2,1)} %param.20) | copy-start | bytes 196612
  6.6 121.9 %copy-start.6 = (f32[4096]{0:T(1024)S(1)}, f32[4096]{0:T(1024)}, u32[]{:S(2)}) copy-start(f32[4096]{0:T(1024)} %param.24) | copy-start | bytes 49156
  6.6 160.2 %all-gather.5.cloned.1.call-start = ((), (), s32[]{:S(2)}) async-start(), calls=%async_computation.3 | async-start | bytes 7569408 | tf_op jit(solution)/shard_map/all_gather | solution.py:391
  104.3 62.4 %copy-start.1 = (f32[2,128]{1,0:T(2,128)S(1)}, f32[2,128]{1,0:T(2,128)}, u32[]{:S(2)}) copy-start(f32[2,128]{1,0:T(2,128)} %param.30) | copy-start | bytes 3076
  106.1 22.2 %all-to-all-start = ((f32[8,5,512]{2,1,0:T(8,128)}), f32[8,5,512]{2,1,0:T(8,128)S(1)}, u32[]{:S(2)}, u32[]{:S(2)}) async-start(f32[8,5,512]{2,1,0:T(8,128)} %broadcast_in_dim.42), calls=%async_computation | async-start | bytes 262144 | tf_op jit(solution)/shard_map/all_to_all | solution.py:19
  166.7 80.8 %copy-start.2 = (f32[256]{0:T(256)S(1)}, f32[256]{0:T(256)}, u32[]{:S(2)}) copy-start(f32[256]{0:T(256)} %param.32) | copy-start | bytes 3076
  220.2 27.3 %all-to-all-start.2 = ((bf16[32,8,128]{2,1,0:T(8,128)(2,1)}), bf16[32,8,128]{2,1,0:T(8,128)(2,1)S(1)}, u32[]{:S(2)}, u32[]{:S(2)}) async-start(bf16[32,8,128]{2,1,0:T(8,128)(2,1)} %chain.1), calls=%async_computation.2 | async-start | bytes 131072 | tf_op jit(solution)/shard_map/all_to_all | solution.py:418
  251.3 26.7 %collective-permute-start = (bf16[4,256,512]{2,1,0:T(8,128)(2,1)S(1)}, bf16[4,256,512]{2,1,0:T(8,128)(2,1)S(1)}, u32[]{:S(2)}, u32[]{:S(2)}) collective-permute-start(bf16[4,256,512]{2,1,0:T(8,128)(2,1)S(1)} %get-tuple-element.42), channel_id=1, source_target_pairs={{0,1},{1,0},{2,3},{3,2},{4,5},{5,4},{6,7},{7,6},{8,9},{9,8},{10,11... | collective-permute-start | bytes 3145736 | tf_op jit(solution)/shard_map/ppermute | solution.py:359
  281.4 10.7 %collective-permute-start.1 = (bf16[256,512]{1,0:T(8,128)(2,1)S(1)}, bf16[256,512]{1,0:T(8,128)(2,1)S(1)}, u32[]{:S(2)}, u32[]{:S(2)}) collective-permute-start(bf16[256,512]{1,0:T(8,128)(2,1)S(1)} %get-tuple-element.44), channel_id=1, source_target_pairs={{0,2},{1,3},{2,4},{3,5},{4,6},{5,7},{6,0},{7,1},{8,10},{9,11},{10,... | collective-permute-start | bytes 786440 | tf_op jit(solution)/shard_map/ppermute | solution.py:364
  284.1 13.5 %collective-permute-start.2 = (bf16[256,512]{1,0:T(8,128)(2,1)S(1)}, bf16[256,512]{1,0:T(8,128)(2,1)S(1)}, u32[]{:S(2)}, u32[]{:S(2)}) collective-permute-start(bf16[256,512]{1,0:T(8,128)(2,1)S(1)} %get-tuple-element.45), channel_id=1, source_target_pairs={{0,4},{1,5},{2,6},{3,7},{4,0},{5,1},{6,2},{7,3},{8,12},{9,13},{10,... | collective-permute-start | bytes 786440 | tf_op jit(solution)/shard_map/ppermute | solution.py:364
  287.7 12.2 %collective-permute-start.3 = (bf16[256,512]{1,0:T(8,128)(2,1)S(1)}, bf16[256,512]{1,0:T(8,128)(2,1)S(1)}, u32[]{:S(2)}, u32[]{:S(2)}) collective-permute-start(bf16[256,512]{1,0:T(8,128)(2,1)S(1)} %get-tuple-element.46), channel_id=1, source_target_pairs={{0,6},{1,7},{2,0},{3,1},{4,2},{5,3},{6,4},{7,5},{8,14},{9,15},{10,... | collective-permute-start | bytes 786440 | tf_op jit(solution)/shard_map/ppermute | solution.py:364
  301.1 14.6 %collective-permute-start.6 = (bf16[256,512]{1,0:T(8,128)(2,1)S(1)}, bf16[256,512]{1,0:T(8,128)(2,1)S(1)}, u32[]{:S(2)}, u32[]{:S(2)}) collective-permute-start(bf16[256,512]{1,0:T(8,128)(2,1)S(1)} %add_convert_fusion.refs_0_), channel_id=1, source_target_pairs={{0,2},{1,3},{2,4},{3,5},{4,6},{5,7},{6,0},{7,1},{8,10},{9,11},{10,... | collective-permute-start | bytes 786440 | tf_op jit(solution)/shard_map/ppermute | solution.py:364
  305.8 13.2 %collective-permute-start.5 = (bf16[256,512]{1,0:T(8,128)(2,1)S(1)}, bf16[256,512]{1,0:T(8,128)(2,1)S(1)}, u32[]{:S(2)}, u32[]{:S(2)}) collective-permute-start(bf16[256,512]{1,0:T(8,128)(2,1)S(1)} %add_convert_fusion.refs_0_), channel_id=1, source_target_pairs={{0,4},{1,5},{2,6},{3,7},{4,0},{5,1},{6,2},{7,3},{8,12},{9,13},{10,... | collective-permute-start | bytes 786440 | tf_op jit(solution)/shard_map/ppermute | solution.py:364
  309.5 12.8 %collective-permute-start.4 = (bf16[256,512]{1,0:T(8,128)(2,1)S(1)}, bf16[256,512]{1,0:T(8,128)(2,1)S(1)}, u32[]{:S(2)}, u32[]{:S(2)}) collective-permute-start(bf16[256,512]{1,0:T(8,128)(2,1)S(1)} %add_convert_fusion.refs_0_), channel_id=1, source_target_pairs={{0,6},{1,7},{2,0},{3,1},{4,2},{5,3},{6,4},{7,5},{8,14},{9,15},{10,... | collective-permute-start | bytes 786440 | tf_op jit(solution)/shard_map/ppermute | solution.py:364
  312.1 12.2 %collective-permute-start.7 = (bf16[256,512]{1,0:T(8,128)(2,1)S(1)}, bf16[256,512]{1,0:T(8,128)(2,1)S(1)}, u32[]{:S(2)}, u32[]{:S(2)}) collective-permute-start(bf16[256,512]{1,0:T(8,128)(2,1)S(1)} %add_convert_fusion.refs_0_), channel_id=1, source_target_pairs={{0,1},{1,0},{2,3},{3,2},{4,5},{5,4},{6,7},{7,6},{8,9},{9,8},{10,11... | collective-permute-start | bytes 786440 | tf_op jit(solution)/shard_map/ppermute | solution.py:359
  315.7 8.6 %collective-permute-start.10 = (bf16[256,512]{1,0:T(8,128)(2,1)S(1)}, bf16[256,512]{1,0:T(8,128)(2,1)S(1)}, u32[]{:S(2)}, u32[]{:S(2)}) collective-permute-start(bf16[256,512]{1,0:T(8,128)(2,1)S(1)} %collective-permute-done.6.refs_3_), channel_id=1, source_target_pairs={{0,1},{1,0},{2,3},{3,2},{4,5},{5,4},{6,7},{7,6},{8,9},{9,8},{10,11... | collective-permute-start | bytes 786440 | tf_op jit(solution)/shard_map/ppermute | solution.py:359
  319.0 5.3 %collective-permute-start.9 = (bf16[256,512]{1,0:T(8,128)(2,1)S(1)}, bf16[256,512]{1,0:T(8,128)(2,1)S(1)}, u32[]{:S(2)}, u32[]{:S(2)}) collective-permute-start(bf16[256,512]{1,0:T(8,128)(2,1)S(1)} %collective-permute-done.5.refs_2_), channel_id=1, source_target_pairs={{0,1},{1,0},{2,3},{3,2},{4,5},{5,4},{6,7},{7,6},{8,9},{9,8},{10,11... | collective-permute-start | bytes 786440 | tf_op jit(solution)/shard_map/ppermute | solution.py:359
  322.3 3.5 %collective-permute-start.8 = (bf16[256,512]{1,0:T(8,128)(2,1)S(1)}, bf16[256,512]{1,0:T(8,128)(2,1)S(1)}, u32[]{:S(2)}, u32[]{:S(2)}) collective-permute-start(bf16[256,512]{1,0:T(8,128)(2,1)S(1)} %collective-permute-done.4.refs_1_), channel_id=1, source_target_pairs={{0,1},{1,0},{2,3},{3,2},{4,5},{5,4},{6,7},{7,6},{8,9},{9,8},{10,11... | collective-permute-start | bytes 786440 | tf_op jit(solution)/shard_map/ppermute | solution.py:359
Sparse Core Ops, SparseCore 0:
  10.4 156.3 all-gather.4

commit v3 on v2

--- a/solution.py
+++ b/solution.py
@@ -11,6 +11,9 @@
 normalizer = 16.0
 f32 = jnp.float32
 bf16 = jnp.bfloat16
+f16 = jnp.float16
+WEIGHT_SCALE = 2.0**17
+TERM_SCALE = 2.0**9
 VMEM_LIMIT = 50 * 1024 * 1024
 
 
@@ -51,33 +54,141 @@
     return jnp.where(rows < DK, both[:, :DV], both[:, DV:])
 
 
+def prepare_kernel(
+    cond_l_ref, cond_c_ref, mod_ref, q_ref, k_ref, v_ref, rank_ref, out_w_ref, out_ref
+):
+    depth = q_ref.shape[0]
+
+    def put(block, array):
+        out_ref[block] = array.astype(f32) * WEIGHT_SCALE
+
+    put(0, out_w_ref[0:depth])
+    put(1, out_w_ref[depth : 2 * depth])
+    put(2, q_ref[...])
+    put(3, k_ref[...])
+    put(4, v_ref[:, 0:128])
+    put(5, v_ref[:, 128:256])
+    put(6, rank_ref[...].astype(f32).T)
+
+    def silu(c):
+        return c / (1.0 + jnp.exp(-c))
+
+    row = iota((16, depth), 0)
+    conds = jnp.where(
+        row == 0, silu(cond_l_ref[...]), jnp.where(row == 1, silu(cond_c_ref[...]), 0.0)
+    ).astype(bf16)
+    out_ref[7] = jnp.zeros((depth, 128), f32)
+    terms = [dot(conds, mod_ref[r]) * TERM_SCALE for r in range(3)]
+    vectors = [(terms[0], 0), (terms[1], 0), (terms[2], 0), (terms[0], 1), (terms[1], 1)]
+    columns = mod_ref.shape[2] // 128
+    lines = len(vectors) * columns
+    for n, (term, at) in enumerate(vectors):
+        for c in range(columns):
+            line = term[at : at + 1, c * 128 : (c + 1) * 128]
+            high = line.astype(bf16).astype(f32)
+            spot = n * columns + c
+            out_ref[7, spot : spot + 1, :] = high
+            out_ref[7, lines + spot : lines + spot + 1, :] = line - high
+
+
+def prepare(cond_latent, cond_context, mod_weight, w_query, w_key, w_value, w_rank, w_out):
+    depth = w_query.shape[0]
+    vmem = pl.BlockSpec(memory_space=pltpu.VMEM)
+    ranks = jnp.swapaxes(w_rank, 1, 2).reshape(128, depth)
+    return pl.pallas_call(
+        prepare_kernel,
+        out_shape=jax.ShapeDtypeStruct((8, depth, 128), f32),
+        in_specs=[vmem] * 8,
+        out_specs=vmem,
+        name="prepare",
+    )(
+        cond_latent.reshape(1, depth), cond_context.reshape(1, depth),
+        mod_weight, w_query, w_key, w_value, ranks, w_out,
+    )
+
+
+def stats_kernel(latent_ref, context_ref, out_ref):
+    T = latent_ref.shape[0]
+    C = context_ref.shape[0]
+    for ref, at, size in ((latent_ref, 0, T), (context_ref, T, C)):
+        x = ref[...].astype(f32)
+        scale = lax.rsqrt(jnp.mean(x * x, axis=-1, keepdims=True) + eps)
+        out_ref[at : at + size, :] = jnp.broadcast_to(scale, (size, 128))
+
+
+def stats(latent, context):
+    T, C = latent.shape[0], context.shape[0]
+    vmem = pl.BlockSpec(memory_space=pltpu.VMEM)
+    return pl.pallas_call(
+        stats_kernel,
+        out_shape=jax.ShapeDtypeStruct((T + C, 128), f32),
+        in_specs=[vmem] * 2,
+        out_specs=vmem,
+        compiler_params=pltpu.CompilerParams(vmem_limit_bytes=VMEM_LIMIT),
+        name="stats",
+    )(latent, context)
+
+
 def mixing_kernel(
-    h_ref, wqk_ref, wv_ref, wr_ref, wd_ref, bias_ref, shift_ref,
+    latent_ref, context_ref, stats_ref, rows_ref, gain_ref,
+    wq_ref, wk_ref, wv0_ref, wv1_ref, wr_ref, wd_ref, bias_ref, shift_ref,
     loc_ref, lift_ref, send_ref, acc,
 ):
     step = pl.program_id(0)
-    T = shift_ref.shape[0]
-    C = h_ref.shape[0] - T
-    h = h_ref[...]
+    T = latent_ref.shape[0]
+    C = context_ref.shape[0]
+    columns = rows_ref.shape[1] // 5
 
     @pl.when(step == 0)
     def _():
         acc[...] = jnp.zeros_like(acc)
 
-    acc[:, 0:256] += dot(h, wqk_ref[...])
-    acc[:, 256:512] += dot(h, wv_ref[...])
-    acc[:, 512:640] += dot(h, wr_ref[...])
+    def modulated(ref, at, size, shift_row, scale_row):
+        parts = []
+        for c in range(columns):
+            cols = slice(c * 128, (c + 1) * 128)
+            spot = scale_row * columns + c
+            scale = gain_ref[0, :, cols] * (1.0 + rows_ref[0, spot : spot + 1, :])
+            spot = shift_row * columns + c
+            shift = rows_ref[0, spot : spot + 1, :]
+            x = ref[:, cols].astype(f32) * stats_ref[at : at + size, :]
+            parts.append((x * scale + shift).astype(bf16))
+        return jnp.concatenate(parts, axis=1)
+
+    w_qk = jnp.concatenate([wq_ref[0], wk_ref[0]], axis=1)
+    w_v = jnp.concatenate([wv0_ref[0], wv1_ref[0]], axis=1)
+    h = modulated(latent_ref, 0, T, 0, 1)
+    hc = modulated(context_ref, T, C, 3, 4)
+    h = jnp.concatenate([h, hc, jnp.zeros((acc.shape[0] - T - C, h.shape[1]), bf16)], axis=0)
+    acc[:, 0:256] += dot(h, w_qk)
+    acc[:, 256:512] += dot(h, w_v)
+    acc[:, 512:640] += dot(h, wr_ref[0])
 
     @pl.when(step == pl.num_programs(0) - 1)
     def _():
+        C = acc.shape[0] - T
         q16 = acc[0:T, 0:128].astype(bf16)
         k16 = acc[0:T, 128:256].astype(bf16)
         v = acc[0:T, 256:512].astype(bf16)
         q = q16.astype(f32)
         k = k16.astype(f32)
         ranks = acc[:, 512:640].astype(bf16)
-        logs = log_sigmoid(dot(ranks, wd_ref[...]) + bias_ref[...]) / normalizer
-        lat = logs[0:T] + shift_ref[...]
+        rank_lane = iota(ranks.shape, 1)
+        none = jnp.zeros_like(ranks)
+        pre = jnp.concatenate(
+            [
+                dot(jnp.where(rank_lane < 64, ranks, none), wd_ref[...]) + bias_ref[0:1, :],
+                dot(jnp.where(rank_lane < 64, none, ranks), wd_ref[...]) + bias_ref[1:2, :],
+            ],
+            axis=1,
+        )
+        logs = log_sigmoid(pre) / normalizer
+
+        def down(h):
+            return jnp.broadcast_to(shift_ref[h : h + 1, :], (128, T)).T
+
+        shifts = jnp.where(iota((T, 128), 1) < DK, down(0), down(1))
+        lat = logs[0:T] + jnp.concatenate([shifts, shifts], axis=1)
         f_high, f_low = halves(lat[:, 0:128])
         b_high, b_low = halves(lat[:, 128:256])
         f_pair = jnp.concatenate([f_high, f_low], axis=1)
@@ -168,23 +279,27 @@
         send_ref[half:n, 16:24, :] = packed(total(b_high, b_low), total(cb_high, cb_low))
 
 
-def mixing(h, gathered, decay_weight, decay_bias, shifts, members):
-    T = shifts.shape[0]
-    rows, width = h.shape
-    steps = 8
+def mixing(
+    latent, context, scales, rows, gain, gathered, w_decay, decay_bias, decay_shift, members
+):
+    T, width = latent.shape
+    C = context.shape[0]
+    steps = rows.shape[0]
     depth = width // steps
     whole = lambda *shape: pl.BlockSpec(shape, lambda i: (0,) * len(shape))
     return pl.pallas_call(
         mixing_kernel,
         grid=(steps,),
         in_specs=[
-            pl.BlockSpec((rows, depth), lambda i: (0, i)),
-            pl.BlockSpec((depth, 256), lambda i: (i, 1)),
-            pl.BlockSpec((depth, 256), lambda i: (i, 2)),
-            pl.BlockSpec((depth, 128), lambda i: (i, 6)),
-            whole(128, 256),
-            whole(1, 256),
-            whole(T, 256),
+            pl.BlockSpec((T, depth), lambda i: (0, i)),
+            pl.BlockSpec((C, depth), lambda i: (0, i)),
+            whole(T + C, 128),
+            pl.BlockSpec((1, *rows.shape[1:]), lambda i: (i, 0, 0)),
+            pl.BlockSpec((1, 1, depth), lambda i: (i, 0, 0)),
+            *[pl.BlockSpec((1, depth, 128), lambda i, b=b: (b, i, 0)) for b in range(2, 7)],
+            whole(128, 128),
+            whole(2, 128),
+            whole(2, T),
         ],
         out_specs=[whole(T, 256), whole(T, 256), whole(members, 24, 128)],
         out_shape=[
@@ -192,10 +307,13 @@
             jax.ShapeDtypeStruct((T, 256), bf16),
             jax.ShapeDtypeStruct((members, 24, 128), bf16),
         ],
-        scratch_shapes=[pltpu.VMEM((rows, 640), f32)],
+        scratch_shapes=[pltpu.VMEM((T + 16, 640), f32)],
         compiler_params=pltpu.CompilerParams(vmem_limit_bytes=VMEM_LIMIT),
         name="mixing",
-    )(h, gathered, gathered, gathered, decay_weight, decay_bias, shifts)
+    )(
+        latent, context, scales, rows, gain.reshape(steps, 1, depth), *[gathered] * 5,
+        w_decay.reshape(128, 128), decay_bias, decay_shift.T,
+    )
 
 
 def chain_kernel(in_ref, out_ref):
@@ -248,7 +366,7 @@
 
 def column(normed, w, j):
     rows = slice(j * 128, (j + 1) * 128)
-    return dot(normed[:, 0:128], w[rows, 0:128]) + dot(normed[:, 128:256], w[rows, 128:256])
+    return dot(normed[:, 0:128], w[0, rows]) + dot(normed[:, 128:256], w[1, rows])
 
 
 def sent_kernel(order_ref, loc_ref, lift_ref, entry_ref, gain_ref, w_ref, normed, out_ref):
@@ -257,7 +375,7 @@
         normalized_output(loc_ref, lift_ref, entry_ref, gain_ref, normed)
 
     w = w_ref[...]
-    for j in range(w.shape[0] // 128):
+    for j in range(w.shape[1] // 128):
         out_ref[0, :, j * 128 : (j + 1) * 128] = column(normed, w, j).astype(bf16)
 
 
@@ -267,7 +385,7 @@
 
         @pl.when(pl.program_id(0) == k)
         def _():
-            for j in range(w.shape[0] // 128):
+            for j in range(w.shape[1] // 128):
                 cols = slice(j * 128, (j + 1) * 128)
                 out_ref[:, cols] = (
                     column(normed, w, j) + received_ref[0, :, cols].astype(f32)
@@ -291,7 +409,7 @@
                 constant_block(T, 256),
                 constant_block(256, 128),
                 constant_block(1, 256),
-                pl.BlockSpec((width, 256), lambda i, order: (order[i], 0)),
+                pl.BlockSpec((2, width, 128), lambda i, order: (0, order[i], 0)),
             ],
             out_specs=[
                 constant_block(T, 256),
@@ -318,7 +436,7 @@
             in_specs=[
                 constant_block(T, 256),
                 pl.BlockSpec((1, T, width), lambda i, order: (i, 0, 0)),
-                pl.BlockSpec((width, 256), lambda i, order: (order[i], 0)),
+                pl.BlockSpec((2, width, 128), lambda i, order: (0, order[i], 0)),
             ],
             out_specs=[constant_block(T, width)] * chips,
         ),
@@ -385,34 +503,21 @@
     members = lax.axis_size("sp")
     pieces = lax.axis_size("tp")
     depth = w_query.shape[0]
-    own = jnp.concatenate(
-        [w_out[:depth], w_out[depth:], w_query, w_key, w_value, w_rank[0], w_rank[1]], axis=1
-    )
-    gathered = lax.all_gather(own, "sp").reshape(members * depth, own.shape[1])
-
-    silu = jnp.stack([jax.nn.silu(cond_latent), jax.nn.silu(cond_context)]).astype(bf16)
-    terms = jnp.einsum("nd,rdc->nrc", silu, mod_weight, preferred_element_type=f32)
-    terms = jnp.concatenate([terms[0], terms[1, :2]], axis=0)
-    summed_terms = lax.all_gather(terms, "sp").sum(axis=0)
+    own = prepare(
+        cond_latent, cond_context, mod_weight, w_query, w_key, w_value, w_rank, w_out
+    ).astype(f16)
+    everyone = lax.all_gather(own, "sp", axis=1, tiled=True)
+
+    gathered = (everyone[:7].astype(f32) * (1.0 / WEIGHT_SCALE)).astype(bf16)
+    lines = 5 * mod_weight.shape[2] // 128
+    sums = everyone[7].reshape(members, depth, 128)[:, : 2 * lines].astype(f32).sum(axis=0)
+    summed_terms = (sums[:lines] + sums[lines:]) * (1.0 / TERM_SCALE)
     rows = sent_to_all(summed_terms, "tp")
-    modulation = jnp.moveaxis(rows, 0, 1).reshape(rows.shape[1], width)
-
-    extra = 16 - context.shape[0]
-    tokens = jnp.concatenate([latent, context, jnp.zeros((extra, width), bf16)], axis=0)
-    widened = tokens.astype(f32)
-    normalized = widened * lax.rsqrt(jnp.mean(widened * widened, axis=-1, keepdims=True) + eps)
-    is_latent = (jnp.arange(T + 16) < T)[:, None]
-    scale = jnp.where(is_latent, modulation[1], modulation[4])
-    shift = jnp.where(is_latent, modulation[0], modulation[3])
-    h = (normalized * norm_gain * (1.0 + scale) + shift).astype(bf16)
-
-    decay_weight = jnp.zeros((128, 256), bf16)
-    decay_weight = decay_weight.at[:64, :128].set(w_decay[0]).at[64:, 128:].set(w_decay[1])
-    shifts = jnp.repeat(decay_shift, DK, axis=1)
-    shifts = jnp.concatenate([shifts, shifts], axis=1)
+    gate = summed_terms.reshape(5, -1)[2]
 
     loc, lift, send = mixing(
-        h, gathered, decay_weight, decay_bias.reshape(1, 256), shifts, members
+        latent, context, stats(latent, context), rows, norm_gain, gathered, w_decay, decay_bias,
+        decay_shift, members,
     )
     received = lax.all_to_all(send, "sp", split_axis=0, concat_axis=0, tiled=True)
     entries = lax.all_to_all(chain(received), "sp", split_axis=0, concat_axis=0, tiled=True)
@@ -429,7 +534,7 @@
     summed = sums[0].astype(f32)
     for i in range(1, chips):
         summed = summed + to_chip(sums[i], i).astype(f32)
-    mixed = (own_latent.astype(f32) + summed_terms[2] * summed).astype(bf16)
+    mixed = (own_latent.astype(f32) + gate * summed).astype(bf16)
     mine = [mixed] + [to_chip(mixed, chips - i) for i in range(1, chips)]
     theirs = [to_partner(piece) for piece in mine]
     return joined(mine + theirs)

time: 335 us -> 325 us (0.970)
  blocking collectives: 134 us -> 189 us
  waiting for transfers between devices: 72.4 us -> 40.9 us
  starting transfers between devices: 78.3 us -> 54.7 us
  between operations: 13.8 us -> 0.3 us
    all_gather x1, blocking collectives: 93.2 us -> 148 us  [local(): everyone = lax.all_gather(own, 'sp', axis=1, tiled=True)]
    all_gather x1 -> x0, waiting for transfers between devices: 34.6 us -> none  [local(): gathered = lax.all_gather(own, 'sp').reshape(members * depth, own.shape[1])]
    ppermute x5, starting transfers between devices: 35.2 us -> 17.1 us  [to_partner(): return lax.ppermute(array, 'tp', [(i, i ^ 1) for i in range(n)])]
    ppermute x6, starting transfers between devices: 21.3 us -> 16 us  [to_chip(): lax.ppermute(array, 'tp', [(i, (i + 2 * ahead) % n) for i in range(n)])]
    convert_element_type x2 -> x3, other arithmetic: 4.84 us -> 10.1 us  [the longest x1 7.82 us: local(): gathered = (everyone[:7].astype(f32) * (1.0 / WEIGHT_SCALE)).astype(bf16)]
    ppermute x6, waiting for transfers between devices: 9.47 us -> 14 us  [to_chip(): lax.ppermute(array, 'tp', [(i, (i + 2 * ahead) % n) for i in range(n)])]
    pallas_call x1 -> x3, Pallas kernels: 11 us -> 13.9 us  [the longest x1 11.4 us: mixing(): pl.pallas_call(mixing_kernel, grid=(steps,), in_specs=[pl.BlockSpec((T, d...]
  transfers between devices with their start and end apart: 14 -> 13, of which waited for: 9 -> 7; matrix products, arithmetic and copies ran while one was open for 3% -> 2% of each run, Pallas kernels for 0% -> 0%
where the time goes in v3:
time: 325 us; the launch traced here: 324 us
  blocking collectives  189 us (58%)
  starting transfers between devices  54.7 us (17%)
  waiting for transfers between devices  40.9 us (13%)
  Pallas kernels  24.5 us (8%)
  other arithmetic  10.2 us (3%)
  local copies, waits for them, and re-layouts  4.14 us (1%)
    all_gather x1, blocking collectives, local(): everyone = lax.all_gather(own, 'sp', axis=1, tiled=True)  148 us
    all_to_all x1, blocking collectives, local(): lax.all_to_all(send, 'sp', split_axis=0, concat_axis=0, tiled=True)  40.8 us
    all_to_all x1, waiting for transfers between devices, local(): lax.all_to_all(chain(received), 'sp', split_axis=0, concat_axis=0, tiled=...  23.5 us
    ppermute x5, starting transfers between devices, to_partner(): return lax.ppermute(array, 'tp', [(i, i ^ 1) for i in range(n)])  17.1 us
    all_to_all x1, starting transfers between devices, sent_to_all(): return lax.all_to_all(copies, axis, split_axis=0, concat_axis=0, tiled=True)  16.9 us
    ppermute x6, starting transfers between devices, to_chip(): lax.ppermute(array, 'tp', [(i, (i + 2 * ahead) % n) for i in range(n)])  16 us
    ppermute x6, waiting for transfers between devices, to_chip(): lax.ppermute(array, 'tp', [(i, (i + 2 * ahead) % n) for i in range(n)])  14 us
    pallas_call x1, Pallas kernels, mixing(): pl.pallas_call(mixing_kernel, grid=(steps,), in_specs=[pl.BlockSpec((T, d...  11.4 us
  transfers between devices with their start and end apart: 13, of which 7 were waited for; matrix products, arithmetic and copies ran while one was open for 2% of the time, Pallas kernels for 0%

profile of v3, /device:TPU:33, one launch (start us, length us, event | category | flops | bytes accessed | tf_op | source)
XLA Modules:
  0.0 323.7 jit_solution(6642970209428039723)
XLA Ops:
  0.0 2.1 prepare.1
  3.2 148.1 %all-gather.1 = f16[8,4096,128]{2,1,0:T(8,128)(2,1)S(1)} all-gather(f16[8,128,128]{2,1,0:T(8,128)(2,1)S(1)} %convert_element_type.31), channel_id=1, replica_groups=mesh['grp'=2,'sp'=32,'tp'=8] {'sp'}, dimensions={1}, use_global_device_ids=true | all-gather | bytes 8650752 | tf_op jit(solution)/shard_map/all_gather | solution.py:509
  151.3 3.2 %copy-done.7 = f16[8,4096,128]{2,1,0:T(8,128)(2,1)} copy-done((f16[8,4096,128]{2,1,0:T(8,128)(2,1)}, f16[8,4096,128]{2,1,0:T(8,128)(2,1)S(1)}, u32[]{:S(2)}) %copy-start.7) | copy-done | bytes 8388632
  155.4 16.9 %all-to-all-start = ((f32[8,20,128]{2,1,0:T(8,128)}), f32[8,20,128]{2,1,0:T(8,128)S(1)}, u32[]{:S(2)}, u32[]{:S(2)}) async-start(f32[8,20,128]{2,1,0:T(8,128)} %broadcast_in_dim.3), calls=%async_computation | async-start | bytes 196608 | tf_op jit(solution)/shard_map/all_to_all | solution.py:22
  172.4 7.8 %multiply_convert_fusion.wq_ref.wk_ref.wv0_ref.wv1_ref.wr_ref.w_ref = bf16[7,4096,128]{2,1,0:T(8,128)(2,1)} fusion(f16[8,4096,128]{2,1,0:T(8,128)(2,1)} %copy-done.7), kind=kLoop, calls=%fused_computation | loop fusion | flops 11010048 | bytes 14680064 | tf_op jit(solution)/shard_map/convert_element_type | solution.py:511
  180.7 11.4 %mixing.1 = (f32[256,256]{1,0:T(8,128)S(1)}, bf16[256,256]{1,0:T(8,128)(2,1)S(1)}, bf16[32,24,128]{2,1,0:T(8,128)(2,1)S(1)}) custom-call(bf16[256,4096]{1,0:T(8,128)(2,1)S(1)} %copy-done, bf16[8,4096]{1,0:T(8,128)(2,1)S(1)} %copy-done.1, f32[264,128]{1,0:T(8,128)S(1)} %stats.1.stats_ref, f32[8,20,128]{2,1,0:T(8,128)S(1)} %all-to-all-done.rows_ref, ...), custom_call_target="tpu_custom_call" | custom-call | tf_op jit(solution)/shard_map/mixing/pallas_call | solution.py:290
  192.1 40.8 %all_to_all.15.in_ref = bf16[32,24,128]{2,1,0:T(8,128)(2,1)} all-to-all(bf16[32,24,128]{2,1,0:T(8,128)(2,1)S(1)} %get-tuple-element.16), channel_id=1, replica_groups=mesh['grp'=2,'sp'=32,'tp'=8] {'sp'}, dimensions={0} | all-to-all | bytes 393216 | tf_op jit(solution)/shard_map/all_to_all | solution.py:522
  234.8 4.8 %all-to-all-start.2 = ((bf16[32,8,128]{2,1,0:T(8,128)(2,1)}), bf16[32,8,128]{2,1,0:T(8,128)(2,1)S(1)}, u32[]{:S(2)}, u32[]{:S(2)}) async-start(bf16[32,8,128]{2,1,0:T(8,128)(2,1)} %chain.1), calls=%async_computation.2 | async-start | bytes 131072 | tf_op jit(solution)/shard_map/all_to_all | solution.py:523
  239.6 23.5 %all-to-all-done.2 = bf16[32,8,128]{2,1,0:T(8,128)(2,1)S(1)} async-done(((bf16[32,8,128]{2,1,0:T(8,128)(2,1)}), bf16[32,8,128]{2,1,0:T(8,128)(2,1)S(1)}, u32[]{:S(2)}, u32[]{:S(2)}) %all-to-all-start.2) | async-done | bytes 65568 | tf_op jit(solution)/shard_map/all_to_all | solution.py:523
  263.1 3.7 %sent.1 = (bf16[256,256]{1,0:T(8,128)(2,1)S(1)}, bf16[4,256,512]{2,1,0:T(8,128)(2,1)S(1)}) custom-call(s32[4]{0:T(128)S(1)} %get-tuple-element.23.order_ref, f32[256,256]{1,0:T(8,128)S(1)} %get-tuple-element.14.loc_ref, bf16[256,256]{1,0:T(8,128)(2,1)S(1)} %get-tuple-element.15.lift_ref, bf16[256,128]{1,0:T(8,128)(2,1)S(1)} %bitcast.13, ...), custom_call_target="tpu_custom_call" | custom-call | tf_op jit(solution)/shard_map/sent/pallas_call | solution.py:402
  266.9 4.5 %collective-permute-start = (bf16[4,256,512]{2,1,0:T(8,128)(2,1)S(1)}, bf16[4,256,512]{2,1,0:T(8,128)(2,1)S(1)}, u32[]{:S(2)}, u32[]{:S(2)}) collective-permute-start(bf16[4,256,512]{2,1,0:T(8,128)(2,1)S(1)} %get-tuple-element.18), channel_id=1, source_target_pairs={{0,1},{1,0},{2,3},{3,2},{4,5},{5,4},{6,7},{7,6},{8,9},{9,8},{10,11... | collective-permute-start | bytes 3145736 | tf_op jit(solution)/shard_map/ppermute | solution.py:477
  271.4 2.3 collective-permute-done.received_ref
  273.6 3.5 %kept.1 = (bf16[256,512]{1,0:T(8,128)(2,1)S(1)}, bf16[256,512]{1,0:T(8,128)(2,1)S(1)}, bf16[256,512]{1,0:T(8,128)(2,1)S(1)}, bf16[256,512]{1,0:T(8,128)(2,1)S(1)}) custom-call(s32[4]{0:T(128)S(1)} %get-tuple-element.24.order_ref, bf16[256,256]{1,0:T(8,128)(2,1)S(1)} %get-tuple-element.17.normed, bf16[4,256,512]{2,1,0:T(8,128)(2,1)S(1)} %collective-permute-done.received_ref, ...), custom_call_target="tpu_custom_call" | custom-call | tf_op jit(solution)/shard_map/kept/pallas_call | solution.py:431
  277.1 3.6 %collective-permute-start.3 = (bf16[256,512]{1,0:T(8,128)(2,1)S(1)}, bf16[256,512]{1,0:T(8,128)(2,1)S(1)}, u32[]{:S(2)}, u32[]{:S(2)}) collective-permute-start(bf16[256,512]{1,0:T(8,128)(2,1)S(1)} %get-tuple-element.22), channel_id=1, source_target_pairs={{0,6},{1,7},{2,0},{3,1},{4,2},{5,3},{6,4},{7,5},{8,14},{9,15},{10,... | collective-permute-start | bytes 786440 | tf_op jit(solution)/shard_map/ppermute | solution.py:482
  280.8 2.5 collective-permute-start.2
  283.3 2.5 collective-permute-start.1
  286.6 5.0 %collective-permute-done.2 = bf16[256,512]{1,0:T(8,128)(2,1)} collective-permute-done((bf16[256,512]{1,0:T(8,128)(2,1)S(1)}, bf16[256,512]{1,0:T(8,128)(2,1)}, u32[]{:S(2)}, u32[]{:S(2)}) %collective-permute-start.2) | collective-permute-done | bytes 262176 | tf_op jit(solution)/shard_map/ppermute | solution.py:482
  291.6 6.6 %collective-permute-done.1 = bf16[256,512]{1,0:T(8,128)(2,1)} collective-permute-done((bf16[256,512]{1,0:T(8,128)(2,1)S(1)}, bf16[256,512]{1,0:T(8,128)(2,1)}, u32[]{:S(2)}, u32[]{:S(2)}) %collective-permute-start.1) | collective-permute-done | bytes 262176 | tf_op jit(solution)/shard_map/ppermute | solution.py:482
  301.4 2.5 collective-permute-start.5
  303.9 2.8 collective-permute-start.6
  306.7 3.2 collective-permute-start.7
  310.0 3.0 collective-permute-start.8
  312.9 4.0 %collective-permute-start.9 = (bf16[256,512]{1,0:T(8,128)(2,1)S(1)}, bf16[256,512]{1,0:T(8,128)(2,1)S(1)}, u32[]{:S(2)}, u32[]{:S(2)}) collective-permute-start(bf16[256,512]{1,0:T(8,128)(2,1)S(1)} %collective-permute-done.5.refs_2_), channel_id=1, source_target_pairs={{0,1},{1,0},{2,3},{3,2},{4,5},{5,4},{6,7},{7,6},{8,9},{9,8},{10,11... | collective-permute-start | bytes 786440 | tf_op jit(solution)/shard_map/ppermute | solution.py:477
  318.6 2.4 collective-permute-start.10
  (36 shorter events, 12.6 us)
Async XLA Ops:
  151.3 3.2 %copy-start.7 = (f16[8,4096,128]{2,1,0:T(8,128)(2,1)}, f16[8,4096,128]{2,1,0:T(8,128)(2,1)S(1)}, u32[]{:S(2)}) copy-start(f16[8,4096,128]{2,1,0:T(8,128)(2,1)S(1)} %all-gather.1) | copy-start | bytes 25165828
  155.4 25.2 %all-to-all-start = ((f32[8,20,128]{2,1,0:T(8,128)}), f32[8,20,128]{2,1,0:T(8,128)S(1)}, u32[]{:S(2)}, u32[]{:S(2)}) async-start(f32[8,20,128]{2,1,0:T(8,128)} %broadcast_in_dim.3), calls=%async_computation | async-start | bytes 196608 | tf_op jit(solution)/shard_map/all_to_all | solution.py:22
  172.3 7.9 %copy-start = (bf16[256,4096]{1,0:T(8,128)(2,1)S(1)}, bf16[256,4096]{1,0:T(8,128)(2,1)}, u32[]{:S(2)}) copy-start(bf16[256,4096]{1,0:T(8,128)(2,1)} %latent_ref.3) | copy-start | bytes 6291460
  172.3 7.9 %copy-start.1 = (bf16[8,4096]{1,0:T(8,128)(2,1)S(1)}, bf16[8,4096]{1,0:T(8,128)(2,1)}, u32[]{:S(2)}) copy-start(bf16[8,4096]{1,0:T(8,128)(2,1)} %context_ref.3) | copy-start | bytes 196612
  172.3 8.4 %copy-start.2 = (bf16[2,64,128]{2,1,0:T(8,128)(2,1)S(1)}, bf16[2,64,128]{2,1,0:T(8,128)(2,1)}, u32[]{:S(2)}) copy-start(bf16[2,64,128]{2,1,0:T(8,128)(2,1)} %param.25) | copy-start | bytes 98308
  172.3 8.4 %copy-start.3 = (f32[4096]{0:T(1024)S(1)}, f32[4096]{0:T(1024)}, u32[]{:S(2)}) copy-start(f32[4096]{0:T(1024)} %param.20) | copy-start | bytes 49156
  172.3 8.4 %copy-start.4 = (f32[256,2]{0,1:T(2,128)S(1)}, f32[256,2]{0,1:T(2,128)}, u32[]{:S(2)}) copy-start(f32[256,2]{0,1:T(2,128)} %param.27) | copy-start | bytes 6148
  172.3 8.4 %copy-start.5 = (f32[2,128]{1,0:T(2,128)S(1)}, f32[2,128]{1,0:T(2,128)}, u32[]{:S(2)}) copy-start(f32[2,128]{1,0:T(2,128)} %bias_ref.1) | copy-start | bytes 3076
  180.7 82.4 %copy-start.6 = (f32[256]{0:T(256)S(1)}, f32[256]{0:T(256)}, u32[]{:S(2)}) copy-start(f32[256]{0:T(256)} %param.28) | copy-start | bytes 3076
  234.8 28.3 %all-to-all-start.2 = ((bf16[32,8,128]{2,1,0:T(8,128)(2,1)}), bf16[32,8,128]{2,1,0:T(8,128)(2,1)S(1)}, u32[]{:S(2)}, u32[]{:S(2)}) async-start(bf16[32,8,128]{2,1,0:T(8,128)(2,1)} %chain.1), calls=%async_computation.2 | async-start | bytes 131072 | tf_op jit(solution)/shard_map/all_to_all | solution.py:523
  266.9 6.8 %collective-permute-start = (bf16[4,256,512]{2,1,0:T(8,128)(2,1)S(1)}, bf16[4,256,512]{2,1,0:T(8,128)(2,1)S(1)}, u32[]{:S(2)}, u32[]{:S(2)}) collective-permute-start(bf16[4,256,512]{2,1,0:T(8,128)(2,1)S(1)} %get-tuple-element.18), channel_id=1, source_target_pairs={{0,1},{1,0},{2,3},{3,2},{4,5},{5,4},{6,7},{7,6},{8,9},{9,8},{10,11... | collective-permute-start | bytes 3145736 | tf_op jit(solution)/shard_map/ppermute | solution.py:477
  277.1 9.4 %collective-permute-start.3 = (bf16[256,512]{1,0:T(8,128)(2,1)S(1)}, bf16[256,512]{1,0:T(8,128)(2,1)S(1)}, u32[]{:S(2)}, u32[]{:S(2)}) collective-permute-start(bf16[256,512]{1,0:T(8,128)(2,1)S(1)} %get-tuple-element.22), channel_id=1, source_target_pairs={{0,6},{1,7},{2,0},{3,1},{4,2},{5,3},{6,4},{7,5},{8,14},{9,15},{10,... | collective-permute-start | bytes 786440 | tf_op jit(solution)/shard_map/ppermute | solution.py:482
  280.8 10.8 %collective-permute-start.2 = (bf16[256,512]{1,0:T(8,128)(2,1)S(1)}, bf16[256,512]{1,0:T(8,128)(2,1)}, u32[]{:S(2)}, u32[]{:S(2)}) collective-permute-start(bf16[256,512]{1,0:T(8,128)(2,1)S(1)} %get-tuple-element.21), channel_id=1, source_target_pairs={{0,4},{1,5},{2,6},{3,7},{4,0},{5,1},{6,2},{7,3},{8,12},{9,13},{10,... | collective-permute-start | bytes 786440 | tf_op jit(solution)/shard_map/ppermute | solution.py:482
  283.3 14.9 %collective-permute-start.1 = (bf16[256,512]{1,0:T(8,128)(2,1)S(1)}, bf16[256,512]{1,0:T(8,128)(2,1)}, u32[]{:S(2)}, u32[]{:S(2)}) collective-permute-start(bf16[256,512]{1,0:T(8,128)(2,1)S(1)} %get-tuple-element.20), channel_id=1, source_target_pairs={{0,2},{1,3},{2,4},{3,5},{4,6},{5,7},{6,0},{7,1},{8,10},{9,11},{10,... | collective-permute-start | bytes 786440 | tf_op jit(solution)/shard_map/ppermute | solution.py:482
  299.4 10.6 %collective-permute-start.4 = (bf16[256,512]{1,0:T(8,128)(2,1)S(1)}, bf16[256,512]{1,0:T(8,128)(2,1)S(1)}, u32[]{:S(2)}, u32[]{:S(2)}) collective-permute-start(bf16[256,512]{1,0:T(8,128)(2,1)S(1)} %add_convert_fusion.refs_0_), channel_id=1, source_target_pairs={{0,6},{1,7},{2,0},{3,1},{4,2},{5,3},{6,4},{7,5},{8,14},{9,15},{10,... | collective-permute-start | bytes 786440 | tf_op jit(solution)/shard_map/ppermute | solution.py:482
  301.4 11.6 %collective-permute-start.5 = (bf16[256,512]{1,0:T(8,128)(2,1)S(1)}, bf16[256,512]{1,0:T(8,128)(2,1)S(1)}, u32[]{:S(2)}, u32[]{:S(2)}) collective-permute-start(bf16[256,512]{1,0:T(8,128)(2,1)S(1)} %add_convert_fusion.refs_0_), channel_id=1, source_target_pairs={{0,4},{1,5},{2,6},{3,7},{4,0},{5,1},{6,2},{7,3},{8,12},{9,13},{10,... | collective-permute-start | bytes 786440 | tf_op jit(solution)/shard_map/ppermute | solution.py:482
  303.9 14.8 %collective-permute-start.6 = (bf16[256,512]{1,0:T(8,128)(2,1)S(1)}, bf16[256,512]{1,0:T(8,128)(2,1)S(1)}, u32[]{:S(2)}, u32[]{:S(2)}) collective-permute-start(bf16[256,512]{1,0:T(8,128)(2,1)S(1)} %add_convert_fusion.refs_0_), channel_id=1, source_target_pairs={{0,2},{1,3},{2,4},{3,5},{4,6},{5,7},{6,0},{7,1},{8,10},{9,11},{10,... | collective-permute-start | bytes 786440 | tf_op jit(solution)/shard_map/ppermute | solution.py:482
  306.7 14.3 %collective-permute-start.7 = (bf16[256,512]{1,0:T(8,128)(2,1)S(1)}, bf16[256,512]{1,0:T(8,128)(2,1)S(1)}, u32[]{:S(2)}, u32[]{:S(2)}) collective-permute-start(bf16[256,512]{1,0:T(8,128)(2,1)S(1)} %add_convert_fusion.refs_0_), channel_id=1, source_target_pairs={{0,1},{1,0},{2,3},{3,2},{4,5},{5,4},{6,7},{7,6},{8,9},{9,8},{10,11... | collective-permute-start | bytes 786440 | tf_op jit(solution)/shard_map/ppermute | solution.py:477
  310.0 11.1 %collective-permute-start.8 = (bf16[256,512]{1,0:T(8,128)(2,1)S(1)}, bf16[256,512]{1,0:T(8,128)(2,1)S(1)}, u32[]{:S(2)}, u32[]{:S(2)}) collective-permute-start(bf16[256,512]{1,0:T(8,128)(2,1)S(1)} %collective-permute-done.4.refs_1_), channel_id=1, source_target_pairs={{0,1},{1,0},{2,3},{3,2},{4,5},{5,4},{6,7},{7,6},{8,9},{9,8},{10,11... | collective-permute-start | bytes 786440 | tf_op jit(solution)/shard_map/ppermute | solution.py:477
  312.9 8.1 %collective-permute-start.9 = (bf16[256,512]{1,0:T(8,128)(2,1)S(1)}, bf16[256,512]{1,0:T(8,128)(2,1)S(1)}, u32[]{:S(2)}, u32[]{:S(2)}) collective-permute-start(bf16[256,512]{1,0:T(8,128)(2,1)S(1)} %collective-permute-done.5.refs_2_), channel_id=1, source_target_pairs={{0,1},{1,0},{2,3},{3,2},{4,5},{5,4},{6,7},{7,6},{8,9},{9,8},{10,11... | collective-permute-start | bytes 786440 | tf_op jit(solution)/shard_map/ppermute | solution.py:477
  318.6 3.6 %collective-permute-start.10 = (bf16[256,512]{1,0:T(8,128)(2,1)S(1)}, bf16[256,512]{1,0:T(8,128)(2,1)S(1)}, u32[]{:S(2)}, u32[]{:S(2)}) collective-permute-start(bf16[256,512]{1,0:T(8,128)(2,1)S(1)} %collective-permute-done.6.refs_3_), channel_id=1, source_target_pairs={{0,1},{1,0},{2,3},{3,2},{4,5},{5,4},{6,7},{7,6},{8,9},{9,8},{10,11... | collective-permute-start | bytes 786440 | tf_op jit(solution)/shard_map/ppermute | solution.py:477

commit v4 on v3

--- a/solution.py
+++ b/solution.py
@@ -14,6 +14,7 @@
 f16 = jnp.float16
 WEIGHT_SCALE = 2.0**17
 TERM_SCALE = 2.0**9
+TERM_ROWS = 8
 VMEM_LIMIT = 50 * 1024 * 1024
 
 
@@ -54,13 +55,18 @@
     return jnp.where(rows < DK, both[:, :DV], both[:, DV:])
 
 
+def summed(where, pair):
+    both = dot(jnp.where(where, 1.0, 0.0).astype(bf16), pair)
+    return both[:, 0:128] + both[:, 128:256]
+
+
 def prepare_kernel(
     cond_l_ref, cond_c_ref, mod_ref, q_ref, k_ref, v_ref, rank_ref, out_w_ref, out_ref
 ):
     depth = q_ref.shape[0]
 
     def put(block, array):
-        out_ref[block] = array.astype(f32) * WEIGHT_SCALE
+        out_ref[block, 0:depth, :] = array.astype(f32) * WEIGHT_SCALE
 
     put(0, out_w_ref[0:depth])
     put(1, out_w_ref[depth : 2 * depth])
@@ -77,7 +83,8 @@
     conds = jnp.where(
         row == 0, silu(cond_l_ref[...]), jnp.where(row == 1, silu(cond_c_ref[...]), 0.0)
     ).astype(bf16)
-    out_ref[7] = jnp.zeros((depth, 128), f32)
+    blocks = out_ref.shape[0]
+    out_ref[:, depth:, :] = jnp.zeros((blocks, TERM_ROWS, 128), f32)
     terms = [dot(conds, mod_ref[r]) * TERM_SCALE for r in range(3)]
     vectors = [(terms[0], 0), (terms[1], 0), (terms[2], 0), (terms[0], 1), (terms[1], 1)]
     columns = mod_ref.shape[2] // 128
@@ -87,8 +94,9 @@
             line = term[at : at + 1, c * 128 : (c + 1) * 128]
             high = line.astype(bf16).astype(f32)
             spot = n * columns + c
-            out_ref[7, spot : spot + 1, :] = high
-            out_ref[7, lines + spot : lines + spot + 1, :] = line - high
+            for at_row, value in ((spot, high), (lines + spot, line - high)):
+                place = depth + at_row % TERM_ROWS
+                out_ref[at_row // TERM_ROWS, place : place + 1, :] = value
 
 
 def prepare(cond_latent, cond_context, mod_weight, w_query, w_key, w_value, w_rank, w_out):
@@ -97,7 +105,7 @@
     ranks = jnp.swapaxes(w_rank, 1, 2).reshape(128, depth)
     return pl.pallas_call(
         prepare_kernel,
-        out_shape=jax.ShapeDtypeStruct((8, depth, 128), f32),
+        out_shape=jax.ShapeDtypeStruct((7, depth + TERM_ROWS, 128), f32),
         in_specs=[vmem] * 8,
         out_specs=vmem,
         name="prepare",
@@ -132,7 +140,7 @@
 def mixing_kernel(
     latent_ref, context_ref, stats_ref, rows_ref, gain_ref,
     wq_ref, wk_ref, wv0_ref, wv1_ref, wr_ref, wd_ref, bias_ref, shift_ref,
-    loc_ref, lift_ref, send_ref, acc,
+    qkv_ref, pairs_ref, send_ref, acc,
 ):
     step = pl.program_id(0)
     T = latent_ref.shape[0]
@@ -155,24 +163,28 @@
             parts.append((x * scale + shift).astype(bf16))
         return jnp.concatenate(parts, axis=1)
 
-    w_qk = jnp.concatenate([wq_ref[0], wk_ref[0]], axis=1)
-    w_v = jnp.concatenate([wv0_ref[0], wv1_ref[0]], axis=1)
+    def weight(ref):
+        depth = ref.shape[2] - TERM_ROWS
+        return jnp.concatenate([ref[0, j, 0:depth] for j in range(ref.shape[1])], axis=0)
+
+    w_qk = jnp.concatenate([weight(wq_ref), weight(wk_ref)], axis=1)
+    w_v = jnp.concatenate([weight(wv0_ref), weight(wv1_ref)], axis=1)
     h = modulated(latent_ref, 0, T, 0, 1)
     hc = modulated(context_ref, T, C, 3, 4)
     h = jnp.concatenate([h, hc, jnp.zeros((acc.shape[0] - T - C, h.shape[1]), bf16)], axis=0)
     acc[:, 0:256] += dot(h, w_qk)
     acc[:, 256:512] += dot(h, w_v)
-    acc[:, 512:640] += dot(h, wr_ref[0])
+    acc[:, 512:640] += dot(h, weight(wr_ref))
 
     @pl.when(step == pl.num_programs(0) - 1)
     def _():
         C = acc.shape[0] - T
-        q16 = acc[0:T, 0:128].astype(bf16)
-        k16 = acc[0:T, 128:256].astype(bf16)
-        v = acc[0:T, 256:512].astype(bf16)
-        q = q16.astype(f32)
+        unscale = 1.0 / WEIGHT_SCALE
+        q16 = (acc[0:T, 0:128] * unscale).astype(bf16)
+        k16 = (acc[0:T, 128:256] * unscale).astype(bf16)
+        v = (acc[0:T, 256:512] * unscale).astype(bf16)
         k = k16.astype(f32)
-        ranks = acc[:, 512:640].astype(bf16)
+        ranks = (acc[:, 512:640] * unscale).astype(bf16)
         rank_lane = iota(ranks.shape, 1)
         none = jnp.zeros_like(ranks)
         pre = jnp.concatenate(
@@ -189,54 +201,17 @@
 
         shifts = jnp.where(iota((T, 128), 1) < DK, down(0), down(1))
         lat = logs[0:T] + jnp.concatenate([shifts, shifts], axis=1)
+        qkv_ref[:, 0:128] = q16
+        qkv_ref[:, 128:256] = k16
+        qkv_ref[:, 256:512] = v
         f_high, f_low = halves(lat[:, 0:128])
         b_high, b_low = halves(lat[:, 128:256])
         f_pair = jnp.concatenate([f_high, f_low], axis=1)
         b_pair = jnp.concatenate([b_high, b_low], axis=1)
-
-        def summed(where, pair):
-            both = dot(jnp.where(where, 1.0, 0.0).astype(bf16), pair)
-            return both[:, 0:128] + both[:, 128:256]
-
+        pairs_ref[:, 0:256] = f_pair
+        pairs_ref[:, 256:512] = b_pair
         r = iota((T, T), 0)
         s = iota((T, T), 1)
-        lane = iota((T, 128), 1)
-        row = iota((T, 128), 0)
-        first = lane < DK
-        zero = jnp.zeros((T, 128), bf16)
-
-        def scores(qs, ks):
-            return (
-                dot_nt(qs, jnp.where(first, ks, zero)),
-                dot_nt(qs, jnp.where(first, zero, ks)),
-            )
-
-        s0, s1 = scores(q16, k16)
-        s0 = 2.0 * s0
-        s1 = 2.0 * s1
-        m = 1
-        while m < T:
-            base = (r // (2 * m)) * (2 * m)
-            ref = base + m
-            upper = r >= ref
-            lower = r < ref
-            d_f = (upper & (s >= ref) & (s <= r)) | (lower & (s > r) & (s < ref))
-            d_b = (upper & (s >= ref) & (s < r)) | (lower & (s >= r) & (s < ref))
-            fac_f = jnp.exp(summed(d_f, f_pair))
-            fac_b = jnp.exp(summed(d_b, b_pair))
-            up = (row & m) != 0
-            qs = (q * jnp.where(up, fac_f, fac_b)).astype(bf16)
-            ks = (k * jnp.where(up, fac_b, fac_f)).astype(bf16)
-            m0, m1 = scores(qs, ks)
-            pick = ((r ^ s) >= m) & ((r ^ s) < 2 * m)
-            s0 = jnp.where(pick, m0, s0)
-            s1 = jnp.where(pick, m1, s1)
-            m *= 2
-        loc_ref[:, 0:128] = dot(s0.astype(bf16), v[:, 0:128])
-        loc_ref[:, 128:256] = dot(s1.astype(bf16), v[:, 128:256])
-
-        lift_ref[:, 0:128] = (q * jnp.exp(summed(s <= r, f_pair))).astype(bf16)
-        lift_ref[:, 128:256] = (q * jnp.exp(summed(s >= r, b_pair))).astype(bf16)
         k_f = (k * jnp.exp(summed(s > r, f_pair))).astype(bf16)
         k_b = (k * jnp.exp(summed(s < r, b_pair))).astype(bf16)
 
@@ -253,8 +228,8 @@
 
         crow = iota((C, 128), 0)
         live = crow < 8
-        kc = jnp.where(live, acc[T : T + C, 128:256].astype(bf16).astype(f32), 0.0)
-        vc = acc[T : T + C, 256:512].astype(bf16)
+        kc = jnp.where(live, (acc[T : T + C, 128:256] * unscale).astype(bf16).astype(f32), 0.0)
+        vc = (acc[T : T + C, 256:512] * unscale).astype(bf16)
         ctx_f = jnp.where(live, logs[T : T + C, 0:128], 0.0)
         ctx_b = jnp.where(live, logs[T : T + C, 128:256], 0.0)
         cf_high, cf_low = halves(ctx_f)
@@ -296,15 +271,21 @@
             whole(T + C, 128),
             pl.BlockSpec((1, *rows.shape[1:]), lambda i: (i, 0, 0)),
             pl.BlockSpec((1, 1, depth), lambda i: (i, 0, 0)),
-            *[pl.BlockSpec((1, depth, 128), lambda i, b=b: (b, i, 0)) for b in range(2, 7)],
+            *[
+                pl.BlockSpec(
+                    (1, gathered.shape[1] // steps, gathered.shape[2], 128),
+                    lambda i, b=b: (b, i, 0, 0),
+                )
+                for b in range(2, 7)
+            ],
             whole(128, 128),
             whole(2, 128),
             whole(2, T),
         ],
-        out_specs=[whole(T, 256), whole(T, 256), whole(members, 24, 128)],
+        out_specs=[whole(T, 512), whole(T, 512), whole(members, 24, 128)],
         out_shape=[
-            jax.ShapeDtypeStruct((T, 256), f32),
-            jax.ShapeDtypeStruct((T, 256), bf16),
+            jax.ShapeDtypeStruct((T, 512), bf16),
+            jax.ShapeDtypeStruct((T, 512), bf16),
             jax.ShapeDtypeStruct((members, 24, 128), bf16),
         ],
         scratch_shapes=[pltpu.VMEM((T + 16, 640), f32)],
@@ -314,6 +295,74 @@
         latent, context, scales, rows, gain.reshape(steps, 1, depth), *[gathered] * 5,
         w_decay.reshape(128, 128), decay_bias, decay_shift.T,
     )
+
+
+def scores_kernel(qkv_ref, pairs_ref, loc_ref, lift_ref):
+    T = qkv_ref.shape[0]
+    q16 = qkv_ref[:, 0:128]
+    k16 = qkv_ref[:, 128:256]
+    v = qkv_ref[:, 256:512]
+    q = q16.astype(f32)
+    k = k16.astype(f32)
+    f_pair = pairs_ref[:, 0:256]
+    b_pair = pairs_ref[:, 256:512]
+    r = iota((T, T), 0)
+    s = iota((T, T), 1)
+    lane = iota((T, 128), 1)
+    row = iota((T, 128), 0)
+    first = lane < DK
+    zero = jnp.zeros((T, 128), bf16)
+
+    def scores(qs, ks):
+        return (
+            dot_nt(qs, jnp.where(first, ks, zero)),
+            dot_nt(qs, jnp.where(first, zero, ks)),
+        )
+
+    s0, s1 = scores(q16, k16)
+    s0 = 2.0 * s0
+    s1 = 2.0 * s1
+    m = 1
+    while m < T:
+        base = (r // (2 * m)) * (2 * m)
+        ref = base + m
+        upper = r >= ref
+        lower = r < ref
+        d_f = (upper & (s >= ref) & (s <= r)) | (lower & (s > r) & (s < ref))
+        d_b = (upper & (s >= ref) & (s < r)) | (lower & (s >= r) & (s < ref))
+        fac_f = jnp.exp(summed(d_f, f_pair))
+        fac_b = jnp.exp(summed(d_b, b_pair))
+        up = (row & m) != 0
+        qs = (q * jnp.where(up, fac_f, fac_b)).astype(bf16)
+        ks = (k * jnp.where(up, fac_b, fac_f)).astype(bf16)
+        m0, m1 = scores(qs, ks)
+        pick = ((r ^ s) >= m) & ((r ^ s) < 2 * m)
+        s0 = jnp.where(pick, m0, s0)
+        s1 = jnp.where(pick, m1, s1)
+        m *= 2
+    loc_ref[:, 0:128] = dot(s0.astype(bf16), v[:, 0:128])
+    loc_ref[:, 128:256] = dot(s1.astype(bf16), v[:, 128:256])
+    lift_ref[:, 0:128] = (q * jnp.exp(summed(s <= r, f_pair))).astype(bf16)
+    lift_ref[:, 128:256] = (q * jnp.exp(summed(s >= r, b_pair))).astype(bf16)
+
+
+def local_scores(qkv, pairs):
+    T = qkv.shape[0]
+    vmem = pl.BlockSpec(memory_space=pltpu.VMEM)
+    return pl.pallas_call(
+        scores_kernel,
+        out_shape=[
+            jax.ShapeDtypeStruct((T, 256), f32),
+            jax.ShapeDtypeStruct((T, 256), bf16),
+        ],
+        in_specs=[vmem] * 2,
+        out_specs=[vmem] * 2,
+        compiler_params=pltpu.CompilerParams(vmem_limit_bytes=VMEM_LIMIT),
+        cost_estimate=pl.CostEstimate(
+            flops=40 * 2 * T * T * 256, bytes_accessed=T * 4096, transcendentals=20 * T * 128
+        ),
+        name="scores",
+    )(qkv, pairs)
 
 
 def chain_kernel(in_ref, out_ref):
@@ -365,8 +414,7 @@
 
 
 def column(normed, w, j):
-    rows = slice(j * 128, (j + 1) * 128)
-    return dot(normed[:, 0:128], w[0, rows]) + dot(normed[:, 128:256], w[1, rows])
+    return (dot(normed[:, 0:128], w[0, j, 0:128]) + dot(normed[:, 128:256], w[1, j, 0:128])) * (1.0 / WEIGHT_SCALE)
 
 
 def sent_kernel(order_ref, loc_ref, lift_ref, entry_ref, gain_ref, w_ref, normed, out_ref):
@@ -375,7 +423,7 @@
         normalized_output(loc_ref, lift_ref, entry_ref, gain_ref, normed)
 
     w = w_ref[...]
-    for j in range(w.shape[1] // 128):
+    for j in range(w.shape[1]):
         out_ref[0, :, j * 128 : (j + 1) * 128] = column(normed, w, j).astype(bf16)
 
 
@@ -385,7 +433,7 @@
 
         @pl.when(pl.program_id(0) == k)
         def _():
-            for j in range(w.shape[1] // 128):
+            for j in range(w.shape[1]):
                 cols = slice(j * 128, (j + 1) * 128)
                 out_ref[:, cols] = (
                     column(normed, w, j) + received_ref[0, :, cols].astype(f32)
@@ -409,7 +457,10 @@
                 constant_block(T, 256),
                 constant_block(256, 128),
                 constant_block(1, 256),
-                pl.BlockSpec((2, width, 128), lambda i, order: (0, order[i], 0)),
+                pl.BlockSpec(
+                    (2, width // 128, gathered.shape[2], 128),
+                    lambda i, order: (0, order[i], 0, 0),
+                ),
             ],
             out_specs=[
                 constant_block(T, 256),
@@ -436,7 +487,10 @@
             in_specs=[
                 constant_block(T, 256),
                 pl.BlockSpec((1, T, width), lambda i, order: (i, 0, 0)),
-                pl.BlockSpec((2, width, 128), lambda i, order: (0, order[i], 0)),
+                pl.BlockSpec(
+                    (2, width // 128, gathered.shape[2], 128),
+                    lambda i, order: (0, order[i], 0, 0),
+                ),
             ],
             out_specs=[constant_block(T, width)] * chips,
         ),
@@ -506,19 +560,19 @@
     own = prepare(
         cond_latent, cond_context, mod_weight, w_query, w_key, w_value, w_rank, w_out
     ).astype(f16)
-    everyone = lax.all_gather(own, "sp", axis=1, tiled=True)
-
-    gathered = (everyone[:7].astype(f32) * (1.0 / WEIGHT_SCALE)).astype(bf16)
+    everyone = lax.all_gather(own, "sp", axis=1, tiled=True).astype(bf16)
+    gathered = everyone.reshape(own.shape[0], members, depth + TERM_ROWS, 128)
     lines = 5 * mod_weight.shape[2] // 128
-    sums = everyone[7].reshape(members, depth, 128)[:, : 2 * lines].astype(f32).sum(axis=0)
-    summed_terms = (sums[:lines] + sums[lines:]) * (1.0 / TERM_SCALE)
+    sums = gathered[:, :, depth:].astype(f32).sum(axis=1).reshape(-1, 128)
+    summed_terms = (sums[:lines] + sums[lines : 2 * lines]) * (1.0 / TERM_SCALE)
     rows = sent_to_all(summed_terms, "tp")
     gate = summed_terms.reshape(5, -1)[2]
 
-    loc, lift, send = mixing(
+    qkv, pairs, send = mixing(
         latent, context, stats(latent, context), rows, norm_gain, gathered, w_decay, decay_bias,
         decay_shift, members,
     )
+    loc, lift = local_scores(qkv, pairs)
     received = lax.all_to_all(send, "sp", split_axis=0, concat_axis=0, tiled=True)
     entries = lax.all_to_all(chain(received), "sp", split_axis=0, concat_axis=0, tiled=True)
     columns = width // pieces

time: 325 us -> 321 us (0.988)
  waiting for transfers between devices: 40.9 us -> 37.2 us
  starting transfers between devices: 54.7 us -> 58.2 us
  local copies, waits for them, and re-layouts: 4.14 us -> 0.68 us
    all_to_all x1, waiting for transfers between devices: 23.5 us -> 18.9 us  [local(): lax.all_to_all(chain(received), 'sp', split_axis=0, concat_axis=0, tiled=...]
    all_to_all x1, waiting for transfers between devices: 0.01 us -> 4.48 us  [sent_to_all(): return lax.all_to_all(copies, axis, split_axis=0, concat_axis=0, tiled=True)]
    ppermute x6, waiting for transfers between devices: 14 us -> 10.1 us  [to_chip(): lax.ppermute(array, 'tp', [(i, (i + 2 * ahead) % n) for i in range(n)])]
    pallas_call x1 -> x2, Pallas kernels: 2.07 us -> 5.7 us  [the longest x1 3.65 us: local_scores(): pl.pallas_call(scores_kernel, out_shape=[jax.ShapeDtypeStruct((T, 256), f...]
    pallas_call x1, Pallas kernels: 11.4 us -> 8.02 us  [mixing(): pl.pallas_call(mixing_kernel, grid=(steps,), in_specs=[pl.BlockSpec((T, d...]
    unnamed x16 -> x14, local copies, waits for them, and re-layouts: 3.29 us -> 0.03 us
  transfers between devices with their start and end apart: 13 -> 13, of which waited for: 7 -> 7; matrix products, arithmetic and copies ran while one was open for 2% -> 0% of each run, Pallas kernels for 0% -> 1%
where the time goes in v4:
time: 321 us
  blocking collectives  188 us (59%)
  starting transfers between devices  58.2 us (18%)
  waiting for transfers between devices  37.2 us (12%)
  Pallas kernels  24.9 us (8%)
  other arithmetic  11.1 us (3%)
    all_gather x1, blocking collectives, local(): everyone = lax.all_gather(own, 'sp', axis=1, tiled=True).astype(bf16)  146 us
    all_to_all x1, blocking collectives, local(): lax.all_to_all(send, 'sp', split_axis=0, concat_axis=0, tiled=True)  42 us
    all_to_all x1, waiting for transfers between devices, local(): lax.all_to_all(chain(received), 'sp', split_axis=0, concat_axis=0, tiled=...  18.9 us
    ppermute x6, starting transfers between devices, to_chip(): lax.ppermute(array, 'tp', [(i, (i + 2 * ahead) % n) for i in range(n)])  18.9 us
    ppermute x5, starting transfers between devices, to_partner(): return lax.ppermute(array, 'tp', [(i, i ^ 1) for i in range(n)])  18.5 us
    all_to_all x1, starting transfers between devices, sent_to_all(): return lax.all_to_all(copies, axis, split_axis=0, concat_axis=0, tiled=True)  16 us
    ppermute x6, waiting for transfers between devices, to_chip(): lax.ppermute(array, 'tp', [(i, (i + 2 * ahead) % n) for i in range(n)])  10.1 us
    pallas_call x1, Pallas kernels, mixing(): pl.pallas_call(mixing_kernel, grid=(steps,), in_specs=[pl.BlockSpec((T, d...  8.02 us
  transfers between devices with their start and end apart: 13, of which 7 were waited for; matrix products, arithmetic and copies ran while one was open for 0% of the time, Pallas kernels for 1%

profile of v4, /device:TPU:33, one launch (start us, length us, event | category | flops | bytes accessed | tf_op | source)
XLA Modules:
  0.0 320.5 jit_solution(12988984645246158843)
XLA Ops:
  3.1 146.1 %all-gather.1 = f16[7,4352,128]{2,1,0:T(8,128)(2,1)} all-gather(f16[7,136,128]{2,1,0:T(8,128)(2,1)S(1)} %convert_element_type.28), channel_id=1, replica_groups=mesh['grp'=2,'sp'=32,'tp'=8] {'sp'}, dimensions={1}, use_global_device_ids=true | all-gather | bytes 8042496 | tf_op jit(solution)/shard_map/all_gather | solution.py:563
  149.2 7.7 %convert_element_type.29 = bf16[7,4352,128]{2,1,0:T(8,128)(2,1)} convert(f16[7,4352,128]{2,1,0:T(8,128)(2,1)} %all-gather.1) | non-fusion elementwise | flops 3899392 | bytes 15597568 | tf_op jit(solution)/shard_map/convert_element_type | solution.py:563
  158.7 16.0 %all-to-all-start = ((f32[8,20,128]{2,1,0:T(8,128)}), f32[8,20,128]{2,1,0:T(8,128)S(1)}, u32[]{:S(2)}, u32[]{:S(2)}) async-start(f32[8,20,128]{2,1,0:T(8,128)} %broadcast_in_dim.3), calls=%async_computation | async-start | bytes 196608 | tf_op jit(solution)/shard_map/all_to_all | solution.py:23
  175.2 4.5 %all-to-all-done.rows_ref = f32[8,20,128]{2,1,0:T(8,128)S(1)} async-done(((f32[8,20,128]{2,1,0:T(8,128)}), f32[8,20,128]{2,1,0:T(8,128)S(1)}, u32[]{:S(2)}, u32[]{:S(2)}) %all-to-all-start) | async-done | bytes 81952 | tf_op jit(solution)/shard_map/all_to_all | solution.py:23
  179.7 8.0 %mixing.1 = (bf16[256,512]{1,0:T(8,128)(2,1)S(1)}, bf16[256,512]{1,0:T(8,128)(2,1)S(1)}, bf16[32,24,128]{2,1,0:T(8,128)(2,1)S(1)}) custom-call(bf16[256,4096]{1,0:T(8,128)(2,1)S(1)} %copy-done, bf16[8,4096]{1,0:T(8,128)(2,1)S(1)} %copy-done.1, f32[264,128]{1,0:T(8,128)S(1)} %stats.1.stats_ref, f32[8,20,128]{2,1,0:T(8,128)S(1)} %all-to-all-done.rows_ref, ...), custom_call_target="tpu_custom_call" | custom-call | tf_op jit(solution)/shard_map/mixing/pallas_call | solution.py:265
  187.8 42.0 %all_to_all.15.in_ref = bf16[32,24,128]{2,1,0:T(8,128)(2,1)} all-to-all(bf16[32,24,128]{2,1,0:T(8,128)(2,1)S(1)} %get-tuple-element.20), channel_id=1, replica_groups=mesh['grp'=2,'sp'=32,'tp'=8] {'sp'}, dimensions={0} | all-to-all | bytes 393216 | tf_op jit(solution)/shard_map/all_to_all | solution.py:576
  231.7 4.8 %all-to-all-start.2 = ((bf16[32,8,128]{2,1,0:T(8,128)(2,1)}), bf16[32,8,128]{2,1,0:T(8,128)(2,1)S(1)}, u32[]{:S(2)}, u32[]{:S(2)}) async-start(bf16[32,8,128]{2,1,0:T(8,128)(2,1)} %chain.1), calls=%async_computation.2 | async-start | bytes 131072 | tf_op jit(solution)/shard_map/all_to_all | solution.py:577
  236.5 3.6 %scores.1 = (f32[256,256]{1,0:T(8,128)S(1)}, bf16[256,256]{1,0:T(8,128)(2,1)S(1)}) custom-call(bf16[256,512]{1,0:T(8,128)(2,1)S(1)} %get-tuple-element.16.qkv_ref, bf16[256,512]{1,0:T(8,128)(2,1)S(1)} %get-tuple-element.17.pairs_ref), custom_call_target="tpu_custom_call" | custom-call | flops 1342177280 | bytes 1048576 | tf_op jit(solution)/shard_map/scores/pallas_call | solution.py:352
  240.2 18.9 %all-to-all-done.2 = bf16[32,8,128]{2,1,0:T(8,128)(2,1)S(1)} async-done(((bf16[32,8,128]{2,1,0:T(8,128)(2,1)}), bf16[32,8,128]{2,1,0:T(8,128)(2,1)S(1)}, u32[]{:S(2)}, u32[]{:S(2)}) %all-to-all-start.2) | async-done | bytes 65568 | tf_op jit(solution)/shard_map/all_to_all | solution.py:577
  259.1 3.7 %sent.1 = (bf16[256,256]{1,0:T(8,128)(2,1)S(1)}, bf16[4,256,512]{2,1,0:T(8,128)(2,1)S(1)}) custom-call(s32[4]{0:T(128)S(1)} %get-tuple-element.27.order_ref, f32[256,256]{1,0:T(8,128)S(1)} %get-tuple-element.18.loc_ref, bf16[256,256]{1,0:T(8,128)(2,1)S(1)} %get-tuple-element.19.lift_ref, bf16[256,128]{1,0:T(8,128)(2,1)S(1)} %bitcast.14, ...), custom_call_target="tpu_custom_call" | custom-call | tf_op jit(solution)/shard_map/sent/pallas_call | solution.py:450
  262.8 5.7 %collective-permute-start = (bf16[4,256,512]{2,1,0:T(8,128)(2,1)S(1)}, bf16[4,256,512]{2,1,0:T(8,128)(2,1)S(1)}, u32[]{:S(2)}, u32[]{:S(2)}) collective-permute-start(bf16[4,256,512]{2,1,0:T(8,128)(2,1)S(1)} %get-tuple-element.22), channel_id=1, source_target_pairs={{0,1},{1,0},{2,3},{3,2},{4,5},{5,4},{6,7},{7,6},{8,9},{9,8},{10,11... | collective-permute-start | bytes 3145736 | tf_op jit(solution)/shard_map/ppermute | solution.py:531
  268.5 2.3 collective-permute-done.received_ref
  270.8 3.5 %kept.1 = (bf16[256,512]{1,0:T(8,128)(2,1)S(1)}, bf16[256,512]{1,0:T(8,128)(2,1)S(1)}, bf16[256,512]{1,0:T(8,128)(2,1)S(1)}, bf16[256,512]{1,0:T(8,128)(2,1)S(1)}) custom-call(s32[4]{0:T(128)S(1)} %get-tuple-element.28.order_ref, bf16[256,256]{1,0:T(8,128)(2,1)S(1)} %get-tuple-element.21.normed, bf16[4,256,512]{2,1,0:T(8,128)(2,1)S(1)} %collective-permute-done.received_ref, ...), custom_call_target="tpu_custom_call" | custom-call | tf_op jit(solution)/shard_map/kept/pallas_call | solution.py:482
  274.3 2.2 collective-permute-start.1
  276.6 3.7 %collective-permute-start.2 = (bf16[256,512]{1,0:T(8,128)(2,1)S(1)}, bf16[256,512]{1,0:T(8,128)(2,1)}, u32[]{:S(2)}, u32[]{:S(2)}) collective-permute-start(bf16[256,512]{1,0:T(8,128)(2,1)S(1)} %get-tuple-element.25), channel_id=1, source_target_pairs={{0,4},{1,5},{2,6},{3,7},{4,0},{5,1},{6,2},{7,3},{8,12},{9,13},{10,... | collective-permute-start | bytes 786440 | tf_op jit(solution)/shard_map/ppermute | solution.py:536
  280.3 2.6 collective-permute-start.3
  282.9 2.7 collective-permute-done.1
  285.6 4.6 %collective-permute-done.2 = bf16[256,512]{1,0:T(8,128)(2,1)} collective-permute-done((bf16[256,512]{1,0:T(8,128)(2,1)S(1)}, bf16[256,512]{1,0:T(8,128)(2,1)}, u32[]{:S(2)}, u32[]{:S(2)}) %collective-permute-start.2) | collective-permute-done | bytes 262176 | tf_op jit(solution)/shard_map/ppermute | solution.py:536
  290.1 2.8 collective-permute-done.3
  294.2 2.9 collective-permute-start.6
  297.1 4.4 %collective-permute-start.4 = (bf16[256,512]{1,0:T(8,128)(2,1)S(1)}, bf16[256,512]{1,0:T(8,128)(2,1)S(1)}, u32[]{:S(2)}, u32[]{:S(2)}) collective-permute-start(bf16[256,512]{1,0:T(8,128)(2,1)S(1)} %add_convert_fusion.refs_0_), channel_id=1, source_target_pairs={{0,6},{1,7},{2,0},{3,1},{4,2},{5,3},{6,4},{7,5},{8,14},{9,15},{10,... | collective-permute-start | bytes 786440 | tf_op jit(solution)/shard_map/ppermute | solution.py:536
  301.5 3.1 collective-permute-start.5
  304.6 3.0 collective-permute-start.7
  309.6 6.0 %collective-permute-start.8 = (bf16[256,512]{1,0:T(8,128)(2,1)S(1)}, bf16[256,512]{1,0:T(8,128)(2,1)S(1)}, u32[]{:S(2)}, u32[]{:S(2)}) collective-permute-start(bf16[256,512]{1,0:T(8,128)(2,1)S(1)} %collective-permute-done.4.refs_1_), channel_id=1, source_target_pairs={{0,1},{1,0},{2,3},{3,2},{4,5},{5,4},{6,7},{7,6},{8,9},{9,8},{10,11... | collective-permute-start | bytes 786440 | tf_op jit(solution)/shard_map/ppermute | solution.py:531
  (34 shorter events, 15.4 us)
Async XLA Ops:
  149.2 25.6 %copy-start = (bf16[256,4096]{1,0:T(8,128)(2,1)S(1)}, bf16[256,4096]{1,0:T(8,128)(2,1)}, u32[]{:S(2)}) copy-start(bf16[256,4096]{1,0:T(8,128)(2,1)} %latent_ref.3) | copy-start | bytes 6291460
  149.2 25.6 %copy-start.1 = (bf16[8,4096]{1,0:T(8,128)(2,1)S(1)}, bf16[8,4096]{1,0:T(8,128)(2,1)}, u32[]{:S(2)}) copy-start(bf16[8,4096]{1,0:T(8,128)(2,1)} %context_ref.3) | copy-start | bytes 196612
  149.2 30.5 %copy-start.2 = (bf16[2,64,128]{2,1,0:T(8,128)(2,1)S(1)}, bf16[2,64,128]{2,1,0:T(8,128)(2,1)}, u32[]{:S(2)}) copy-start(bf16[2,64,128]{2,1,0:T(8,128)(2,1)} %param.25) | copy-start | bytes 98308
  149.2 30.5 %copy-start.3 = (f32[4096]{0:T(1024)S(1)}, f32[4096]{0:T(1024)}, u32[]{:S(2)}) copy-start(f32[4096]{0:T(1024)} %param.20) | copy-start | bytes 49156
  149.2 30.5 %copy-start.4 = (f32[256,2]{0,1:T(2,128)S(1)}, f32[256,2]{0,1:T(2,128)}, u32[]{:S(2)}) copy-start(f32[256,2]{0,1:T(2,128)} %param.27) | copy-start | bytes 6148
  149.2 30.5 %copy-start.5 = (f32[2,128]{1,0:T(2,128)S(1)}, f32[2,128]{1,0:T(2,128)}, u32[]{:S(2)}) copy-start(f32[2,128]{1,0:T(2,128)} %bias_ref.1) | copy-start | bytes 3076
  158.7 21.0 %all-to-all-start = ((f32[8,20,128]{2,1,0:T(8,128)}), f32[8,20,128]{2,1,0:T(8,128)S(1)}, u32[]{:S(2)}, u32[]{:S(2)}) async-start(f32[8,20,128]{2,1,0:T(8,128)} %broadcast_in_dim.3), calls=%async_computation | async-start | bytes 196608 | tf_op jit(solution)/shard_map/all_to_all | solution.py:23
  179.7 79.4 %copy-start.6 = (f32[256]{0:T(256)S(1)}, f32[256]{0:T(256)}, u32[]{:S(2)}) copy-start(f32[256]{0:T(256)} %param.28) | copy-start | bytes 3076
  231.7 27.4 %all-to-all-start.2 = ((bf16[32,8,128]{2,1,0:T(8,128)(2,1)}), bf16[32,8,128]{2,1,0:T(8,128)(2,1)S(1)}, u32[]{:S(2)}, u32[]{:S(2)}) async-start(bf16[32,8,128]{2,1,0:T(8,128)(2,1)} %chain.1), calls=%async_computation.2 | async-start | bytes 131072 | tf_op jit(solution)/shard_map/all_to_all | solution.py:577
  262.8 8.0 %collective-permute-start = (bf16[4,256,512]{2,1,0:T(8,128)(2,1)S(1)}, bf16[4,256,512]{2,1,0:T(8,128)(2,1)S(1)}, u32[]{:S(2)}, u32[]{:S(2)}) collective-permute-start(bf16[4,256,512]{2,1,0:T(8,128)(2,1)S(1)} %get-tuple-element.22), channel_id=1, source_target_pairs={{0,1},{1,0},{2,3},{3,2},{4,5},{5,4},{6,7},{7,6},{8,9},{9,8},{10,11... | collective-permute-start | bytes 3145736 | tf_op jit(solution)/shard_map/ppermute | solution.py:531
  274.3 11.2 %collective-permute-start.1 = (bf16[256,512]{1,0:T(8,128)(2,1)S(1)}, bf16[256,512]{1,0:T(8,128)(2,1)S(1)}, u32[]{:S(2)}, u32[]{:S(2)}) collective-permute-start(bf16[256,512]{1,0:T(8,128)(2,1)S(1)} %get-tuple-element.24), channel_id=1, source_target_pairs={{0,2},{1,3},{2,4},{3,5},{4,6},{5,7},{6,0},{7,1},{8,10},{9,11},{10,... | collective-permute-start | bytes 786440 | tf_op jit(solution)/shard_map/ppermute | solution.py:536
  276.6 13.6 %collective-permute-start.2 = (bf16[256,512]{1,0:T(8,128)(2,1)S(1)}, bf16[256,512]{1,0:T(8,128)(2,1)}, u32[]{:S(2)}, u32[]{:S(2)}) collective-permute-start(bf16[256,512]{1,0:T(8,128)(2,1)S(1)} %get-tuple-element.25), channel_id=1, source_target_pairs={{0,4},{1,5},{2,6},{3,7},{4,0},{5,1},{6,2},{7,3},{8,12},{9,13},{10,... | collective-permute-start | bytes 786440 | tf_op jit(solution)/shard_map/ppermute | solution.py:536
  280.3 12.7 %collective-permute-start.3 = (bf16[256,512]{1,0:T(8,128)(2,1)S(1)}, bf16[256,512]{1,0:T(8,128)(2,1)}, u32[]{:S(2)}, u32[]{:S(2)}) collective-permute-start(bf16[256,512]{1,0:T(8,128)(2,1)S(1)} %get-tuple-element.26), channel_id=1, source_target_pairs={{0,6},{1,7},{2,0},{3,1},{4,2},{5,3},{6,4},{7,5},{8,14},{9,15},{10,... | collective-permute-start | bytes 786440 | tf_op jit(solution)/shard_map/ppermute | solution.py:536
  294.2 13.4 %collective-permute-start.6 = (bf16[256,512]{1,0:T(8,128)(2,1)S(1)}, bf16[256,512]{1,0:T(8,128)(2,1)S(1)}, u32[]{:S(2)}, u32[]{:S(2)}) collective-permute-start(bf16[256,512]{1,0:T(8,128)(2,1)S(1)} %add_convert_fusion.refs_0_), channel_id=1, source_target_pairs={{0,2},{1,3},{2,4},{3,5},{4,6},{5,7},{6,0},{7,1},{8,10},{9,11},{10,... | collective-permute-start | bytes 786440 | tf_op jit(solution)/shard_map/ppermute | solution.py:536
  297.1 12.5 %collective-permute-start.4 = (bf16[256,512]{1,0:T(8,128)(2,1)S(1)}, bf16[256,512]{1,0:T(8,128)(2,1)S(1)}, u32[]{:S(2)}, u32[]{:S(2)}) collective-permute-start(bf16[256,512]{1,0:T(8,128)(2,1)S(1)} %add_convert_fusion.refs_0_), channel_id=1, source_target_pairs={{0,6},{1,7},{2,0},{3,1},{4,2},{5,3},{6,4},{7,5},{8,14},{9,15},{10,... | collective-permute-start | bytes 786440 | tf_op jit(solution)/shard_map/ppermute | solution.py:536
  301.5 14.1 %collective-permute-start.5 = (bf16[256,512]{1,0:T(8,128)(2,1)S(1)}, bf16[256,512]{1,0:T(8,128)(2,1)S(1)}, u32[]{:S(2)}, u32[]{:S(2)}) collective-permute-start(bf16[256,512]{1,0:T(8,128)(2,1)S(1)} %add_convert_fusion.refs_0_), channel_id=1, source_target_pairs={{0,4},{1,5},{2,6},{3,7},{4,0},{5,1},{6,2},{7,3},{8,12},{9,13},{10,... | collective-permute-start | bytes 786440 | tf_op jit(solution)/shard_map/ppermute | solution.py:536
  304.6 12.9 %collective-permute-start.7 = (bf16[256,512]{1,0:T(8,128)(2,1)S(1)}, bf16[256,512]{1,0:T(8,128)(2,1)S(1)}, u32[]{:S(2)}, u32[]{:S(2)}) collective-permute-start(bf16[256,512]{1,0:T(8,128)(2,1)S(1)} %add_convert_fusion.refs_0_), channel_id=1, source_target_pairs={{0,1},{1,0},{2,3},{3,2},{4,5},{5,4},{6,7},{7,6},{8,9},{9,8},{10,11... | collective-permute-start | bytes 786440 | tf_op jit(solution)/shard_map/ppermute | solution.py:531
  307.6 9.9 %collective-permute-start.10 = (bf16[256,512]{1,0:T(8,128)(2,1)S(1)}, bf16[256,512]{1,0:T(8,128)(2,1)S(1)}, u32[]{:S(2)}, u32[]{:S(2)}) collective-permute-start(bf16[256,512]{1,0:T(8,128)(2,1)S(1)} %collective-permute-done.6.refs_3_), channel_id=1, source_target_pairs={{0,1},{1,0},{2,3},{3,2},{4,5},{5,4},{6,7},{7,6},{8,9},{9,8},{10,11... | collective-permute-start | bytes 786440 | tf_op jit(solution)/shard_map/ppermute | solution.py:531
  309.6 8.0 %collective-permute-start.8 = (bf16[256,512]{1,0:T(8,128)(2,1)S(1)}, bf16[256,512]{1,0:T(8,128)(2,1)S(1)}, u32[]{:S(2)}, u32[]{:S(2)}) collective-permute-start(bf16[256,512]{1,0:T(8,128)(2,1)S(1)} %collective-permute-done.4.refs_1_), channel_id=1, source_target_pairs={{0,1},{1,0},{2,3},{3,2},{4,5},{5,4},{6,7},{7,6},{8,9},{9,8},{10,11... | collective-permute-start | bytes 786440 | tf_op jit(solution)/shard_map/ppermute | solution.py:531
  315.6 3.5 %collective-permute-start.9 = (bf16[256,512]{1,0:T(8,128)(2,1)S(1)}, bf16[256,512]{1,0:T(8,128)(2,1)S(1)}, u32[]{:S(2)}, u32[]{:S(2)}) collective-permute-start(bf16[256,512]{1,0:T(8,128)(2,1)S(1)} %collective-permute-done.5.refs_2_), channel_id=1, source_target_pairs={{0,1},{1,0},{2,3},{3,2},{4,5},{5,4},{6,7},{7,6},{8,9},{9,8},{10,11... | collective-permute-start | bytes 786440 | tf_op jit(solution)/shard_map/ppermute | solution.py:531

commit v5 on v4

--- a/solution.py
+++ b/solution.py
@@ -14,7 +14,12 @@
 f16 = jnp.float16
 WEIGHT_SCALE = 2.0**17
 TERM_SCALE = 2.0**9
-TERM_ROWS = 8
+CUTS = 4
+OUT_ROWS = 64
+TERM_ROWS = 16
+HEAD_ROWS = 160
+PART = 80
+NEAR = 8
 VMEM_LIMIT = 50 * 1024 * 1024
 
 
@@ -60,21 +65,35 @@
     return both[:, 0:128] + both[:, 128:256]
 
 
+def packed_decays(latent_decay, context_decay):
+    lanes = iota(latent_decay.shape, 1)
+    lh, ll = halves(latent_decay)
+    ch, cl = halves(context_decay)
+    lat2 = jnp.where(lanes < 32, lh.astype(f32), ll.astype(f32))
+    ctx2 = jnp.where(lanes < 96, ch.astype(f32), cl.astype(f32))
+    return jnp.where(lanes < 64, lat2, ctx2)
+
+
 def prepare_kernel(
     cond_l_ref, cond_c_ref, mod_ref, q_ref, k_ref, v_ref, rank_ref, out_w_ref, out_ref
 ):
     depth = q_ref.shape[0]
 
-    def put(block, array):
-        out_ref[block, 0:depth, :] = array.astype(f32) * WEIGHT_SCALE
+    quarter = depth // CUTS
+
+    def put(base, array):
+        scaled = array.astype(f32) * WEIGHT_SCALE
+        for cut in range(CUTS):
+            out_ref[cut, base : base + quarter, :] = scaled[cut * quarter : (cut + 1) * quarter]
 
     put(0, out_w_ref[0:depth])
-    put(1, out_w_ref[depth : 2 * depth])
-    put(2, q_ref[...])
-    put(3, k_ref[...])
-    put(4, v_ref[:, 0:128])
-    put(5, v_ref[:, 128:256])
-    put(6, rank_ref[...].astype(f32).T)
+    put(quarter, out_w_ref[depth : 2 * depth])
+    heads = OUT_ROWS + TERM_ROWS
+    put(heads, q_ref[...])
+    put(heads + quarter, k_ref[...])
+    put(heads + 2 * quarter, v_ref[:, 0:128])
+    put(heads + 3 * quarter, v_ref[:, 128:256])
+    put(heads + 4 * quarter, rank_ref[...].astype(f32).T)
 
     def silu(c):
         return c / (1.0 + jnp.exp(-c))
@@ -83,8 +102,7 @@
     conds = jnp.where(
         row == 0, silu(cond_l_ref[...]), jnp.where(row == 1, silu(cond_c_ref[...]), 0.0)
     ).astype(bf16)
-    blocks = out_ref.shape[0]
-    out_ref[:, depth:, :] = jnp.zeros((blocks, TERM_ROWS, 128), f32)
+    out_ref[:, OUT_ROWS:heads, :] = jnp.zeros((CUTS, TERM_ROWS, 128), f32)
     terms = [dot(conds, mod_ref[r]) * TERM_SCALE for r in range(3)]
     vectors = [(terms[0], 0), (terms[1], 0), (terms[2], 0), (terms[0], 1), (terms[1], 1)]
     columns = mod_ref.shape[2] // 128
@@ -95,7 +113,7 @@
             high = line.astype(bf16).astype(f32)
             spot = n * columns + c
             for at_row, value in ((spot, high), (lines + spot, line - high)):
-                place = depth + at_row % TERM_ROWS
+                place = OUT_ROWS + at_row % TERM_ROWS
                 out_ref[at_row // TERM_ROWS, place : place + 1, :] = value
 
 
@@ -105,7 +123,7 @@
     ranks = jnp.swapaxes(w_rank, 1, 2).reshape(128, depth)
     return pl.pallas_call(
         prepare_kernel,
-        out_shape=jax.ShapeDtypeStruct((7, depth + TERM_ROWS, 128), f32),
+        out_shape=jax.ShapeDtypeStruct((CUTS, OUT_ROWS + TERM_ROWS + HEAD_ROWS, 128), f32),
         in_specs=[vmem] * 8,
         out_specs=vmem,
         name="prepare",
@@ -139,7 +157,7 @@
 
 def mixing_kernel(
     latent_ref, context_ref, stats_ref, rows_ref, gain_ref,
-    wq_ref, wk_ref, wv0_ref, wv1_ref, wr_ref, wd_ref, bias_ref, shift_ref,
+    upper_ref, lower_ref, wd_ref, bias_ref, shift_ref,
     qkv_ref, pairs_ref, send_ref, acc,
 ):
     step = pl.program_id(0)
@@ -163,18 +181,27 @@
             parts.append((x * scale + shift).astype(bf16))
         return jnp.concatenate(parts, axis=1)
 
-    def weight(ref):
-        depth = ref.shape[2] - TERM_ROWS
-        return jnp.concatenate([ref[0, j, 0:depth] for j in range(ref.shape[1])], axis=0)
-
-    w_qk = jnp.concatenate([weight(wq_ref), weight(wk_ref)], axis=1)
-    w_v = jnp.concatenate([weight(wv0_ref), weight(wv1_ref)], axis=1)
+    held = [
+        [
+            jnp.concatenate([upper_ref[cut, j], lower_ref[cut, j]], axis=0)
+            for cut in range(upper_ref.shape[0])
+        ]
+        for j in range(upper_ref.shape[1])
+    ]
+    quarter = HEAD_ROWS // 5
+
+    def weight(n):
+        rows = slice(n * quarter, (n + 1) * quarter)
+        return jnp.concatenate([part[rows] for cuts in held for part in cuts], axis=0)
+
+    w_qk = jnp.concatenate([weight(0), weight(1)], axis=1)
+    w_v = jnp.concatenate([weight(2), weight(3)], axis=1)
     h = modulated(latent_ref, 0, T, 0, 1)
     hc = modulated(context_ref, T, C, 3, 4)
     h = jnp.concatenate([h, hc, jnp.zeros((acc.shape[0] - T - C, h.shape[1]), bf16)], axis=0)
     acc[:, 0:256] += dot(h, w_qk)
     acc[:, 256:512] += dot(h, w_v)
-    acc[:, 512:640] += dot(h, weight(wr_ref))
+    acc[:, 512:640] += dot(h, weight(4))
 
     @pl.when(step == pl.num_programs(0) - 1)
     def _():
@@ -220,11 +247,12 @@
             return jnp.exp(dot_tn(high, ones) + dot_tn(low, ones))
 
         n = send_ref.shape[0]
+        slab = send_ref.shape[1] // 3
         st_f = head_state(k_f, v)
         st_b = head_state(k_b, v)
         half = n // 2
-        send_ref[0:half, 0:8, :] = st_f.reshape(half, 8, 128).astype(bf16)
-        send_ref[half:n, 0:8, :] = st_b.reshape(half, 8, 128).astype(bf16)
+        send_ref[0:half, 0:slab, :] = st_f.reshape(half, slab, 128).astype(bf16)
+        send_ref[half:n, 0:slab, :] = st_b.reshape(half, slab, 128).astype(bf16)
 
         crow = iota((C, 128), 0)
         live = crow < 8
@@ -238,24 +266,19 @@
         sc = iota((C, C), 1)
         kc_f = (kc * jnp.exp(summed(sc > rc, jnp.concatenate([cf_high, cf_low], axis=1)))).astype(bf16)
         kc_b = (kc * jnp.exp(summed(sc < rc, jnp.concatenate([cb_high, cb_low], axis=1)))).astype(bf16)
-        send_ref[0:half, 8:16, :] = head_state(kc_f, vc).reshape(half, 8, 128).astype(bf16)
-        send_ref[half:n, 8:16, :] = head_state(kc_b, vc).reshape(half, 8, 128).astype(bf16)
-
-        lanes = iota((128, 128), 1)
+        send_ref[0:half, slab : 2 * slab, :] = head_state(kc_f, vc).reshape(half, slab, 128).astype(bf16)
+        send_ref[half:n, slab : 2 * slab, :] = head_state(kc_b, vc).reshape(half, slab, 128).astype(bf16)
 
         def packed(latent_total, context_total):
-            lh, ll = halves(latent_total)
-            ch, cl = halves(context_total)
-            lat2 = jnp.where(lanes < 32, lh.astype(f32), ll.astype(f32))
-            ctx2 = jnp.where(lanes < 96, ch.astype(f32), cl.astype(f32))
-            return jnp.where(lanes < 64, lat2, ctx2).reshape(half, 8, 128).astype(bf16)
-
-        send_ref[0:half, 16:24, :] = packed(total(f_high, f_low), total(cf_high, cf_low))
-        send_ref[half:n, 16:24, :] = packed(total(b_high, b_low), total(cb_high, cb_low))
+            both = packed_decays(latent_total, context_total)
+            return both.reshape(half, slab, 128).astype(bf16)
+
+        send_ref[0:half, 2 * slab :, :] = packed(total(f_high, f_low), total(cf_high, cf_low))
+        send_ref[half:n, 2 * slab :, :] = packed(total(b_high, b_low), total(cb_high, cb_low))
 
 
 def mixing(
-    latent, context, scales, rows, gain, gathered, w_decay, decay_bias, decay_shift, members
+    latent, context, scales, rows, gain, gathered, w_decay, decay_bias, decay_shift
 ):
     T, width = latent.shape
     C = context.shape[0]
@@ -273,26 +296,26 @@
             pl.BlockSpec((1, 1, depth), lambda i: (i, 0, 0)),
             *[
                 pl.BlockSpec(
-                    (1, gathered.shape[1] // steps, gathered.shape[2], 128),
-                    lambda i, b=b: (b, i, 0, 0),
+                    (CUTS, gathered.shape[1] // steps, PART, 128),
+                    lambda i, b=b: (0, i, b, 0),
                 )
-                for b in range(2, 7)
+                for b in (1, 2)
             ],
             whole(128, 128),
             whole(2, 128),
             whole(2, T),
         ],
-        out_specs=[whole(T, 512), whole(T, 512), whole(members, 24, 128)],
+        out_specs=[whole(T, 512), whole(T, 512), whole(NEAR, 3 * 256 // NEAR, 128)],
         out_shape=[
             jax.ShapeDtypeStruct((T, 512), bf16),
             jax.ShapeDtypeStruct((T, 512), bf16),
-            jax.ShapeDtypeStruct((members, 24, 128), bf16),
+            jax.ShapeDtypeStruct((NEAR, 3 * 256 // NEAR, 128), bf16),
         ],
         scratch_shapes=[pltpu.VMEM((T + 16, 640), f32)],
         compiler_params=pltpu.CompilerParams(vmem_limit_bytes=VMEM_LIMIT),
         name="mixing",
     )(
-        latent, context, scales, rows, gain.reshape(steps, 1, depth), *[gathered] * 5,
+        latent, context, scales, rows, gain.reshape(steps, 1, depth), gathered, gathered,
         w_decay.reshape(128, 128), decay_bias, decay_shift.T,
     )
 
@@ -365,37 +388,98 @@
     )(qkv, pairs)
 
 
-def chain_kernel(in_ref, out_ref):
+def slab_parts(ref, at, slab):
+    rows = ref[at, 2 * slab : 3 * slab, :].astype(f32)
+
+    def decay(lane):
+        both = rows[:, lane : lane + 1] + rows[:, lane + 32 : lane + 33]
+        return jnp.broadcast_to(both, (slab, 128))
+
+    return (
+        ref[at, 0:slab, :].astype(f32),
+        ref[at, slab : 2 * slab, :].astype(f32),
+        decay(0),
+        decay(64),
+    )
+
+
+def ordered(backward, i, count):
+    return jnp.where(backward, count - 1 - i, i)
+
+
+def near_kernel(in_ref, state_ref, decay_ref, total_ref):
     n = in_ref.shape[0]
-    backward = lax.axis_index("sp") >= n // 2
-
-    def place(i):
-        return jnp.where(backward, n - 1 - i, i)
-
-    def decay(at, lane):
-        rows = in_ref[at, 16:24, :].astype(f32)
-        return rows[:, lane : lane + 1] + rows[:, lane + 32 : lane + 33]
-
-    state = jnp.zeros((8, 128), f32)
+    slab = in_ref.shape[1] // 3
+    backward = lax.rem(lax.axis_index("sp"), n) >= n // 2
+    lat = jnp.zeros((slab, 128), f32)
+    ctx = jnp.zeros((slab, 128), f32)
+    lat_decay = jnp.ones((slab, 128), f32)
+    ctx_decay = jnp.ones((slab, 128), f32)
     for i in range(n):
-        at = place(i)
-        state = decay(at, 64) * state + in_ref[at, 8:16, :].astype(f32)
-    for i in range(n):
-        at = place(i)
-        out_ref[at] = state.astype(bf16)
-        if i + 1 < n:
-            state = decay(at, 0) * state + in_ref[at, 0:8, :].astype(f32)
-
-
-def chain(received):
-    n = received.shape[0]
-    return pl.pallas_call(
-        chain_kernel,
-        out_shape=jax.ShapeDtypeStruct((n, 8, 128), bf16),
-        in_specs=[pl.BlockSpec(memory_space=pltpu.VMEM)],
-        out_specs=pl.BlockSpec(memory_space=pltpu.VMEM),
-        name="chain",
+        at = ordered(backward, i, n)
+        state_ref[at] = lat
+        decay_ref[at] = lat_decay
+        own_lat, own_ctx, dl, dc = slab_parts(in_ref, at, slab)
+        lat = dl * lat + own_lat
+        ctx = dc * ctx + own_ctx
+        lat_decay = dl * lat_decay
+        ctx_decay = dc * ctx_decay
+    total_ref[0:slab, :] = lat.astype(bf16)
+    total_ref[slab : 2 * slab, :] = ctx.astype(bf16)
+    total_ref[2 * slab :, :] = packed_decays(lat_decay, ctx_decay).astype(bf16)
+
+
+def far_kernel(totals_ref, state_ref, decay_ref, out_ref):
+    groups = totals_ref.shape[0]
+    n = state_ref.shape[0]
+    slab = state_ref.shape[1]
+    place = lax.axis_index("sp")
+    backward = lax.rem(place, n) >= n // 2
+    group = place // n
+    mine = ordered(backward, group, groups)
+    start = jnp.zeros((slab, 128), f32)
+    for i in range(groups):
+        _, ctx, _, dc = slab_parts(totals_ref, ordered(backward, i, groups), slab)
+        start = dc * start + ctx
+    for i in range(groups - 1):
+        lat, _, dl, _ = slab_parts(totals_ref, ordered(backward, i, groups), slab)
+        start = jnp.where(i < mine, dl * start + lat, start)
+    for m in range(n):
+        out_ref[m] = (decay_ref[m] * start + state_ref[m]).astype(bf16)
+
+
+def states_before(sent):
+    n, rows, _ = sent.shape
+    slab = rows // 3
+    members = lax.axis_size("sp")
+    near = [list(range(i, i + n)) for i in range(0, members, n)]
+    far = [list(range(i, members, n)) for i in range(n)]
+    vmem = pl.BlockSpec(memory_space=pltpu.VMEM)
+    received = lax.all_to_all(
+        sent, "sp", split_axis=0, concat_axis=0, tiled=True, axis_index_groups=near
+    )
+    state, decay, total = pl.pallas_call(
+        near_kernel,
+        out_shape=[
+            jax.ShapeDtypeStruct((n, slab, 128), f32),
+            jax.ShapeDtypeStruct((n, slab, 128), f32),
+            jax.ShapeDtypeStruct((rows, 128), bf16),
+        ],
+        in_specs=[vmem],
+        out_specs=[vmem] * 3,
+        name="near",
     )(received)
+    totals = lax.all_gather(total, "sp", axis_index_groups=far)
+    entries = pl.pallas_call(
+        far_kernel,
+        out_shape=jax.ShapeDtypeStruct((n, slab, 128), bf16),
+        in_specs=[vmem] * 3,
+        out_specs=vmem,
+        name="far",
+    )(totals, state, decay)
+    return lax.all_to_all(
+        entries, "sp", split_axis=0, concat_axis=0, tiled=True, axis_index_groups=near
+    )
 
 
 def normalized_output(loc_ref, lift_ref, entry_ref, gain_ref, normed):
@@ -414,7 +498,16 @@
 
 
 def column(normed, w, j):
-    return (dot(normed[:, 0:128], w[0, j, 0:128]) + dot(normed[:, 128:256], w[1, j, 0:128])) * (1.0 / WEIGHT_SCALE)
+    quarter = OUT_ROWS // 2
+    halves_of = [
+        jnp.concatenate(
+            [w[cut, j, n * quarter : (n + 1) * quarter] for cut in range(CUTS)], axis=0
+        )
+        for n in range(2)
+    ]
+    return (dot(normed[:, 0:128], halves_of[0]) + dot(normed[:, 128:256], halves_of[1])) * (
+        1.0 / WEIGHT_SCALE
+    )
 
 
 def sent_kernel(order_ref, loc_ref, lift_ref, entry_ref, gain_ref, w_ref, normed, out_ref):
@@ -458,7 +551,7 @@
                 constant_block(256, 128),
                 constant_block(1, 256),
                 pl.BlockSpec(
-                    (2, width // 128, gathered.shape[2], 128),
+                    (CUTS, width // 128, PART, 128),
                     lambda i, order: (0, order[i], 0, 0),
                 ),
             ],
@@ -488,7 +581,7 @@
                 constant_block(T, 256),
                 pl.BlockSpec((1, T, width), lambda i, order: (i, 0, 0)),
                 pl.BlockSpec(
-                    (2, width // 128, gathered.shape[2], 128),
+                    (CUTS, width // 128, PART, 128),
                     lambda i, order: (0, order[i], 0, 0),
                 ),
             ],
@@ -561,26 +654,25 @@
         cond_latent, cond_context, mod_weight, w_query, w_key, w_value, w_rank, w_out
     ).astype(f16)
     everyone = lax.all_gather(own, "sp", axis=1, tiled=True).astype(bf16)
-    gathered = everyone.reshape(own.shape[0], members, depth + TERM_ROWS, 128)
+    gathered = everyone.reshape(CUTS, members, own.shape[1], 128)
     lines = 5 * mod_weight.shape[2] // 128
-    sums = gathered[:, :, depth:].astype(f32).sum(axis=1).reshape(-1, 128)
+    sums = gathered[:, :, OUT_ROWS : OUT_ROWS + TERM_ROWS].astype(f32).sum(axis=1).reshape(-1, 128)
     summed_terms = (sums[:lines] + sums[lines : 2 * lines]) * (1.0 / TERM_SCALE)
     rows = sent_to_all(summed_terms, "tp")
     gate = summed_terms.reshape(5, -1)[2]
 
     qkv, pairs, send = mixing(
         latent, context, stats(latent, context), rows, norm_gain, gathered, w_decay, decay_bias,
-        decay_shift, members,
+        decay_shift,
     )
     loc, lift = local_scores(qkv, pairs)
-    received = lax.all_to_all(send, "sp", split_axis=0, concat_axis=0, tiled=True)
-    entries = lax.all_to_all(chain(received), "sp", split_axis=0, concat_axis=0, tiled=True)
+    entries = states_before(send)
     columns = width // pieces
     chips = pieces // 2
     place = lax.axis_index("tp")
     order = 2 * ((place // 2 + jnp.arange(chips)) % chips) + place % 2
     normed, sent = sent_parts(
-        order ^ 1, loc, lift, entries.reshape(members * 8, 128), out_gain.reshape(1, 256),
+        order ^ 1, loc, lift, entries.reshape(256, 128), out_gain.reshape(1, 256),
         gathered, columns,
     )
     sums = kept_parts(order, normed, to_partner(sent), gathered, columns)

time: 321 us -> 315 us (0.981)
  waiting for transfers between devices: 37.2 us -> 24.3 us
  starting transfers between devices: 58.2 us -> 62.6 us
    all_to_all x1, blocking collectives: 42 us -> 16.5 us  [states_before(): lax.all_to_all(sent, 'sp', split_axis=0, concat_axis=0, tiled=True, axis_...]
    all_gather x0 -> x1, blocking collectives: none -> 25.5 us  [states_before(): totals = lax.all_gather(total, 'sp', axis_index_groups=far)]
    all_to_all x1, waiting for transfers between devices: 18.9 us -> 6.08 us  [states_before(): lax.all_to_all(entries, 'sp', split_axis=0, concat_axis=0, tiled=True, ax...]
where the time goes in v5:
time: 315 us; the launch traced here: 314 us
  blocking collectives  189 us (60%)
  starting transfers between devices  62.6 us (20%)
  Pallas kernels  26.5 us (8%)
  waiting for transfers between devices  24.3 us (8%)
  other arithmetic  11.2 us (4%)
    all_gather x1, blocking collectives, local(): everyone = lax.all_gather(own, 'sp', axis=1, tiled=True).astype(bf16)  147 us
    all_gather x1, blocking collectives, states_before(): totals = lax.all_gather(total, 'sp', axis_index_groups=far)  25.5 us
    ppermute x5, starting transfers between devices, to_partner(): return lax.ppermute(array, 'tp', [(i, i ^ 1) for i in range(n)])  20.2 us
    ppermute x6, starting transfers between devices, to_chip(): lax.ppermute(array, 'tp', [(i, (i + 2 * ahead) % n) for i in range(n)])  19 us
    all_to_all x1, blocking collectives, states_before(): lax.all_to_all(sent, 'sp', split_axis=0, concat_axis=0, tiled=True, axis_...  16.5 us
    all_to_all x1, starting transfers between devices, sent_to_all(): return lax.all_to_all(copies, axis, split_axis=0, concat_axis=0, tiled=True)  16 us
    ppermute x6, waiting for transfers between devices, to_chip(): lax.ppermute(array, 'tp', [(i, (i + 2 * ahead) % n) for i in range(n)])  9.96 us
    convert_element_type x1, other arithmetic, local(): everyone = lax.all_gather(own, 'sp', axis=1, tiled=True).astype(bf16)  7.79 us
  transfers between devices with their start and end apart: 13, of which 7 were waited for; matrix products, arithmetic and copies ran while one was open for 0% of the time, Pallas kernels for 1%

profile of v5, /device:TPU:33, one launch (start us, length us, event | category | flops | bytes accessed | tf_op | source)
XLA Modules:
  0.0 314.1 jit_solution(6630486227729796800)
XLA Ops:
  3.1 146.6 %all-gather.2 = f16[4,7680,128]{2,1,0:T(8,128)(2,1)} all-gather(f16[4,240,128]{2,1,0:T(8,128)(2,1)S(1)} %convert_element_type.28), channel_id=1, replica_groups=mesh['grp'=2,'sp'=32,'tp'=8] {'sp'}, dimensions={1}, use_global_device_ids=true | all-gather | bytes 8110080 | tf_op jit(solution)/shard_map/all_gather | solution.py:656
  149.8 7.8 %convert_element_type.29 = bf16[4,7680,128]{2,1,0:T(8,128)(2,1)} convert(f16[4,7680,128]{2,1,0:T(8,128)(2,1)} %all-gather.2) | non-fusion elementwise | flops 3932160 | bytes 15728640 | tf_op jit(solution)/shard_map/convert_element_type | solution.py:656
  159.3 16.0 %all-to-all-start = ((f32[8,20,128]{2,1,0:T(8,128)}), f32[8,20,128]{2,1,0:T(8,128)S(1)}, u32[]{:S(2)}, u32[]{:S(2)}) async-start(f32[8,20,128]{2,1,0:T(8,128)} %broadcast_in_dim.3), calls=%async_computation | async-start | bytes 196608 | tf_op jit(solution)/shard_map/all_to_all | solution.py:28
  175.9 4.5 %all-to-all-done.rows_ref = f32[8,20,128]{2,1,0:T(8,128)S(1)} async-done(((f32[8,20,128]{2,1,0:T(8,128)}), f32[8,20,128]{2,1,0:T(8,128)S(1)}, u32[]{:S(2)}, u32[]{:S(2)}) %all-to-all-start) | async-done | bytes 81952 | tf_op jit(solution)/shard_map/all_to_all | solution.py:28
  180.4 7.8 %mixing.1 = (bf16[256,512]{1,0:T(8,128)(2,1)S(1)}, bf16[256,512]{1,0:T(8,128)(2,1)S(1)}, bf16[8,96,128]{2,1,0:T(8,128)(2,1)S(1)}) custom-call(bf16[256,4096]{1,0:T(8,128)(2,1)S(1)} %copy-done, bf16[8,4096]{1,0:T(8,128)(2,1)S(1)} %copy-done.1, f32[264,128]{1,0:T(8,128)S(1)} %stats.1.stats_ref, f32[8,20,128]{2,1,0:T(8,128)S(1)} %all-to-all-done.rows_ref, ...), custom_call_target="tpu_custom_call" | custom-call | tf_op jit(solution)/shard_map/mixing/pallas_call | solution.py:288
  188.2 16.5 %all_to_all.15.in_ref = bf16[8,96,128]{2,1,0:T(8,128)(2,1)} all-to-all(bf16[8,96,128]{2,1,0:T(8,128)(2,1)S(1)} %get-tuple-element.23), channel_id=1, replica_groups={{0,8,16,24,32,40,48,56},{64,72,80,88,96,104,112,120},{128,136,144,152,1..., dimensions={0} | all-to-all | bytes 393216 | tf_op jit(solution)/shard_map/all_to_all | solution.py:458
  206.4 25.5 %all-gather = bf16[384,128]{1,0:T(8,128)(2,1)} all-gather(bf16[96,128]{1,0:T(8,128)(2,1)} %get-tuple-element.24), channel_id=2, replica_groups={{0,64,128,192},{8,72,136,200},{16,80,144,208},{24,88,152,216},{32,96,16..., dimensions={0}, use_global_device_ids=true | all-gather | bytes 122880 | tf_op jit(solution)/shard_map/all_gather | solution.py:472
  233.8 7.4 %all-to-all-start.2 = ((bf16[8,32,128]{2,1,0:T(8,128)(2,1)}), bf16[8,32,128]{2,1,0:T(8,128)(2,1)S(1)}, u32[]{:S(2)}, u32[]{:S(2)}) async-start(bf16[8,32,128]{2,1,0:T(8,128)(2,1)} %far.1), calls=%async_computation.2 | async-start | bytes 131072 | tf_op jit(solution)/shard_map/all_to_all | solution.py:480
  241.2 3.6 %scores.1 = (f32[256,256]{1,0:T(8,128)S(1)}, bf16[256,256]{1,0:T(8,128)(2,1)S(1)}) custom-call(bf16[256,512]{1,0:T(8,128)(2,1)S(1)} %get-tuple-element.19.qkv_ref, bf16[256,512]{1,0:T(8,128)(2,1)S(1)} %get-tuple-element.20.pairs_ref), custom_call_target="tpu_custom_call" | custom-call | flops 1342177280 | bytes 1048576 | tf_op jit(solution)/shard_map/scores/pallas_call | solution.py:375
  244.8 6.1 %all-to-all-done.2 = bf16[8,32,128]{2,1,0:T(8,128)(2,1)S(1)} async-done(((bf16[8,32,128]{2,1,0:T(8,128)(2,1)}), bf16[8,32,128]{2,1,0:T(8,128)(2,1)S(1)}, u32[]{:S(2)}, u32[]{:S(2)}) %all-to-all-start.2) | async-done | bytes 65568 | tf_op jit(solution)/shard_map/all_to_all | solution.py:480
  250.9 3.8 %sent.1 = (bf16[256,256]{1,0:T(8,128)(2,1)S(1)}, bf16[4,256,512]{2,1,0:T(8,128)(2,1)S(1)}) custom-call(s32[4]{0:T(128)S(1)} %get-tuple-element.33.order_ref, f32[256,256]{1,0:T(8,128)S(1)} %get-tuple-element.21.loc_ref, bf16[256,256]{1,0:T(8,128)(2,1)S(1)} %get-tuple-element.22.lift_ref, bf16[256,128]{1,0:T(8,128)(2,1)S(1)} %bitcast.15, ...), custom_call_target="tpu_custom_call" | custom-call | tf_op jit(solution)/shard_map/sent/pallas_call | solution.py:543
  254.7 7.3 %collective-permute-start = (bf16[4,256,512]{2,1,0:T(8,128)(2,1)S(1)}, bf16[4,256,512]{2,1,0:T(8,128)(2,1)S(1)}, u32[]{:S(2)}, u32[]{:S(2)}) collective-permute-start(bf16[4,256,512]{2,1,0:T(8,128)(2,1)S(1)} %get-tuple-element.28), channel_id=1, source_target_pairs={{0,1},{1,0},{2,3},{3,2},{4,5},{5,4},{6,7},{7,6},{8,9},{9,8},{10,11... | collective-permute-start | bytes 3145736 | tf_op jit(solution)/shard_map/ppermute | solution.py:624
  262.0 2.3 collective-permute-done.received_ref
  264.3 3.6 %kept.1 = (bf16[256,512]{1,0:T(8,128)(2,1)S(1)}, bf16[256,512]{1,0:T(8,128)(2,1)S(1)}, bf16[256,512]{1,0:T(8,128)(2,1)S(1)}, bf16[256,512]{1,0:T(8,128)(2,1)S(1)}) custom-call(s32[4]{0:T(128)S(1)} %get-tuple-element.34.order_ref, bf16[256,256]{1,0:T(8,128)(2,1)S(1)} %get-tuple-element.27.normed, bf16[4,256,512]{2,1,0:T(8,128)(2,1)S(1)} %collective-permute-done.received_ref, ...), custom_call_target="tpu_custom_call" | custom-call | tf_op jit(solution)/shard_map/kept/pallas_call | solution.py:575
  270.1 3.7 %collective-permute-start.2 = (bf16[256,512]{1,0:T(8,128)(2,1)S(1)}, bf16[256,512]{1,0:T(8,128)(2,1)}, u32[]{:S(2)}, u32[]{:S(2)}) collective-permute-start(bf16[256,512]{1,0:T(8,128)(2,1)S(1)} %get-tuple-element.31), channel_id=1, source_target_pairs={{0,4},{1,5},{2,6},{3,7},{4,0},{5,1},{6,2},{7,3},{8,12},{9,13},{10,... | collective-permute-start | bytes 786440 | tf_op jit(solution)/shard_map/ppermute | solution.py:629
  273.8 2.7 collective-permute-start.3
  276.6 2.6 collective-permute-done.1
  279.1 4.5 %collective-permute-done.2 = bf16[256,512]{1,0:T(8,128)(2,1)} collective-permute-done((bf16[256,512]{1,0:T(8,128)(2,1)S(1)}, bf16[256,512]{1,0:T(8,128)(2,1)}, u32[]{:S(2)}, u32[]{:S(2)}) %collective-permute-start.2) | collective-permute-done | bytes 262176 | tf_op jit(solution)/shard_map/ppermute | solution.py:629
  283.7 2.9 collective-permute-done.3
  287.8 3.1 collective-permute-start.6
  290.8 4.2 %collective-permute-start.4 = (bf16[256,512]{1,0:T(8,128)(2,1)S(1)}, bf16[256,512]{1,0:T(8,128)(2,1)S(1)}, u32[]{:S(2)}, u32[]{:S(2)}) collective-permute-start(bf16[256,512]{1,0:T(8,128)(2,1)S(1)} %add_convert_fusion.refs_0_), channel_id=1, source_target_pairs={{0,6},{1,7},{2,0},{3,1},{4,2},{5,3},{6,4},{7,5},{8,14},{9,15},{10,... | collective-permute-start | bytes 786440 | tf_op jit(solution)/shard_map/ppermute | solution.py:629
  295.0 3.1 collective-permute-start.5
  298.2 3.0 collective-permute-start.7
  303.1 6.0 %collective-permute-start.8 = (bf16[256,512]{1,0:T(8,128)(2,1)S(1)}, bf16[256,512]{1,0:T(8,128)(2,1)S(1)}, u32[]{:S(2)}, u32[]{:S(2)}) collective-permute-start(bf16[256,512]{1,0:T(8,128)(2,1)S(1)} %collective-permute-done.4.refs_1_), channel_id=1, source_target_pairs={{0,1},{1,0},{2,3},{3,2},{4,5},{5,4},{6,7},{7,6},{8,9},{9,8},{10,11... | collective-permute-start | bytes 786440 | tf_op jit(solution)/shard_map/ppermute | solution.py:624
  (36 shorter events, 19.4 us)
Async XLA Ops:
  149.7 25.6 %copy-start = (bf16[256,4096]{1,0:T(8,128)(2,1)S(1)}, bf16[256,4096]{1,0:T(8,128)(2,1)}, u32[]{:S(2)}) copy-start(bf16[256,4096]{1,0:T(8,128)(2,1)} %latent_ref.3) | copy-start | bytes 6291460
  149.7 25.6 %copy-start.1 = (bf16[8,4096]{1,0:T(8,128)(2,1)S(1)}, bf16[8,4096]{1,0:T(8,128)(2,1)}, u32[]{:S(2)}) copy-start(bf16[8,4096]{1,0:T(8,128)(2,1)} %context_ref.3) | copy-start | bytes 196612
  149.7 30.6 %copy-start.2 = (bf16[2,64,128]{2,1,0:T(8,128)(2,1)S(1)}, bf16[2,64,128]{2,1,0:T(8,128)(2,1)}, u32[]{:S(2)}) copy-start(bf16[2,64,128]{2,1,0:T(8,128)(2,1)} %param.25) | copy-start | bytes 98308
  149.7 30.6 %copy-start.3 = (f32[4096]{0:T(1024)S(1)}, f32[4096]{0:T(1024)}, u32[]{:S(2)}) copy-start(f32[4096]{0:T(1024)} %param.20) | copy-start | bytes 49156
  149.7 30.6 %copy-start.4 = (f32[256,2]{0,1:T(2,128)S(1)}, f32[256,2]{0,1:T(2,128)}, u32[]{:S(2)}) copy-start(f32[256,2]{0,1:T(2,128)} %param.27) | copy-start | bytes 6148
  149.7 30.6 %copy-start.5 = (f32[2,128]{1,0:T(2,128)S(1)}, f32[2,128]{1,0:T(2,128)}, u32[]{:S(2)}) copy-start(f32[2,128]{1,0:T(2,128)} %bias_ref.1) | copy-start | bytes 3076
  159.3 21.0 %all-to-all-start = ((f32[8,20,128]{2,1,0:T(8,128)}), f32[8,20,128]{2,1,0:T(8,128)S(1)}, u32[]{:S(2)}, u32[]{:S(2)}) async-start(f32[8,20,128]{2,1,0:T(8,128)} %broadcast_in_dim.3), calls=%async_computation | async-start | bytes 196608 | tf_op jit(solution)/shard_map/all_to_all | solution.py:28
  180.4 70.6 %copy-start.6 = (f32[256]{0:T(256)S(1)}, f32[256]{0:T(256)}, u32[]{:S(2)}) copy-start(f32[256]{0:T(256)} %param.28) | copy-start | bytes 3076
  233.8 17.2 %all-to-all-start.2 = ((bf16[8,32,128]{2,1,0:T(8,128)(2,1)}), bf16[8,32,128]{2,1,0:T(8,128)(2,1)S(1)}, u32[]{:S(2)}, u32[]{:S(2)}) async-start(bf16[8,32,128]{2,1,0:T(8,128)(2,1)} %far.1), calls=%async_computation.2 | async-start | bytes 131072 | tf_op jit(solution)/shard_map/all_to_all | solution.py:480
  254.7 9.6 %collective-permute-start = (bf16[4,256,512]{2,1,0:T(8,128)(2,1)S(1)}, bf16[4,256,512]{2,1,0:T(8,128)(2,1)S(1)}, u32[]{:S(2)}, u32[]{:S(2)}) collective-permute-start(bf16[4,256,512]{2,1,0:T(8,128)(2,1)S(1)} %get-tuple-element.28), channel_id=1, source_target_pairs={{0,1},{1,0},{2,3},{3,2},{4,5},{5,4},{6,7},{7,6},{8,9},{9,8},{10,11... | collective-permute-start | bytes 3145736 | tf_op jit(solution)/shard_map/ppermute | solution.py:624
  267.9 11.2 %collective-permute-start.1 = (bf16[256,512]{1,0:T(8,128)(2,1)S(1)}, bf16[256,512]{1,0:T(8,128)(2,1)S(1)}, u32[]{:S(2)}, u32[]{:S(2)}) collective-permute-start(bf16[256,512]{1,0:T(8,128)(2,1)S(1)} %get-tuple-element.30), channel_id=1, source_target_pairs={{0,2},{1,3},{2,4},{3,5},{4,6},{5,7},{6,0},{7,1},{8,10},{9,11},{10,... | collective-permute-start | bytes 786440 | tf_op jit(solution)/shard_map/ppermute | solution.py:629
  270.1 13.5 %collective-permute-start.2 = (bf16[256,512]{1,0:T(8,128)(2,1)S(1)}, bf16[256,512]{1,0:T(8,128)(2,1)}, u32[]{:S(2)}, u32[]{:S(2)}) collective-permute-start(bf16[256,512]{1,0:T(8,128)(2,1)S(1)} %get-tuple-element.31), channel_id=1, source_target_pairs={{0,4},{1,5},{2,6},{3,7},{4,0},{5,1},{6,2},{7,3},{8,12},{9,13},{10,... | collective-permute-start | bytes 786440 | tf_op jit(solution)/shard_map/ppermute | solution.py:629
  273.8 12.7 %collective-permute-start.3 = (bf16[256,512]{1,0:T(8,128)(2,1)S(1)}, bf16[256,512]{1,0:T(8,128)(2,1)}, u32[]{:S(2)}, u32[]{:S(2)}) collective-permute-start(bf16[256,512]{1,0:T(8,128)(2,1)S(1)} %get-tuple-element.32), channel_id=1, source_target_pairs={{0,6},{1,7},{2,0},{3,1},{4,2},{5,3},{6,4},{7,5},{8,14},{9,15},{10,... | collective-permute-start | bytes 786440 | tf_op jit(solution)/shard_map/ppermute | solution.py:629
  287.8 13.4 %collective-permute-start.6 = (bf16[256,512]{1,0:T(8,128)(2,1)S(1)}, bf16[256,512]{1,0:T(8,128)(2,1)S(1)}, u32[]{:S(2)}, u32[]{:S(2)}) collective-permute-start(bf16[256,512]{1,0:T(8,128)(2,1)S(1)} %add_convert_fusion.refs_0_), channel_id=1, source_target_pairs={{0,2},{1,3},{2,4},{3,5},{4,6},{5,7},{6,0},{7,1},{8,10},{9,11},{10,... | collective-permute-start | bytes 786440 | tf_op jit(solution)/shard_map/ppermute | solution.py:629
  290.8 12.3 %collective-permute-start.4 = (bf16[256,512]{1,0:T(8,128)(2,1)S(1)}, bf16[256,512]{1,0:T(8,128)(2,1)S(1)}, u32[]{:S(2)}, u32[]{:S(2)}) collective-permute-start(bf16[256,512]{1,0:T(8,128)(2,1)S(1)} %add_convert_fusion.refs_0_), channel_id=1, source_target_pairs={{0,6},{1,7},{2,0},{3,1},{4,2},{5,3},{6,4},{7,5},{8,14},{9,15},{10,... | collective-permute-start | bytes 786440 | tf_op jit(solution)/shard_map/ppermute | solution.py:629
  295.0 14.1 %collective-permute-start.5 = (bf16[256,512]{1,0:T(8,128)(2,1)S(1)}, bf16[256,512]{1,0:T(8,128)(2,1)S(1)}, u32[]{:S(2)}, u32[]{:S(2)}) collective-permute-start(bf16[256,512]{1,0:T(8,128)(2,1)S(1)} %add_convert_fusion.refs_0_), channel_id=1, source_target_pairs={{0,4},{1,5},{2,6},{3,7},{4,0},{5,1},{6,2},{7,3},{8,12},{9,13},{10,... | collective-permute-start | bytes 786440 | tf_op jit(solution)/shard_map/ppermute | solution.py:629
  298.2 12.9 %collective-permute-start.7 = (bf16[256,512]{1,0:T(8,128)(2,1)S(1)}, bf16[256,512]{1,0:T(8,128)(2,1)S(1)}, u32[]{:S(2)}, u32[]{:S(2)}) collective-permute-start(bf16[256,512]{1,0:T(8,128)(2,1)S(1)} %add_convert_fusion.refs_0_), channel_id=1, source_target_pairs={{0,1},{1,0},{2,3},{3,2},{4,5},{5,4},{6,7},{7,6},{8,9},{9,8},{10,11... | collective-permute-start | bytes 786440 | tf_op jit(solution)/shard_map/ppermute | solution.py:624
  301.2 9.9 %collective-permute-start.10 = (bf16[256,512]{1,0:T(8,128)(2,1)S(1)}, bf16[256,512]{1,0:T(8,128)(2,1)S(1)}, u32[]{:S(2)}, u32[]{:S(2)}) collective-permute-start(bf16[256,512]{1,0:T(8,128)(2,1)S(1)} %collective-permute-done.6.refs_3_), channel_id=1, source_target_pairs={{0,1},{1,0},{2,3},{3,2},{4,5},{5,4},{6,7},{7,6},{8,9},{9,8},{10,11... | collective-permute-start | bytes 786440 | tf_op jit(solution)/shard_map/ppermute | solution.py:624
  303.1 8.0 %collective-permute-start.8 = (bf16[256,512]{1,0:T(8,128)(2,1)S(1)}, bf16[256,512]{1,0:T(8,128)(2,1)S(1)}, u32[]{:S(2)}, u32[]{:S(2)}) collective-permute-start(bf16[256,512]{1,0:T(8,128)(2,1)S(1)} %collective-permute-done.4.refs_1_), channel_id=1, source_target_pairs={{0,1},{1,0},{2,3},{3,2},{4,5},{5,4},{6,7},{7,6},{8,9},{9,8},{10,11... | collective-permute-start | bytes 786440 | tf_op jit(solution)/shard_map/ppermute | solution.py:624
  309.1 3.5 %collective-permute-start.9 = (bf16[256,512]{1,0:T(8,128)(2,1)S(1)}, bf16[256,512]{1,0:T(8,128)(2,1)S(1)}, u32[]{:S(2)}, u32[]{:S(2)}) collective-permute-start(bf16[256,512]{1,0:T(8,128)(2,1)S(1)} %collective-permute-done.5.refs_2_), channel_id=1, source_target_pairs={{0,1},{1,0},{2,3},{3,2},{4,5},{5,4},{6,7},{7,6},{8,9},{9,8},{10,11... | collective-permute-start | bytes 786440 | tf_op jit(solution)/shard_map/ppermute | solution.py:624

commit v6 on v5

--- a/solution.py
+++ b/solution.py
@@ -18,9 +18,9 @@
 OUT_ROWS = 64
 TERM_ROWS = 16
 HEAD_ROWS = 160
-PART = 80
 NEAR = 8
-VMEM_LIMIT = 50 * 1024 * 1024
+VMEM_LIMIT = 24 * 1024 * 1024
+MIXING_LIMIT = 50 * 1024 * 1024
 
 
 def sent_to_all(array, axis):
@@ -157,7 +157,7 @@
 
 def mixing_kernel(
     latent_ref, context_ref, stats_ref, rows_ref, gain_ref,
-    upper_ref, lower_ref, wd_ref, bias_ref, shift_ref,
+    weight_ref, wd_ref, bias_ref, shift_ref,
     qkv_ref, pairs_ref, send_ref, acc,
 ):
     step = pl.program_id(0)
@@ -181,18 +181,18 @@
             parts.append((x * scale + shift).astype(bf16))
         return jnp.concatenate(parts, axis=1)
 
-    held = [
-        [
-            jnp.concatenate([upper_ref[cut, j], lower_ref[cut, j]], axis=0)
-            for cut in range(upper_ref.shape[0])
-        ]
-        for j in range(upper_ref.shape[1])
-    ]
     quarter = HEAD_ROWS // 5
 
     def weight(n):
         rows = slice(n * quarter, (n + 1) * quarter)
-        return jnp.concatenate([part[rows] for cuts in held for part in cuts], axis=0)
+        return jnp.concatenate(
+            [
+                weight_ref[cut, j, rows]
+                for j in range(weight_ref.shape[1])
+                for cut in range(weight_ref.shape[0])
+            ],
+            axis=0,
+        )
 
     w_qk = jnp.concatenate([weight(0), weight(1)], axis=1)
     w_v = jnp.concatenate([weight(2), weight(3)], axis=1)
@@ -294,13 +294,9 @@
             whole(T + C, 128),
             pl.BlockSpec((1, *rows.shape[1:]), lambda i: (i, 0, 0)),
             pl.BlockSpec((1, 1, depth), lambda i: (i, 0, 0)),
-            *[
-                pl.BlockSpec(
-                    (CUTS, gathered.shape[1] // steps, PART, 128),
-                    lambda i, b=b: (0, i, b, 0),
-                )
-                for b in (1, 2)
-            ],
+            pl.BlockSpec(
+                (CUTS, gathered.shape[1] // steps, HEAD_ROWS, 128), lambda i: (0, i, 0, 0)
+            ),
             whole(128, 128),
             whole(2, 128),
             whole(2, T),
@@ -312,10 +308,10 @@
             jax.ShapeDtypeStruct((NEAR, 3 * 256 // NEAR, 128), bf16),
         ],
         scratch_shapes=[pltpu.VMEM((T + 16, 640), f32)],
-        compiler_params=pltpu.CompilerParams(vmem_limit_bytes=VMEM_LIMIT),
+        compiler_params=pltpu.CompilerParams(vmem_limit_bytes=MIXING_LIMIT),
         name="mixing",
     )(
-        latent, context, scales, rows, gain.reshape(steps, 1, depth), gathered, gathered,
+        latent, context, scales, rows, gain.reshape(steps, 1, depth), gathered,
         w_decay.reshape(128, 128), decay_bias, decay_shift.T,
     )
 
@@ -467,6 +463,7 @@
         ],
         in_specs=[vmem],
         out_specs=[vmem] * 3,
+        compiler_params=pltpu.CompilerParams(vmem_limit_bytes=VMEM_LIMIT),
         name="near",
     )(received)
     totals = lax.all_gather(total, "sp", axis_index_groups=far)
@@ -475,6 +472,7 @@
         out_shape=jax.ShapeDtypeStruct((n, slab, 128), bf16),
         in_specs=[vmem] * 3,
         out_specs=vmem,
+        compiler_params=pltpu.CompilerParams(vmem_limit_bytes=VMEM_LIMIT),
         name="far",
     )(totals, state, decay)
     return lax.all_to_all(
@@ -551,7 +549,7 @@
                 constant_block(256, 128),
                 constant_block(1, 256),
                 pl.BlockSpec(
-                    (CUTS, width // 128, PART, 128),
+                    (CUTS, width // 128, OUT_ROWS, 128),
                     lambda i, order: (0, order[i], 0, 0),
                 ),
             ],
@@ -581,7 +579,7 @@
                 constant_block(T, 256),
                 pl.BlockSpec((1, T, width), lambda i, order: (i, 0, 0)),
                 pl.BlockSpec(
-                    (CUTS, width // 128, PART, 128),
+                    (CUTS, width // 128, OUT_ROWS, 128),
                     lambda i, order: (0, order[i], 0, 0),
                 ),
             ],
@@ -653,11 +651,14 @@
     own = prepare(
         cond_latent, cond_context, mod_weight, w_query, w_key, w_value, w_rank, w_out
     ).astype(f16)
-    everyone = lax.all_gather(own, "sp", axis=1, tiled=True).astype(bf16)
-    gathered = everyone.reshape(CUTS, members, own.shape[1], 128)
+    everyone = lax.all_gather(own, "sp", axis=1, tiled=True)
+    everyone = everyone.reshape(CUTS, members, own.shape[1], 128)
+    heads = OUT_ROWS + TERM_ROWS
     lines = 5 * mod_weight.shape[2] // 128
-    sums = gathered[:, :, OUT_ROWS : OUT_ROWS + TERM_ROWS].astype(f32).sum(axis=1).reshape(-1, 128)
+    sums = everyone[:, :, OUT_ROWS:heads].astype(f32).sum(axis=1).reshape(-1, 128)
     summed_terms = (sums[:lines] + sums[lines : 2 * lines]) * (1.0 / TERM_SCALE)
+    out_gathered = everyone[:, :, :OUT_ROWS].astype(bf16)
+    gathered = everyone[:, :, heads:].astype(bf16)
     rows = sent_to_all(summed_terms, "tp")
     gate = summed_terms.reshape(5, -1)[2]
 
@@ -673,9 +674,9 @@
     order = 2 * ((place // 2 + jnp.arange(chips)) % chips) + place % 2
     normed, sent = sent_parts(
         order ^ 1, loc, lift, entries.reshape(256, 128), out_gain.reshape(1, 256),
-        gathered, columns,
-    )
-    sums = kept_parts(order, normed, to_partner(sent), gathered, columns)
+        out_gathered, columns,
+    )
+    sums = kept_parts(order, normed, to_partner(sent), out_gathered, columns)
     own_latent = lax.dynamic_slice_in_dim(latent, place * columns, columns, 1)
     summed = sums[0].astype(f32)
     for i in range(1, chips):

time: 315 us -> 302 us (0.959)
  blocking collectives: 189 us -> 169 us
  waiting for transfers between devices: 24.3 us -> 34.1 us
  Pallas kernels: 26.5 us -> 21.4 us
    all_to_all x1 -> x0, blocking collectives: 16.5 us -> none  [states_before(): lax.all_to_all(sent, 'sp', split_axis=0, concat_axis=0, tiled=True, axis_...]
    all_to_all x0 -> x1, waiting for transfers between devices: none -> 12.9 us  [states_before(): lax.all_to_all(sent, 'sp', split_axis=0, concat_axis=0, tiled=True, axis_...]
    all_to_all x1, waiting for transfers between devices: 4.48 us -> 0.01 us  [sent_to_all(): return lax.all_to_all(copies, axis, split_axis=0, concat_axis=0, tiled=True)]
    ppermute x6, waiting for transfers between devices: 9.96 us -> 13.9 us  [to_chip(): lax.ppermute(array, 'tp', [(i, (i + 2 * ahead) % n) for i in range(n)])]
    all_to_all x0 -> x1, starting transfers between devices: none -> 3.73 us  [states_before(): lax.all_to_all(sent, 'sp', split_axis=0, concat_axis=0, tiled=True, axis_...]
    convert_element_type x1 -> x2, other arithmetic: 7.79 us -> 8.1 us  [the longest x1 5.99 us: local(): gathered = everyone[:, :, heads:].astype(bf16)]
  transfers between devices with their start and end apart: 13 -> 14, of which waited for: 7 -> 7; matrix products, arithmetic and copies ran while one was open for 0% -> 3% of each run, Pallas kernels for 1% -> 1%
where the time goes in v6:
time: 302 us; the launch traced here: 301 us
  blocking collectives  169 us (56%)
  starting transfers between devices  62.6 us (21%)
  waiting for transfers between devices  34.1 us (11%)
  Pallas kernels  21.4 us (7%)
  other arithmetic  10.4 us (3%)
  local copies, waits for them, and re-layouts  3.75 us (1%)
    all_gather x1, blocking collectives, local(): everyone = lax.all_gather(own, 'sp', axis=1, tiled=True)  145 us
    all_gather x1, blocking collectives, states_before(): totals = lax.all_gather(total, 'sp', axis_index_groups=far)  24.3 us
    ppermute x5, starting transfers between devices, to_partner(): return lax.ppermute(array, 'tp', [(i, i ^ 1) for i in range(n)])  19.5 us
    ppermute x6, starting transfers between devices, to_chip(): lax.ppermute(array, 'tp', [(i, (i + 2 * ahead) % n) for i in range(n)])  17.1 us
    all_to_all x1, starting transfers between devices, sent_to_all(): return lax.all_to_all(copies, axis, split_axis=0, concat_axis=0, tiled=True)  16.3 us
    ppermute x6, waiting for transfers between devices, to_chip(): lax.ppermute(array, 'tp', [(i, (i + 2 * ahead) % n) for i in range(n)])  13.9 us
    all_to_all x1, waiting for transfers between devices, states_before(): lax.all_to_all(sent, 'sp', split_axis=0, concat_axis=0, tiled=True, axis_...  12.9 us
    pallas_call x1, Pallas kernels, mixing(): pl.pallas_call(mixing_kernel, grid=(steps,), in_specs=[pl.BlockSpec((T, d...  8.48 us
  transfers between devices with their start and end apart: 14, of which 7 were waited for; matrix products, arithmetic and copies ran while one was open for 3% of the time, Pallas kernels for 1%

profile of v6, /device:TPU:33, one launch (start us, length us, event | category | flops | bytes accessed | tf_op | source)
XLA Modules:
  0.0 301.4 jit_solution(3476471738414586567)
XLA Ops:
  3.1 144.5 %all-gather.2 = f16[4,7680,128]{2,1,0:T(8,128)(2,1)S(1)} all-gather(f16[4,240,128]{2,1,0:T(8,128)(2,1)S(1)} %convert_element_type.31), channel_id=1, replica_groups=mesh['grp'=2,'sp'=32,'tp'=8] {'sp'}, dimensions={1}, use_global_device_ids=true | all-gather | bytes 8110080 | tf_op jit(solution)/shard_map/all_gather | solution.py:654
  147.7 3.1 %copy-done.7 = f16[4,7680,128]{2,1,0:T(8,128)(2,1)} copy-done((f16[4,7680,128]{2,1,0:T(8,128)(2,1)}, f16[4,7680,128]{2,1,0:T(8,128)(2,1)S(1)}, u32[]{:S(2)}) %copy-start.7) | copy-done | bytes 7864344
  151.5 16.3 %all-to-all-start = ((f32[8,20,128]{2,1,0:T(8,128)}), f32[8,20,128]{2,1,0:T(8,128)S(1)}, u32[]{:S(2)}, u32[]{:S(2)}) async-start(f32[8,20,128]{2,1,0:T(8,128)} %broadcast_in_dim.3), calls=%async_computation | async-start | bytes 196608 | tf_op jit(solution)/shard_map/all_to_all | solution.py:28
  167.8 6.0 %slice_convert_fusion.weight_ref = bf16[4,32,160,128]{3,2,1,0:T(8,128)(2,1)} fusion(f16[4,32,240,128]{3,2,1,0:T(8,128)(2,1)} %bitcast.22), kind=kLoop, calls=%fused_computation | loop fusion | flops 2621440 | bytes 10485760 | tf_op jit(solution)/shard_map/convert_element_type | solution.py:661
  174.4 8.5 %mixing.1 = (bf16[256,512]{1,0:T(8,128)(2,1)S(1)}, bf16[256,512]{1,0:T(8,128)(2,1)S(1)}, bf16[8,96,128]{2,1,0:T(8,128)(2,1)}) custom-call(bf16[256,4096]{1,0:T(8,128)(2,1)S(1)} %copy-done, bf16[8,4096]{1,0:T(8,128)(2,1)S(1)} %copy-done.1, f32[264,128]{1,0:T(8,128)S(1)} %stats.1.stats_ref, f32[8,20,128]{2,1,0:T(8,128)S(1)} %all-to-all-done.rows_ref, ...), custom_call_target="tpu_custom_call" | custom-call | tf_op jit(solution)/shard_map/mixing/pallas_call | solution.py:288
  182.9 3.7 %all-to-all-start.1 = ((bf16[8,96,128]{2,1,0:T(8,128)(2,1)}), bf16[8,96,128]{2,1,0:T(8,128)(2,1)S(1)}, u32[]{:S(2)}, u32[]{:S(2)}) async-start(bf16[8,96,128]{2,1,0:T(8,128)(2,1)} %get-tuple-element.23), calls=%async_computation.1 | async-start | bytes 393216 | tf_op jit(solution)/shard_map/all_to_all | solution.py:454
  186.6 12.9 %all-to-all-done.1.in_ref = bf16[8,96,128]{2,1,0:T(8,128)(2,1)S(1)} async-done(((bf16[8,96,128]{2,1,0:T(8,128)(2,1)}), bf16[8,96,128]{2,1,0:T(8,128)(2,1)S(1)}, u32[]{:S(2)}, u32[]{:S(2)}) %all-to-all-start.1) | async-done | bytes 196640 | tf_op jit(solution)/shard_map/all_to_all | solution.py:454
  199.7 24.3 %all-gather = bf16[384,128]{1,0:T(8,128)(2,1)S(1)} all-gather(bf16[96,128]{1,0:T(8,128)(2,1)S(1)} %get-tuple-element.24), channel_id=2, replica_groups={{0,64,128,192},{8,72,136,200},{16,80,144,208},{24,88,152,216},{32,96,16..., dimensions={0}, use_global_device_ids=true | all-gather | bytes 122880 | tf_op jit(solution)/shard_map/all_gather | solution.py:469
  224.9 5.9 %all-to-all-start.2 = ((bf16[8,32,128]{2,1,0:T(8,128)(2,1)}), bf16[8,32,128]{2,1,0:T(8,128)(2,1)S(1)}, u32[]{:S(2)}, u32[]{:S(2)}) async-start(bf16[8,32,128]{2,1,0:T(8,128)(2,1)} %far.1), calls=%async_computation.2 | async-start | bytes 131072 | tf_op jit(solution)/shard_map/all_to_all | solution.py:478
  232.9 3.6 %scores.1 = (f32[256,256]{1,0:T(8,128)S(1)}, bf16[256,256]{1,0:T(8,128)(2,1)S(1)}) custom-call(bf16[256,512]{1,0:T(8,128)(2,1)S(1)} %get-tuple-element.19.qkv_ref, bf16[256,512]{1,0:T(8,128)(2,1)S(1)} %get-tuple-element.20.pairs_ref), custom_call_target="tpu_custom_call" | custom-call | flops 1342177280 | bytes 1048576 | tf_op jit(solution)/shard_map/scores/pallas_call | solution.py:371
  236.6 4.0 %all-to-all-done.2 = bf16[8,32,128]{2,1,0:T(8,128)(2,1)S(1)} async-done(((bf16[8,32,128]{2,1,0:T(8,128)(2,1)}), bf16[8,32,128]{2,1,0:T(8,128)(2,1)S(1)}, u32[]{:S(2)}, u32[]{:S(2)}) %all-to-all-start.2) | async-done | bytes 65568 | tf_op jit(solution)/shard_map/all_to_all | solution.py:478
  242.7 6.9 %collective-permute-start = (bf16[4,256,512]{2,1,0:T(8,128)(2,1)S(1)}, bf16[4,256,512]{2,1,0:T(8,128)(2,1)S(1)}, u32[]{:S(2)}, u32[]{:S(2)}) collective-permute-start(bf16[4,256,512]{2,1,0:T(8,128)(2,1)S(1)} %get-tuple-element.28), channel_id=1, source_target_pairs={{0,1},{1,0},{2,3},{3,2},{4,5},{5,4},{6,7},{7,6},{8,9},{9,8},{10,11... | collective-permute-start | bytes 3145736 | tf_op jit(solution)/shard_map/ppermute | solution.py:622
  249.6 2.3 collective-permute-done.received_ref
  253.9 4.8 %collective-permute-start.3 = (bf16[256,512]{1,0:T(8,128)(2,1)S(1)}, bf16[256,512]{1,0:T(8,128)(2,1)S(1)}, u32[]{:S(2)}, u32[]{:S(2)}) collective-permute-start(bf16[256,512]{1,0:T(8,128)(2,1)S(1)} %get-tuple-element.32), channel_id=1, source_target_pairs={{0,6},{1,7},{2,0},{3,1},{4,2},{5,3},{6,4},{7,5},{8,14},{9,15},{10,... | collective-permute-start | bytes 786440 | tf_op jit(solution)/shard_map/ppermute | solution.py:627
  258.7 2.5 collective-permute-start.2
  261.3 2.5 collective-permute-start.1
  263.8 5.7 %collective-permute-done.3 = bf16[256,512]{1,0:T(8,128)(2,1)S(1)} collective-permute-done((bf16[256,512]{1,0:T(8,128)(2,1)S(1)}, bf16[256,512]{1,0:T(8,128)(2,1)S(1)}, u32[]{:S(2)}, u32[]{:S(2)}) %collective-permute-start.3) | collective-permute-done | bytes 262176 | tf_op jit(solution)/shard_map/ppermute | solution.py:627
  269.5 6.5 %collective-permute-done.1 = bf16[256,512]{1,0:T(8,128)(2,1)S(1)} collective-permute-done((bf16[256,512]{1,0:T(8,128)(2,1)S(1)}, bf16[256,512]{1,0:T(8,128)(2,1)S(1)}, u32[]{:S(2)}, u32[]{:S(2)}) %collective-permute-start.1) | collective-permute-done | bytes 262176 | tf_op jit(solution)/shard_map/ppermute | solution.py:627
  279.1 2.5 collective-permute-start.5
  281.6 2.8 collective-permute-start.6
  284.5 3.2 %collective-permute-start.7 = (bf16[256,512]{1,0:T(8,128)(2,1)S(1)}, bf16[256,512]{1,0:T(8,128)(2,1)S(1)}, u32[]{:S(2)}, u32[]{:S(2)}) collective-permute-start(bf16[256,512]{1,0:T(8,128)(2,1)S(1)} %add_convert_fusion.refs_0_), channel_id=1, source_target_pairs={{0,1},{1,0},{2,3},{3,2},{4,5},{5,4},{6,7},{7,6},{8,9},{9,8},{10,11... | collective-permute-start | bytes 786440 | tf_op jit(solution)/shard_map/ppermute | solution.py:622
  287.7 3.0 collective-permute-start.8
  290.7 4.0 %collective-permute-start.9 = (bf16[256,512]{1,0:T(8,128)(2,1)S(1)}, bf16[256,512]{1,0:T(8,128)(2,1)S(1)}, u32[]{:S(2)}, u32[]{:S(2)}) collective-permute-start(bf16[256,512]{1,0:T(8,128)(2,1)S(1)} %collective-permute-done.5.refs_2_), channel_id=1, source_target_pairs={{0,1},{1,0},{2,3},{3,2},{4,5},{5,4},{6,7},{7,6},{8,9},{9,8},{10,11... | collective-permute-start | bytes 786440 | tf_op jit(solution)/shard_map/ppermute | solution.py:622
  296.4 2.4 collective-permute-start.10
  (40 shorter events, 19.1 us)
Async XLA Ops:
  147.7 3.1 %copy-start.7 = (f16[4,7680,128]{2,1,0:T(8,128)(2,1)}, f16[4,7680,128]{2,1,0:T(8,128)(2,1)S(1)}, u32[]{:S(2)}) copy-start(f16[4,7680,128]{2,1,0:T(8,128)(2,1)S(1)} %all-gather.2) | copy-start | bytes 23592964
  151.5 22.9 %all-to-all-start = ((f32[8,20,128]{2,1,0:T(8,128)}), f32[8,20,128]{2,1,0:T(8,128)S(1)}, u32[]{:S(2)}, u32[]{:S(2)}) async-start(f32[8,20,128]{2,1,0:T(8,128)} %broadcast_in_dim.3), calls=%async_computation | async-start | bytes 196608 | tf_op jit(solution)/shard_map/all_to_all | solution.py:28
  167.8 6.0 %copy-start = (bf16[256,4096]{1,0:T(8,128)(2,1)S(1)}, bf16[256,4096]{1,0:T(8,128)(2,1)}, u32[]{:S(2)}) copy-start(bf16[256,4096]{1,0:T(8,128)(2,1)} %latent_ref.3) | copy-start | bytes 6291460
  167.8 6.0 %copy-start.1 = (bf16[8,4096]{1,0:T(8,128)(2,1)S(1)}, bf16[8,4096]{1,0:T(8,128)(2,1)}, u32[]{:S(2)}) copy-start(bf16[8,4096]{1,0:T(8,128)(2,1)} %context_ref.3) | copy-start | bytes 196612
  167.8 6.6 %copy-start.2 = (bf16[2,64,128]{2,1,0:T(8,128)(2,1)S(1)}, bf16[2,64,128]{2,1,0:T(8,128)(2,1)}, u32[]{:S(2)}) copy-start(bf16[2,64,128]{2,1,0:T(8,128)(2,1)} %param.25) | copy-start | bytes 98308
  167.8 6.6 %copy-start.3 = (f32[4096]{0:T(1024)S(1)}, f32[4096]{0:T(1024)}, u32[]{:S(2)}) copy-start(f32[4096]{0:T(1024)} %param.20) | copy-start | bytes 49156
  167.8 6.6 %copy-start.4 = (f32[256,2]{0,1:T(2,128)S(1)}, f32[256,2]{0,1:T(2,128)}, u32[]{:S(2)}) copy-start(f32[256,2]{0,1:T(2,128)} %param.27) | copy-start | bytes 6148
  167.8 6.6 %copy-start.5 = (f32[2,128]{1,0:T(2,128)S(1)}, f32[2,128]{1,0:T(2,128)}, u32[]{:S(2)}) copy-start(f32[2,128]{1,0:T(2,128)} %bias_ref.1) | copy-start | bytes 3076
  182.9 57.7 %copy-start.6 = (f32[256]{0:T(256)S(1)}, f32[256]{0:T(256)}, u32[]{:S(2)}) copy-start(f32[256]{0:T(256)} %param.28) | copy-start | bytes 3076
  182.9 16.6 %all-to-all-start.1 = ((bf16[8,96,128]{2,1,0:T(8,128)(2,1)}), bf16[8,96,128]{2,1,0:T(8,128)(2,1)S(1)}, u32[]{:S(2)}, u32[]{:S(2)}) async-start(bf16[8,96,128]{2,1,0:T(8,128)(2,1)} %get-tuple-element.23), calls=%async_computation.1 | async-start | bytes 393216 | tf_op jit(solution)/shard_map/all_to_all | solution.py:454
  224.9 15.6 %all-to-all-start.2 = ((bf16[8,32,128]{2,1,0:T(8,128)(2,1)}), bf16[8,32,128]{2,1,0:T(8,128)(2,1)S(1)}, u32[]{:S(2)}, u32[]{:S(2)}) async-start(bf16[8,32,128]{2,1,0:T(8,128)(2,1)} %far.1), calls=%async_computation.2 | async-start | bytes 131072 | tf_op jit(solution)/shard_map/all_to_all | solution.py:478
  242.7 9.1 %collective-permute-start = (bf16[4,256,512]{2,1,0:T(8,128)(2,1)S(1)}, bf16[4,256,512]{2,1,0:T(8,128)(2,1)S(1)}, u32[]{:S(2)}, u32[]{:S(2)}) collective-permute-start(bf16[4,256,512]{2,1,0:T(8,128)(2,1)S(1)} %get-tuple-element.28), channel_id=1, source_target_pairs={{0,1},{1,0},{2,3},{3,2},{4,5},{5,4},{6,7},{7,6},{8,9},{9,8},{10,11... | collective-permute-start | bytes 3145736 | tf_op jit(solution)/shard_map/ppermute | solution.py:622
  253.9 15.6 %collective-permute-start.3 = (bf16[256,512]{1,0:T(8,128)(2,1)S(1)}, bf16[256,512]{1,0:T(8,128)(2,1)S(1)}, u32[]{:S(2)}, u32[]{:S(2)}) collective-permute-start(bf16[256,512]{1,0:T(8,128)(2,1)S(1)} %get-tuple-element.32), channel_id=1, source_target_pairs={{0,6},{1,7},{2,0},{3,1},{4,2},{5,3},{6,4},{7,5},{8,14},{9,15},{10,... | collective-permute-start | bytes 786440 | tf_op jit(solution)/shard_map/ppermute | solution.py:627
  258.7 10.7 %collective-permute-start.2 = (bf16[256,512]{1,0:T(8,128)(2,1)S(1)}, bf16[256,512]{1,0:T(8,128)(2,1)S(1)}, u32[]{:S(2)}, u32[]{:S(2)}) collective-permute-start(bf16[256,512]{1,0:T(8,128)(2,1)S(1)} %get-tuple-element.31), channel_id=1, source_target_pairs={{0,4},{1,5},{2,6},{3,7},{4,0},{5,1},{6,2},{7,3},{8,12},{9,13},{10,... | collective-permute-start | bytes 786440 | tf_op jit(solution)/shard_map/ppermute | solution.py:627
  261.3 14.8 %collective-permute-start.1 = (bf16[256,512]{1,0:T(8,128)(2,1)S(1)}, bf16[256,512]{1,0:T(8,128)(2,1)S(1)}, u32[]{:S(2)}, u32[]{:S(2)}) collective-permute-start(bf16[256,512]{1,0:T(8,128)(2,1)S(1)} %get-tuple-element.30), channel_id=1, source_target_pairs={{0,2},{1,3},{2,4},{3,5},{4,6},{5,7},{6,0},{7,1},{8,10},{9,11},{10,... | collective-permute-start | bytes 786440 | tf_op jit(solution)/shard_map/ppermute | solution.py:627
  277.2 10.6 %collective-permute-start.4 = (bf16[256,512]{1,0:T(8,128)(2,1)S(1)}, bf16[256,512]{1,0:T(8,128)(2,1)S(1)}, u32[]{:S(2)}, u32[]{:S(2)}) collective-permute-start(bf16[256,512]{1,0:T(8,128)(2,1)S(1)} %add_convert_fusion.refs_0_), channel_id=1, source_target_pairs={{0,6},{1,7},{2,0},{3,1},{4,2},{5,3},{6,4},{7,5},{8,14},{9,15},{10,... | collective-permute-start | bytes 786440 | tf_op jit(solution)/shard_map/ppermute | solution.py:627
  279.1 11.6 %collective-permute-start.5 = (bf16[256,512]{1,0:T(8,128)(2,1)S(1)}, bf16[256,512]{1,0:T(8,128)(2,1)S(1)}, u32[]{:S(2)}, u32[]{:S(2)}) collective-permute-start(bf16[256,512]{1,0:T(8,128)(2,1)S(1)} %add_convert_fusion.refs_0_), channel_id=1, source_target_pairs={{0,4},{1,5},{2,6},{3,7},{4,0},{5,1},{6,2},{7,3},{8,12},{9,13},{10,... | collective-permute-start | bytes 786440 | tf_op jit(solution)/shard_map/ppermute | solution.py:627
  281.6 14.8 %collective-permute-start.6 = (bf16[256,512]{1,0:T(8,128)(2,1)S(1)}, bf16[256,512]{1,0:T(8,128)(2,1)S(1)}, u32[]{:S(2)}, u32[]{:S(2)}) collective-permute-start(bf16[256,512]{1,0:T(8,128)(2,1)S(1)} %add_convert_fusion.refs_0_), channel_id=1, source_target_pairs={{0,2},{1,3},{2,4},{3,5},{4,6},{5,7},{6,0},{7,1},{8,10},{9,11},{10,... | collective-permute-start | bytes 786440 | tf_op jit(solution)/shard_map/ppermute | solution.py:627
  284.5 14.3 %collective-permute-start.7 = (bf16[256,512]{1,0:T(8,128)(2,1)S(1)}, bf16[256,512]{1,0:T(8,128)(2,1)S(1)}, u32[]{:S(2)}, u32[]{:S(2)}) collective-permute-start(bf16[256,512]{1,0:T(8,128)(2,1)S(1)} %add_convert_fusion.refs_0_), channel_id=1, source_target_pairs={{0,1},{1,0},{2,3},{3,2},{4,5},{5,4},{6,7},{7,6},{8,9},{9,8},{10,11... | collective-permute-start | bytes 786440 | tf_op jit(solution)/shard_map/ppermute | solution.py:622
  287.7 11.1 %collective-permute-start.8 = (bf16[256,512]{1,0:T(8,128)(2,1)S(1)}, bf16[256,512]{1,0:T(8,128)(2,1)S(1)}, u32[]{:S(2)}, u32[]{:S(2)}) collective-permute-start(bf16[256,512]{1,0:T(8,128)(2,1)S(1)} %collective-permute-done.4.refs_1_), channel_id=1, source_target_pairs={{0,1},{1,0},{2,3},{3,2},{4,5},{5,4},{6,7},{7,6},{8,9},{9,8},{10,11... | collective-permute-start | bytes 786440 | tf_op jit(solution)/shard_map/ppermute | solution.py:622
  290.7 8.1 %collective-permute-start.9 = (bf16[256,512]{1,0:T(8,128)(2,1)S(1)}, bf16[256,512]{1,0:T(8,128)(2,1)S(1)}, u32[]{:S(2)}, u32[]{:S(2)}) collective-permute-start(bf16[256,512]{1,0:T(8,128)(2,1)S(1)} %collective-permute-done.5.refs_2_), channel_id=1, source_target_pairs={{0,1},{1,0},{2,3},{3,2},{4,5},{5,4},{6,7},{7,6},{8,9},{9,8},{10,11... | collective-permute-start | bytes 786440 | tf_op jit(solution)/shard_map/ppermute | solution.py:622
  296.4 3.6 %collective-permute-start.10 = (bf16[256,512]{1,0:T(8,128)(2,1)S(1)}, bf16[256,512]{1,0:T(8,128)(2,1)S(1)}, u32[]{:S(2)}, u32[]{:S(2)}) collective-permute-start(bf16[256,512]{1,0:T(8,128)(2,1)S(1)} %collective-permute-done.6.refs_3_), channel_id=1, source_target_pairs={{0,1},{1,0},{2,3},{3,2},{4,5},{5,4},{6,7},{7,6},{8,9},{9,8},{10,11... | collective-permute-start | bytes 786440 | tf_op jit(solution)/shard_map/ppermute | solution.py:622
